TPU v7x, 256 devices: a whole 4x4x8 slice. The times are simulated.
256 devices in a mesh: sp: 64 (over z, y, core), tp: 4 (over x).
Axes of the slice: x: 4, y: 4, z: 8, core: 2. Of those that a mesh axis runs over, the one named last changes fastest.
Arguments:
- tokens: bfloat16 [16384, 2048], P(('sp', 'tp')), may hold values from -6 to 6
- norm_gain: float32 [2048], replicated, may hold values from 0.1 to 6, as said below
- query_weight: bfloat16 [2048, 16, 128], P(None, 'tp'), may hold values from -0.21875 to 0.21875
- key_weight: bfloat16 [2048, 4, 128], P(None, 'tp'), may hold values from -0.125 to 0.125
- value_weight: bfloat16 [2048, 4, 128], P(None, 'tp'), may hold values from -0.125 to 0.125
- mix_lambda: float32 [16], P('tp'), may hold values from 0.3 to 0.8
- head_gain: float32 [128], replicated, may hold values from 0.1 to 1.9
- pool_weight: bfloat16 [2048, 4, 512], P(None, 'tp'), may hold values from -0.125 to 0.125
- pool_mix: bfloat16 [4, 512, 512], P('tp'), may hold values from -0.25 to 0.25
- pool_scale: float32 [4, 512], P('tp'), may hold values from 0.1 to 1.9
- gate_weight: bfloat16 [2048, 2, 2048], P(None, None, 'tp'), may hold values from -0.125 to 0.125
- out_weight: bfloat16 [2048, 2048], P('tp'), may hold values from -0.125 to 0.125
Outputs:
- mixed: bfloat16 [16384, 2048], P(('sp', 'tp'))
- log_sums: float32 [2, 16, 16384], P(None, 'tp', 'sp')
Inputs may be any that keep to these rules, and one draw needn't show every extreme that they name: `norm_gain`: positive.
All inputs are finite; a program needn't handle non-finite values.
Results may differ from a plain program's by a relative error of at most 0.013.
Values may be sent and summed in bfloat16 or wider, within the bound.
No kernel may reach another device: no remote copies, remote signals or barrier semaphores. Data moves between devices by JAX's collectives and lax.ppermute only.
A program may use at most 128 MiB of HBM per device.

v0:
```python
import math

import jax
import jax.numpy as jnp
from jax import lax
from jax.sharding import PartitionSpec as P

WINDOW = 16


NORM_EPS = 1e-06


def copy_for_each(array, axis):
    size = lax.axis_size(axis)
    return lax.all_to_all(
        jnp.broadcast_to(array[None], (size, *array.shape)), axis, 0, 0, tiled=True
    )


def laid_out(pieces, dim):
    shape = list(pieces.shape[1:])
    shape[dim] *= pieces.shape[0]
    return jnp.moveaxis(pieces, 0, dim).reshape(shape)


def collect(array, axis, dim):
    pieces = copy_for_each(array, axis)
    return laid_out(pieces, dim)


def sent_together(arrays, axis, dim, along):
    ends, at = ([], 0)
    for a in arrays[:-1]:
        at += a.shape[along]
        ends.append(at)
    both = jnp.concatenate(arrays, axis=along)
    return tuple(jnp.split(lax.all_gather(both, axis, axis=dim, tiled=True), ends, axis=along))


def shifted(block, axis, distance):
    devices = range(lax.axis_size(axis))
    route = [(i - distance, i) for i in devices if i - distance in devices]
    return lax.ppermute(block, axis, route)


def cut_along(array, dim, size):
    before, after = (array.shape[:dim], array.shape[dim + 1 :])
    return jnp.moveaxis(array.reshape(*before, size, -1, *after), dim, 0)


def sent_and_summed(array, axis, dim):
    size = lax.axis_size(axis)
    pieces = lax.all_to_all(cut_along(array, dim, size), axis, 0, 0, tiled=True)
    return jnp.sum(pieces.astype(jnp.float32), axis=0)


def attend(
    queries, key_buffer, value_buffer, key_start, query_start, weight_lambda, head_dim, value_dim
):
    tok_rows, kv_local, group_size = (queries.shape[0], queries.shape[1], queries.shape[2])
    total_keys = key_buffer.shape[0]
    block_keys = math.gcd(total_keys, 512)
    keys_split = key_buffer.reshape(total_keys, kv_local, 2, head_dim)
    values_split = value_buffer.reshape(total_keys, kv_local, value_dim)
    query_pos = query_start + jnp.arange(tok_rows, dtype=jnp.int32)
    score_scale = head_dim ** (-0.5)
    low_index = jnp.maximum(0, -key_start)
    high_index = query_start + tok_rows
    first_block = low_index // block_keys
    last_block = (high_index + block_keys - 1) // block_keys

    def online_step(block_index, carry):
        running_max, running_sum, accum = carry
        key_begin = block_index * block_keys
        block_keys_arr = lax.dynamic_slice_in_dim(keys_split, key_begin, block_keys, 0)
        scores = (
            jnp.einsum(
                "qgrmd,kgmd->grmqk", queries, block_keys_arr, preferred_element_type=jnp.float32
            )
            * score_scale
        )
        key_pos = key_begin + jnp.arange(block_keys, dtype=jnp.int32)
        visible = (key_pos[None, :] <= query_pos[:, None]) & (key_pos[None, :] >= 0)
        block_max = jnp.max(jnp.where(visible, scores, -1e30), axis=4)
        new_max = jnp.maximum(running_max, block_max)
        rescale = jnp.exp(running_max - new_max)
        probs = jnp.where(visible, jnp.exp(scores - new_max[..., None]), 0.0)
        new_sum = running_sum * rescale + jnp.sum(probs, axis=4)
        block_values = lax.dynamic_slice_in_dim(values_split, key_begin, block_keys, 0)
        new_accum = accum * rescale[..., None] + jnp.einsum(
            "grmqk,kgd->grmqd",
            probs.astype(jnp.bfloat16),
            block_values,
            preferred_element_type=jnp.float32,
        )
        return (new_max, new_sum, new_accum)

    start_carry = (
        jnp.full((kv_local, group_size, 2, tok_rows), -1e30, jnp.float32),
        jnp.zeros((kv_local, group_size, 2, tok_rows), jnp.float32),
        jnp.zeros((kv_local, group_size, 2, tok_rows, value_dim), jnp.float32),
    )
    running_max, running_sum, accum = lax.fori_loop(
        first_block, last_block, online_step, start_carry
    )
    first_map = accum[:, :, 0] / running_sum[:, :, 0, :, None]
    second_map = accum[:, :, 1] / running_sum[:, :, 1, :, None]
    head_out = first_map - weight_lambda[:, :, None, None] * second_map
    log_sums = running_max + jnp.log(running_sum)
    return (head_out, log_sums)


def finish_heads(head_out, log_sums, head_gain, heads_local, value_dim):
    tok_rows = head_out.shape[2]
    head_outs = head_out.reshape(heads_local, tok_rows, value_dim)
    normed_heads = (
        head_outs
        * lax.rsqrt(jnp.mean(head_outs * head_outs, axis=2, keepdims=True) + NORM_EPS)
        * head_gain
    )
    attended = jnp.transpose(normed_heads, (1, 0, 2)).reshape(tok_rows, heads_local * value_dim)
    log_out = jnp.transpose(log_sums.reshape(heads_local, 2, tok_rows), (1, 0, 2))
    return (attended, log_out)


def local(
    tokens,
    norm_gain,
    query_weight,
    key_weight,
    value_weight,
    mix_lambda,
    head_gain,
    pool_weight,
    pool_mix,
    pool_scale,
    gate_weight,
    out_weight,
):
    model_width = tokens.shape[1]
    heads_local = query_weight.shape[1]
    kv_local = key_weight.shape[1]
    head_dim = query_weight.shape[2] // 2
    value_dim = value_weight.shape[2]
    groups_local = pool_weight.shape[1]
    group_width = pool_weight.shape[2]
    channels = gate_weight.shape[2]
    matrices = (
        query_weight.reshape(model_width, -1),
        key_weight.reshape(model_width, -1),
        value_weight.reshape(model_width, -1),
        pool_weight.reshape(model_width, -1),
        gate_weight.reshape(model_width, -1),
    )

    def project(rows_piece):
        inputs = rows_piece.astype(jnp.float32)
        normed = (
            inputs
            * lax.rsqrt(jnp.mean(inputs * inputs, axis=1, keepdims=True) + NORM_EPS)
            * norm_gain
        ).astype(jnp.bfloat16)
        return jnp.concatenate(
            [
                jnp.dot(normed, matrix, preferred_element_type=jnp.float32).astype(jnp.bfloat16)
                for matrix in matrices
            ],
            axis=1,
        )

    joined = project(collect(tokens, "tp", 0))
    tok_rows = joined.shape[0]
    bounds = [0]
    for matrix in matrices:
        bounds.append(bounds[-1] + matrix.shape[1])
    queries = joined[:, bounds[0] : bounds[1]].reshape(
        tok_rows, kv_local, heads_local // kv_local, 2, head_dim
    )
    keys_own = joined[:, bounds[1] : bounds[2]]
    values_own = joined[:, bounds[2] : bounds[3]]
    pool_in = joined[:, bounds[3] : bounds[4]]
    gate_pre = joined[:, bounds[4] : bounds[5]].reshape(tok_rows, 2, channels)
    rim_rows = pool_in[tok_rows - WINDOW :]
    seq_index = lax.axis_index("sp")
    query_start = seq_index * tok_rows
    key_buffer, value_buffer = sent_together((keys_own, values_own), "sp", 0, 1)
    rim_prev = shifted(rim_rows, "sp", 1)
    key_start = jnp.int32(0)
    lambda_local = mix_lambda.reshape(kv_local, heads_local // kv_local)
    head_out, log_sums = attend(
        queries, key_buffer, value_buffer, key_start, query_start, lambda_local, head_dim, value_dim
    )
    attended, log_out = finish_heads(head_out, log_sums, head_gain, heads_local, value_dim)
    positions = query_start + jnp.arange(tok_rows, dtype=jnp.int32)
    pool_split = pool_in.reshape(tok_rows, groups_local, group_width)
    extended = (
        jnp.concatenate([rim_prev, pool_in], axis=0)
        .astype(jnp.float32)
        .reshape(WINDOW + tok_rows, groups_local, group_width)
    )
    group_index = lax.axis_index("tp") * groups_local + 0
    window_span = jnp.left_shift(jnp.int32(2), group_index)
    window_sum = jnp.zeros((tok_rows, group_width), jnp.float32)
    for back_rows in range(WINDOW):
        window_sum = window_sum + jnp.where(
            back_rows < window_span,
            extended[WINDOW - back_rows : WINDOW - back_rows + tok_rows, 0],
            0.0,
        )
    counts = jnp.minimum(positions + 1, window_span).astype(jnp.float32)
    means = window_sum / counts[:, None]
    pooled = (means - pool_split[:, 0].astype(jnp.float32)).astype(jnp.bfloat16)
    group_parts = jnp.dot(pooled, pool_mix[0], preferred_element_type=jnp.float32) * pool_scale[0]
    merged = (
        jax.nn.sigmoid(gate_pre[:, 0].astype(jnp.float32)) * attended
        + jax.nn.sigmoid(gate_pre[:, 1].astype(jnp.float32)) * group_parts
    ).astype(jnp.bfloat16)
    mixed = sent_and_summed(
        jnp.dot(merged, out_weight, preferred_element_type=jnp.float32).astype(jnp.bfloat16),
        "tp",
        0,
    )
    return (mixed.astype(jnp.bfloat16), log_out)


def solution(mesh):
    in_specs = (
        P(("sp", "tp"), None),
        P(),
        P(None, "tp", None),
        P(None, "tp", None),
        P(None, "tp", None),
        P("tp"),
        P(),
        P(None, "tp", None),
        P("tp", None, None),
        P("tp", None),
        P(None, None, "tp"),
        P("tp", None),
    )
    out_specs = (P(("sp", "tp"), None), P(None, "tp", "sp"))
    return jax.shard_map(local, mesh=mesh, in_specs=in_specs, out_specs=out_specs, check_vma=False)
```

profile of v0, /device:TPU:248, one launch (start us, length us, event | category | flops | bytes accessed | tf_op | source)
XLA Modules:
  0.0 330.0 jit_solution(275592292067196041)
XLA Ops:
  8.5 19.2 %all_to_all.10 = bf16[4,64,2048]{2,1,0:T(8,128)(2,1)S(1)} all-to-all(bf16[4,64,2048]{2,1,0:T(8,128)(2,1)S(1)} %broadcast_in_dim.56), channel_id=1, replica_groups=mesh['sp'=64,'tp'=4] {'tp'}, dimensions={0} | all-to-all | bytes 2097152 | tf_op jit(solution)/shard_map/all_to_all | solution.py:16
  30.0 5.3 %copy.48 = bf16[256,8,2,512]{3,1,2,0:T(8,128)(2,1)} copy(bf16[256,8,2,512]{3,2,1,0:T(2,128)(2,1)} %bitcast.152) | data formatting | bytes 8388608
  35.4 2.3 fusion.36
  39.6 4.3 %convolution_convert_fusion.1 = bf16[256,1024]{1,0:T(8,128)(2,1)} fusion(bf16[256,2048]{1,0:T(8,128)(2,1)S(1)} %bitcast.149, bf16[2048,1024]{1,0:T(8,128)(2,1)} %bitcast.153), kind=kOutput, calls=%fused_computation.41 | convolution fusion | flops 1074003968 | bytes 5767168 | tf_op jit(solution)/shard_map/dot_general | solution.py:166
  46.3 3.1 fusion.39
  53.1 60.7 %all-gather.2.cloned.1.call-done = bf16[16384,256]{0,1:T(8,128)(2,1)} async-done(((bf16[256,256]{0,1:T(8,128)(2,1)}), bf16[16384,256]{0,1:T(8,128)(2,1)}) %all-gather.2.cloned.1.call-update) | async-done | bytes 8388624 | tf_op jit(solution)/shard_map/all_gather | solution.py:38
  113.7 5.8 %slice_bitcast_fusion = (bf16[16384,1,128]{0,2,1:T(8,128)(2,1)}, bf16[16384,128]{0,1:T(8,128)(2,1)}) fusion(bf16[16384,256]{0,1:T(8,128)(2,1)} %all-gather.2.cloned.1.call-done), kind=kLoop, calls=%fused_computation.29 | loop fusion | bytes 16777216 | tf_op jit(solution)/shard_map/reshape | solution.py:65
  119.6 170.0 %while.15 = (s32[]{:T(128)}, f32[1,4,2,256]{3,1,2,0:T(4,128)S(1)}, f32[1,4,2,256]{3,1,2,0:T(4,128)S(1)}, f32[1,4,2,256,128]{4,3,2,1,0:T(8,128)S(1)}, s32[]{:T(12...) while((s32[]{:T(128)}, f32[1,4,2,256]{3,1,2,0:T(4,128)S(1)}, ...), condition=%wide.region_4.5_spmd.clone, body=%wide.region_1.4_spmd.clone.sunk | while | flops 411836160 | bytes 15744191 | solution.py:104
  127.9 2.3 fusion.144
  133.2 2.3 fusion.144
  138.5 2.3 fusion.144
  143.8 2.3 fusion.144
  154.4 2.3 fusion.144
  159.7 2.3 fusion.144
  165.0 2.3 fusion.144
  170.4 2.3 fusion.144
  175.7 2.3 fusion.144
  186.3 2.3 fusion.144
  191.6 2.3 fusion.144
  196.9 2.3 fusion.144
  202.2 2.3 fusion.144
  292.6 9.9 %convolution_convert_fusion = bf16[256,2048]{1,0:T(8,128)(2,1)} fusion(bf16[512,2048]{1,0:T(8,128)(2,1)S(1)} %copy-done, bf16[1,512,512]{2,1,0:T(8,128)(2,1)} %param.22, f32[256,512]{1,0:T(8,128)S(1)} %copy.39, bf16[256,512]{1,0:T(8,128)(2,1)} %copy-done.4, f32[272,512]{1,0:T(8,128)} %maximum_convert_fusion, bf16[256,1,512]{2,1,0:T(2,128)(2,1)} %get-tuple-element.133, ...), kind=kOutput, calls=%fused_computation.32 | convolution fusion | flops 677904384 | bytes 13896720 | tf_op jit(solution)/shard_map/dot_general | solution.py:220
  302.5 4.2 %all-to-all-start.1 = ((bf16[4,64,2048]{2,1,0:T(8,128)(2,1)}), bf16[4,64,2048]{2,1,0:T(8,128)(2,1)S(1)}, u32[]{:S(2)}, u32[]{:S(2)}) async-start(bf16[4,64,2048]{2,1,0:T(8,128)(2,1)} %bitcast.156), calls=%async_computation.1 | async-start | bytes 2097152 | tf_op jit(solution)/shard_map/all_to_all | solution.py:54
  307.4 14.9 %all-to-all-done.1 = bf16[4,64,2048]{2,1,0:T(8,128)(2,1)S(1)} async-done(((bf16[4,64,2048]{2,1,0:T(8,128)(2,1)}), bf16[4,64,2048]{2,1,0:T(8,128)(2,1)S(1)}, u32[]{:S(2)}, u32[]{:S(2)}) %all-to-all-start.1) | async-done | bytes 1048608 | tf_op jit(solution)/shard_map/all_to_all | solution.py:54
  (386 shorter events, 153.1 us)
Async XLA Ops:
  7.2 285.4 %copy-start = (bf16[512,2048]{1,0:T(8,128)(2,1)S(1)}, bf16[512,2048]{1,0:T(8,128)(2,1)}, u32[]{:S(2)}) copy-start(bf16[512,2048]{1,0:T(8,128)(2,1)} %param.25) | copy-start | bytes 6291460
  7.2 20.8 %copy-start.5 = (f32[2048]{0:T(1024)S(1)}, f32[2048]{0:T(1024)}, u32[]{:S(2)}) copy-start(f32[2048]{0:T(1024)} %param.15) | copy-start | bytes 24580
  7.2 106.5 %all-gather.2.cloned.1.call-start = ((), (), s32[]{:S(2)}) async-start(), calls=%async_computation.2 | async-start | bytes 8519680 | tf_op jit(solution)/shard_map/all_gather | solution.py:38
  7.2 21.1 %copy-start.2 = (bf16[2048,1,128]{2,0,1:T(8,128)(2,1)S(1)}, bf16[2048,1,128]{2,0,1:T(8,128)(2,1)}, u32[]{:S(2)}) copy-start(bf16[2048,1,128]{2,0,1:T(8,128)(2,1)} %param.18) | copy-start | bytes 1572868
  7.2 21.6 %copy-start.3 = (bf16[2048,1,128]{2,0,1:T(8,128)(2,1)S(1)}, bf16[2048,1,128]{2,0,1:T(8,128)(2,1)}, u32[]{:S(2)}) copy-start(bf16[2048,1,128]{2,0,1:T(8,128)(2,1)} %param.17) | copy-start | bytes 1572868
  37.7 14.5 %copy-start.4 = (bf16[256,512]{1,0:T(8,128)(2,1)}, bf16[256,512]{1,0:T(8,128)(2,1)S(1)}, u32[]{:S(2)}) copy-start(bf16[256,512]{1,0:T(8,128)(2,1)S(1)} %fusion.36) | copy-start | bytes 786436
  37.7 14.4 %collective-permute-start = (bf16[16,512]{1,0:T(8,128)(2,1)S(1)}, bf16[16,512]{1,0:T(8,128)(2,1)S(1)}, u32[]{:S(2)}, u32[]{:S(2)}) collective-permute-start(bf16[16,512]{1,0:T(8,128)(2,1)S(1)} %slice.112), channel_id=1, source_target_pairs={{0,4},{4,8},{8,12},{12,16},{16,20},{20,24},{24,28},{28,32},{32,36}... | collective-permute-start | bytes 49160 | tf_op jit(solution)/shard_map/ppermute | solution.py:44
  46.2 3.1 copy-start.1
  119.6 171.3 %copy-start.6 = (f32[4]{0:T(128)S(1)}, f32[4]{0:T(128)}, u32[]{:S(2)}) copy-start(f32[4]{0:T(128)} %param.19) | copy-start | bytes 52
  119.6 172.7 %copy-start.7 = (f32[128]{0:T(128)S(1)}, f32[128]{0:T(128)}, u32[]{:S(2)}) copy-start(f32[128]{0:T(128)} %param.20) | copy-start | bytes 1540
  289.6 3.0 copy-start.8
  302.5 19.8 %all-to-all-start.1 = ((bf16[4,64,2048]{2,1,0:T(8,128)(2,1)}), bf16[4,64,2048]{2,1,0:T(8,128)(2,1)S(1)}, u32[]{:S(2)}, u32[]{:S(2)}) async-start(bf16[4,64,2048]{2,1,0:T(8,128)(2,1)} %bitcast.156), calls=%async_computation.1 | async-start | bytes 2097152 | tf_op jit(solution)/shard_map/all_to_all | solution.py:54
Sparse Core Ops, SparseCore 0:
  30.1 83.5 all-gather.1
where the time goes:
time: 332 us; the launch traced here: 330 us
  matrix products  149 us (45%)
  waiting for transfers between devices  75.6 us (23%)
  other arithmetic  43.5 us (13%)
  local copies, waits for them, and re-layouts  19.3 us (6%)
  blocking collectives  19.2 us (6%)
  between operations  14.3 us (4%)
  starting transfers between devices  6.2 us (2%)
    dot_general x32, matrix products, online_step(): jnp.einsum('grmqk,kgd->grmqd', probs.astype(jnp.bfloat16), block_values,...  73.1 us
    all_gather x1, waiting for transfers between devices, sent_together(): lax.all_gather(both, axis, axis=dim, tiled=True)  60.7 us
    dot_general x32, matrix products, online_step(): jnp.einsum('qgrmd,kgmd->grmqk', queries, block_keys_arr, preferred_elemen...  55 us
    another operation x32, other arithmetic  30.4 us
    all_to_all x1, blocking collectives, copy_for_each(): lax.all_to_all(jnp.broadcast_to(array[None], (size, *array.shape)), axis,...  19.2 us
    all_to_all x1, waiting for transfers between devices, sent_and_summed(): pieces = lax.all_to_all(cut_along(array, dim, size), axis, 0, 0, tiled=True)  14.9 us
    dot_general x5, matrix products, project(): jnp.dot(normed, matrix, preferred_element_type=jnp.float32)  10.7 us
    dot_general x1, matrix products, local(): jnp.dot(merged, out_weight, preferred_element_type=jnp.float32)  9.88 us
  transfers between devices with their start and end apart: 3, of which 2 were waited for; matrix products, arithmetic and copies ran while one was open for 7% of the time, Pallas kernels for 0%

commit v1 on v0

v1 whole, which is shorter than its diff:
```python
import functools
import math

import jax
import jax.numpy as jnp
from jax import lax
from jax.experimental import pallas as pl
from jax.experimental.pallas import tpu as pltpu
from jax.sharding import Mesh
from jax.sharding import PartitionSpec as P

NORM_EPS = 1e-06
WINDOW = 16
ROWS = 256
HALF = 128
MAPS = 8
ST = 152
NEG = -1e30
LIMIT = 64.0
LOG2E = math.log2(math.e)
VMEM = pl.BlockSpec(memory_space=pltpu.VMEM)
SMEM = pl.BlockSpec(memory_space=pltpu.SMEM)
F32 = jnp.float32
BF16 = jnp.bfloat16


def vmem(mib):
    return pltpu.CompilerParams(vmem_limit_bytes=mib << 20)


def ring(size, step):
    return [(i, (i + step) % size) for i in range(size)]


def dot(a, b):
    return jnp.dot(a, b, preferred_element_type=F32)


def with_ones(v0, v1):
    values = jnp.concatenate([v0, v1], axis=1)
    return jnp.concatenate([values, jnp.ones((16, values.shape[1]), BF16)], axis=0)


def first_kernel(place_ref, kv_ref, oth_kv_ref, q_ref, own_ref, oth_ref):
    keys = jnp.concatenate([kv_ref[0, 0, :, :HALF], kv_ref[1, 0, :, :HALF]], axis=0)
    oth_keys = jnp.concatenate([oth_kv_ref[0, 0, :, :HALF], oth_kv_ref[1, 0, :, :HALF]], axis=0)
    values = with_ones(kv_ref[0, 0, :, HALF:], kv_ref[1, 0, :, HALF:])
    row = lax.broadcasted_iota(jnp.int32, (ROWS, ROWS), 0)
    col = lax.broadcasted_iota(jnp.int32, (ROWS, ROWS), 1)
    diagonal = row <= col
    for i in range(MAPS):
        q_own, q_oth = q_ref[i, :, :ROWS], q_ref[i, :, ROWS:]
        s = jnp.where(diagonal, dot(keys, q_own), NEG)
        top = jnp.max(s, axis=0, keepdims=True)
        p = jnp.exp2(s - top).astype(BF16)
        own_ref[i, 0:144] = dot(values, p)
        own_ref[i, 144:152] = jnp.broadcast_to(top, (8, ROWS))
        top = jnp.max(jnp.where(diagonal, dot(oth_keys, q_oth), NEG), axis=0, keepdims=True)
        oth_ref[i, 144:152] = jnp.broadcast_to(top, (8, ROWS))
        oth_ref[i, 0:144] = jnp.zeros((144, ROWS), F32)

    @pl.when(place_ref[2] == 0)
    def _():
        for i in range(MAPS):
            before = oth_ref[i, 144:145]
            s = dot(keys, q_ref[i, :, ROWS:])
            top = jnp.maximum(before, jnp.max(s, axis=0, keepdims=True))
            p = jnp.exp2(s - top).astype(BF16)
            oth_ref[i, 0:144] = dot(values, p)
            oth_ref[i, 144:152] = jnp.broadcast_to(top, (8, ROWS))


def chunk_kernel(plan, n_in, *refs):
    place_ref, q_ref = refs[0], refs[1]
    ins = refs[2 : 2 + n_in]
    own_in, oth_in, own_ref, oth_ref, keys_ref, values_ref, p_a, p_b, over_ref, list_ref = refs[2 + n_in :]
    probs = (p_a, p_b)
    z, y = place_ref[0], place_ref[1]
    visible = jnp.int32(0)
    at = 0
    for _, dy, planes in plan:
        for dz in planes:
            sees = ((z + dz) & 7) * 4 + ((y + dy) & 3) < z * 4 + y
            list_ref[visible] = at
            visible = visible + sees.astype(jnp.int32)
            at += 1

    def fetch(which, slot):
        at = 0
        rows = slice(slot * ROWS, slot * ROWS + HALF), slice(slot * ROWS + HALF, slot * ROWS + ROWS)
        for pair, _, planes in plan:
            count = len(planes)

            @pl.when((which >= at) & (which < at + count))
            def _(pair=pair, at=at):
                b = which - at
                for half in range(2):
                    source = ins[pair[half]].at[b] if isinstance(pair, tuple) else ins[pair].at[half, b]
                    keys_ref[rows[half]] = source[:, :HALF]
                    values_ref[0:HALF, rows[half]] = source[:, HALF:]
            at += count

    own_ref[...] = own_in[...]
    oth_ref[...] = oth_in[...]

    @pl.when(visible > 0)
    def _():
        over_ref[...] = jnp.full(over_ref.shape, NEG, F32)
        values_ref[HALF:144] = jnp.ones((16, 2 * ROWS), BF16)

        def two_blocks(t, carry):
            fetch(list_ref[2 * t], 0)
            second = 2 * t + 1 < visible
            fetch(list_ref[jnp.minimum(2 * t + 1, visible - 1)], 1)

            @pl.when(jnp.logical_not(second))
            def _():
                values_ref[:, ROWS:] = jnp.zeros((144, ROWS), BF16)

            keys, values = keys_ref[...], values_ref[...]

            def scores(i):
                top = jnp.concatenate([own_ref[i, 144:145], oth_ref[i, 144:145]], axis=1)
                s = dot(keys, q_ref[i]) - top
                over_ref[i] = jnp.maximum(over_ref[i], jnp.max(s.reshape(-1, 8, 2 * ROWS), axis=0))
                probs[i % 2][...] = jnp.exp2(s).astype(BF16)

            scores(0)
            for i in range(MAPS):
                if i + 1 < MAPS:
                    scores(i + 1)
                out = dot(values, probs[i % 2][...])
                own_ref[i, 0:144] = own_ref[i, 0:144] + out[:, :ROWS]
                oth_ref[i, 0:144] = oth_ref[i, 0:144] + out[:, ROWS:]
            return carry

        lax.fori_loop(0, (visible + 1) // 2, two_blocks, 0)

        @pl.when(jnp.logical_not(jnp.max(over_ref[...]) <= LIMIT))
        def _():
            own_ref[...] = own_in[...]
            oth_ref[...] = oth_in[...]
            values_ref[HALF:144] = jnp.ones((16, 2 * ROWS), BF16)

            def one_block(t, carry):
                fetch(list_ref[t], 0)

                def one_map(i, carry):
                    before = jnp.concatenate([own_ref[i, 144:145], oth_ref[i, 144:145]], axis=1)
                    s = dot(keys_ref[:ROWS], q_ref[i])
                    top = jnp.maximum(before, jnp.max(s, axis=0, keepdims=True))
                    scale = jnp.exp2(before - top)
                    out = dot(values_ref[:, :ROWS], jnp.exp2(s - top).astype(BF16))
                    top8 = jnp.broadcast_to(top, (8, 2 * ROWS))
                    own_ref[i, 0:144] = own_ref[i, 0:144] * scale[:, :ROWS] + out[:, :ROWS]
                    oth_ref[i, 0:144] = oth_ref[i, 0:144] * scale[:, ROWS:] + out[:, ROWS:]
                    own_ref[i, 144:152] = top8[:, :ROWS]
                    oth_ref[i, 144:152] = top8[:, ROWS:]
                    return carry

                return lax.fori_loop(0, MAPS, one_map, carry)

            lax.fori_loop(0, visible, one_block, 0)


STATE = (pltpu.VMEM((MAPS, ST, ROWS), F32), pltpu.VMEM((MAPS, ST, ROWS), F32))


def in_vmem(array):
    return pltpu.with_memory_space_constraint(array, pltpu.VMEM)


def attend_chunk(place, q, state, plan, arrays, name):
    n = len(arrays)
    blocks = sum(len(planes) for _, _, planes in plan)
    return pl.pallas_call(
        functools.partial(chunk_kernel, plan, n),
        out_shape=STATE,
        in_specs=[SMEM, VMEM] + [VMEM] * n + [VMEM, VMEM],
        out_specs=(VMEM, VMEM),
        scratch_shapes=[
            pltpu.VMEM((2 * ROWS, HALF), BF16),
            pltpu.VMEM((144, 2 * ROWS), BF16),
            pltpu.VMEM((2 * ROWS, 2 * ROWS), BF16),
            pltpu.VMEM((2 * ROWS, 2 * ROWS), BF16),
            pltpu.VMEM((MAPS, 8, 2 * ROWS), F32),
            pltpu.SMEM((blocks + 1,), jnp.int32),
        ],
        cost_estimate=pl.CostEstimate(
            flops=blocks * MAPS * 2 * 256 * 512 * 512, transcendentals=blocks * MAPS * 256 * 512, bytes_accessed=1 << 20
        ),
        compiler_params=vmem(20),
        name=name,
    )(place, in_vmem(q), *arrays, in_vmem(state[0]), in_vmem(state[1]))


def pool_kernel(place_ref, pool_ref, rim_ref, gate_ref, mix_ref, scale_ref, keep_ref, part_ref):
    span = jnp.left_shift(jnp.int32(2), place_ref[3])
    start = ((place_ref[0] * 4 + place_ref[1]) * 2 + place_ref[2]) * ROWS
    now = pool_ref[...].astype(F32)
    sums = jnp.concatenate([rim_ref[...].astype(F32), now], axis=0)
    rows = WINDOW + ROWS
    picked = jnp.zeros((ROWS, now.shape[1]), F32)
    for width in (1, 2, 4, 8):
        sums = sums + jnp.concatenate([jnp.zeros((width, now.shape[1]), F32), sums[: rows - width]], axis=0)
        picked = jnp.where(span == 2 * width, sums[WINDOW:], picked)
    position = start + lax.broadcasted_iota(jnp.int32, (ROWS, 1), 0)
    counts = jnp.minimum(position + 1, span).astype(F32)
    pooled = (picked / counts - now).astype(BF16)
    mixed = dot(pooled, mix_ref[...]) * scale_ref[...]
    width = now.shape[1]
    keep_ref[...] = jax.nn.sigmoid(gate_ref[:, :width].astype(F32))
    part_ref[...] = jax.nn.sigmoid(gate_ref[:, width:].astype(F32)) * mixed


def finish_kernel(lam_ref, a_ref, b_ref, gain_ref, keep_ref, part_ref, w_ref, out_ref, log_ref, merged_ref):
    for h in range(MAPS // 2):
        maps = []
        for m in range(2):
            i = 2 * h + m
            top_a, top_b = a_ref[i, 144:145], b_ref[i, 144:145]
            top = jnp.maximum(top_a, top_b)
            wa, wb = jnp.exp2(top_a - top), jnp.exp2(top_b - top)
            total = a_ref[i, 128:129] * wa + b_ref[i, 128:129] * wb
            log_ref[i : i + 1, :] = (top + jnp.log2(total)) * (1.0 / LOG2E)
            maps.append((a_ref[i, 0:128] * wa + b_ref[i, 0:128] * wb) / total)
        head = maps[0] - lam_ref[h] * maps[1]
        head = head * lax.rsqrt(jnp.mean(head * head, axis=0, keepdims=True) + NORM_EPS)
        cols = slice(h * 128, h * 128 + 128)
        attended = head.T * gain_ref[...]
        merged_ref[:, cols] = (keep_ref[:, cols] * attended + part_ref[:, cols]).astype(BF16)
    out_ref[...] = dot(merged_ref[...], w_ref[...]).astype(BF16)


def local(tokens, norm_gain, query_weight, key_weight, value_weight, mix_lambda, head_gain, pool_weight, pool_mix, pool_scale, gate_weight, out_weight):
    width = tokens.shape[1]
    z, y, c = lax.axis_index("z"), lax.axis_index("y"), lax.axis_index("c")
    place = jnp.stack([z, y, c, lax.axis_index("x")])
    pieces = lax.all_to_all(jnp.broadcast_to(tokens[None], (4, *tokens.shape)), "x", 0, 0, tiled=True)
    gate_w, query_w = gate_weight.reshape(width, -1), query_weight.reshape(width, -1)
    pieces, gate_w, query_w = lax.optimization_barrier((pieces, gate_w, query_w))
    inputs = pieces.reshape(ROWS, width).astype(F32)
    normed = (inputs * lax.rsqrt(jnp.mean(inputs * inputs, axis=1, keepdims=True) + NORM_EPS) * norm_gain).astype(BF16)

    def project(weight):
        return dot(normed, weight.reshape(width, -1)).astype(BF16)

    keys = project(key_weight)
    values_t = lax.dot_general(value_weight.reshape(width, 128), normed, (((0,), (1,)), ((), ())), preferred_element_type=F32).astype(BF16)
    kv = jnp.concatenate(
        [keys.reshape(2, 1, HALF, HALF), jnp.transpose(values_t.reshape(HALF, 2, HALF), (1, 0, 2))[:, None]], axis=3
    )
    up, down = [kv], [kv]
    for k in range(4):
        up.append(lax.ppermute(up[-1], "z", ring(8, 1)))
        if k < 3:
            down.append(lax.ppermute(down[-1], "z", ring(8, -1)))
    near = jnp.concatenate([kv, up[1], down[1]], axis=1)
    far = jnp.concatenate([up[2], up[3], up[4], down[2], down[3]], axis=1)
    near_at, far_at = (0, -1, 1), (-2, -3, -4, 2, 3)

    def around_y(group):
        low = lax.ppermute(group, "y", ring(4, 1))
        high = lax.ppermute(group, "y", ring(4, -1))
        a = lax.ppermute(low[0], "y", ring(4, 1))
        b = lax.ppermute(high[1], "y", ring(4, -1))
        return low, high, a, b

    scale = (query_weight.shape[2] // 2) ** -0.5 * LOG2E
    q_own = (
        lax.dot_general(query_w, normed, (((0,), (1,)), ((), ())), preferred_element_type=F32) * scale
    ).astype(BF16)
    q_oth = lax.ppermute(q_own, "c", [(0, 1), (1, 0)])
    kv_oth = lax.ppermute(kv, "c", [(0, 1), (1, 0)])
    q = jnp.concatenate([q_own, q_oth], axis=1).reshape(4, 2, 64, 2 * ROWS)
    zero = jnp.zeros((4, 64, 2 * ROWS), BF16)
    q = jnp.stack([jnp.concatenate([q[:, 0], zero], axis=1), jnp.concatenate([zero, q[:, 1]], axis=1)], axis=1)
    q = q.reshape(MAPS, 128, 2 * ROWS)

    pool_in = project(pool_weight)
    gate_pre = project(gate_w)
    rim = lax.ppermute(pool_in[ROWS - WINDOW :], ("z", "y", "c"), [(i, i + 1) for i in range(63)])
    part_shape = jax.ShapeDtypeStruct((ROWS, 512), F32)
    keep, part = pl.pallas_call(
        pool_kernel,
        out_shape=(part_shape, part_shape),
        in_specs=[SMEM] + [VMEM] * 5,
        out_specs=(VMEM, VMEM),
        compiler_params=vmem(16),
        name="pool",
    )(place, pool_in, rim, gate_pre, pool_mix[0], pool_scale)

    state = pl.pallas_call(
        first_kernel, out_shape=STATE, in_specs=[SMEM, VMEM, VMEM, VMEM], out_specs=(VMEM, VMEM), compiler_params=vmem(16), name="first"
    )(place, kv, kv_oth, in_vmem(q))
    state, keep, part = lax.optimization_barrier((state, keep, part))
    state = attend_chunk(place, q, state, ((0, 0, (-1,)), (1, 0, (1,))), (up[1], down[1]), "z_near")
    state = attend_chunk(place, q, state, ((0, 0, far_at),), (far,), "z_far")
    for group, at, name in ((near, near_at, "near"), (far, far_at, "far")):
        low, high, a, b = around_y(group)
        state = attend_chunk(place, q, state, ((0, -1, at), (1, 1, at)), (low, high), "y_" + name)
        state = attend_chunk(place, q, state, (((0, 1), 2, at),), (a, b), "d_" + name)
    other = lax.ppermute(state[1], "c", [(0, 1), (1, 0)])
    out, logs = pl.pallas_call(
        finish_kernel,
        out_shape=(jax.ShapeDtypeStruct((ROWS, width), BF16), jax.ShapeDtypeStruct((MAPS, ROWS), F32)),
        in_specs=[SMEM] + [VMEM] * 6,
        out_specs=(VMEM, VMEM),
        scratch_shapes=[pltpu.VMEM((ROWS, 512), BF16)],
        compiler_params=vmem(24),
        name="finish",
    )(mix_lambda, state[0], other, head_gain[None], keep, part, out_weight)
    shares = lax.all_to_all(out.reshape(4, 64, width), "x", 0, 0, tiled=True)
    mixed = jnp.sum(shares.astype(F32), axis=0).astype(BF16)
    return mixed, jnp.transpose(logs.reshape(4, 2, ROWS), (1, 0, 2))


def solution(mesh):
    fine = Mesh(mesh.devices.reshape(8, 4, 2, 4), ("z", "y", "c", "x"))
    sp = ("z", "y", "c")
    in_specs = (
        P((*sp, "x"), None),
        P(),
        P(None, "x", None),
        P(None, "x", None),
        P(None, "x", None),
        P("x"),
        P(),
        P(None, "x", None),
        P("x", None, None),
        P("x", None),
        P(None, None, "x"),
        P("x", None),
    )
    out_specs = (P((*sp, "x"), None), P(None, "x", sp))
    return jax.shard_map(local, mesh=fine, in_specs=in_specs, out_specs=out_specs, check_vma=False)
```

time: 332 us -> 270 us (0.81)
  matrix products: 149 us -> 5.05 us
  starting transfers between devices: 6.2 us -> 138 us
  Pallas kernels: 0 us -> 66.9 us
  waiting for transfers between devices: 75.6 us -> 31.9 us
  other arithmetic: 43.5 us -> 4.53 us
  blocking collectives: 19.2 us -> 0 us
  between operations: 14.3 us -> 1.32 us
    dot_general x70 -> x5, matrix products: 149 us -> 5.05 us  [the longest x3 3.92 us: dot(): return jnp.dot(a, b, preferred_element_type=F32)]
    all_to_all x1 -> x2, starting transfers between devices: 4.25 us -> 101 us  [the longest x1 96.3 us: local(): shares = lax.all_to_all(out.reshape(4, 64, width), 'x', 0, 0, tiled=True)]
    pallas_call x0 -> x9, Pallas kernels: none -> 66.9 us  [the longest x6 58.1 us: attend_chunk(): pl.pallas_call(functools.partial(chunk_kernel, plan, n), out_shape=STATE,...]
    all_gather x1 -> x0, waiting for transfers between devices: 60.7 us -> none  [sent_together(): lax.all_gather(both, axis, axis=dim, tiled=True)]
    ppermute x1 -> x19, starting transfers between devices: 1.92 us -> 37.1 us  [the longest x2 18.4 us: around_y(): b = lax.ppermute(high[1], 'y', ring(4, -1))]
    another operation x32 -> x2, other arithmetic: 30.4 us -> 0.18 us  [the longest x1 0.1 us: local(): jnp.stack([jnp.concatenate([q[:, 0], zero], axis=1), jnp.concatenate([zer...]
    all_to_all x1 -> x0, blocking collectives: 19.2 us -> none  [copy_for_each(): lax.all_to_all(jnp.broadcast_to(array[None], (size, *array.shape)), axis,...]
    ppermute x1 -> x19, waiting for transfers between devices: 0.01 us -> 9.37 us  [the longest x4 4.03 us: local(): up.append(lax.ppermute(up[-1], 'z', ring(8, 1)))]
  transfers between devices with their start and end apart: 3 -> 21, of which waited for: 2 -> 6; matrix products, arithmetic and copies ran while one was open for 7% -> 8% of each run, Pallas kernels for 0% -> 22%
where the time goes in v1:
time: 270 us; the launch traced here: 266 us
  starting transfers between devices  138 us (51%)
  Pallas kernels  66.9 us (25%)
  waiting for transfers between devices  31.9 us (12%)
  local copies, waits for them, and re-layouts  18.8 us (7%)
  matrix products  5.05 us (2%)
  other arithmetic  4.53 us (2%)
    all_to_all x1, starting transfers between devices, local(): shares = lax.all_to_all(out.reshape(4, 64, width), 'x', 0, 0, tiled=True)  96.3 us
    pallas_call x6, Pallas kernels, attend_chunk(): pl.pallas_call(functools.partial(chunk_kernel, plan, n), out_shape=STATE,...  58.1 us
    ppermute x2, starting transfers between devices, around_y(): b = lax.ppermute(high[1], 'y', ring(4, -1))  18.4 us
    all_to_all x1, waiting for transfers between devices, local(): shares = lax.all_to_all(out.reshape(4, 64, width), 'x', 0, 0, tiled=True)  14.8 us
    unnamed x36, local copies, waits for them, and re-layouts  10.5 us
    all_to_all x1, waiting for transfers between devices, local(): lax.all_to_all(jnp.broadcast_to(tokens[None], (4, *tokens.shape)), 'x', 0...  7.76 us
  transfers between devices with their start and end apart: 21, of which 6 were waited for; matrix products, arithmetic and copies ran while one was open for 8% of the time, Pallas kernels for 22%

profile of v1, /device:TPU:248, one launch (start us, length us, event | category | flops | bytes accessed | tf_op | source)
XLA Modules:
  0.0 266.1 jit_solution(16938823725657740856)
XLA Ops:
  0.6 2.2 broadcast_in_dim.6
  2.8 4.3 %all-to-all-start = ((bf16[4,64,2048]{2,1,0:T(8,128)(2,1)}), bf16[4,64,2048]{2,1,0:T(8,128)(2,1)S(1)}, u32[]{:S(2)}, u32[]{:S(2)}) async-start(bf16[4,64,2048]{2,1,0:T(8,128)(2,1)} %broadcast_in_dim.6), calls=%async_computation | async-start | bytes 2097152 | tf_op jit(solution)/shard_map/all_to_all | solution.py:239
  7.1 5.5 %copy.28 = bf16[256,8,2,512]{3,1,2,0:T(8,128)(2,1)} copy(bf16[256,8,2,512]{3,2,1,0:T(2,128)(2,1)} %bitcast.80) | data formatting | bytes 8388608
  14.5 7.8 %all-to-all-done = bf16[4,64,2048]{2,1,0:T(8,128)(2,1)S(1)} async-done(((bf16[4,64,2048]{2,1,0:T(8,128)(2,1)}), bf16[4,64,2048]{2,1,0:T(8,128)(2,1)S(1)}, u32[]{:S(2)}, u32[]{:S(2)}) %all-to-all-start) | async-done | bytes 1048608 | tf_op jit(solution)/shard_map/all_to_all | solution.py:239
  26.7 2.0 collective-permute-start.5
  31.0 2.1 collective-permute-start.17
  39.0 2.3 collective-permute-start.12
  44.4 2.1 copy.22
  47.9 5.1 %first.1 = (f32[8,152,256]{2,1,0:T(8,128)S(1)}, f32[8,152,256]{2,1,0:T(8,128)S(1)}) custom-call(s32[4]{0:T(128)S(1)} %pad_add_fusion.place_ref.refs_0_, bf16[2,1,128,256]{3,2,1,0:T(8,128)(2,1)S(1)} %pad_maximum_fusion.3.kv_ref, bf16[2,1,128,256]{3,2,1,0:T(8,128)(2,1)S(1)} %collective-permute-done.16.oth_kv_ref, bf16[8,128,512]{2,1,0:T(8,128)(2,1)S(1)} %bitcast.68), custom_call_target="tpu_custom_call" | custom-call | tf_op jit(solution)/shard_map/first/pallas_call | solution.py:293
  53.0 2.3 collective-permute-start.3
  55.3 11.0 %z_near.1 = (f32[8,152,256]{2,1,0:T(8,128)S(1)}, f32[8,152,256]{2,1,0:T(8,128)S(1)}) custom-call(s32[4]{0:T(128)S(1)} %pad_add_fusion.place_ref.refs_0_, bf16[8,128,512]{2,1,0:T(8,128)(2,1)S(1)} %bitcast.69, bf16[2,1,128,256]{3,2,1,0:T(8,128)(2,1)S(1)} %collective-permute-done.1.refs_2_, bf16[2,1,128,256]{3,2,1,0:T(8,128)(2,1)} %collective-permute-done.5.refs_3_, ...), custom_call_target="tpu_custom_call" | custom-call | flops 2147483648 | bytes 1048576 | tf_op jit(solution)/shard_map/z_near/pallas_call | solution.py:176
  67.3 4.0 %collective-permute-done.4 = bf16[2,1,128,256]{3,2,1,0:T(8,128)(2,1)S(1)} collective-permute-done((bf16[2,1,128,256]{3,2,1,0:T(8,128)(2,1)S(1)}, bf16[2,1,128,256]{3,2,1,0:T(8,128)(2,1)S(1)}, u32[]{:S(2)}, u32[]{:S(2)}) %collective-permute-start.4) | collective-permute-done | bytes 131104 | tf_op jit(solution)/shard_map/ppermute | solution.py:255
  73.1 2.5 collective-permute-start.8
  75.6 17.3 %z_far.1 = (f32[8,152,256]{2,1,0:T(8,128)S(1)}, f32[8,152,256]{2,1,0:T(8,128)S(1)}) custom-call(s32[4]{0:T(128)S(1)} %pad_add_fusion.place_ref.refs_0_, bf16[8,128,512]{2,1,0:T(8,128)(2,1)S(1)} %bitcast.70, bf16[2,5,128,256]{3,2,1,0:T(8,128)(2,1)S(1)} %constant_dynamic-update-slice_fusion.refs_2_, f32[8,152,256]{2,1,0:T(8,128)S(1)} %get-tuple-element.36.refs_3_, ...), custom_call_target="tpu_custom_call" | custom-call | flops 5368709120 | bytes 1048576 | tf_op jit(solution)/shard_map/z_far/pallas_call | solution.py:176
  93.8 1.9 collective-permute-start.13
  96.7 17.0 %collective-permute-start.15 = (bf16[3,128,256]{2,1,0:T(8,128)(2,1)S(1)}, bf16[3,128,256]{2,1,0:T(8,128)(2,1)S(1)}, u32[]{:S(2)}, u32[]{:S(2)}) collective-permute-start(bf16[3,128,256]{2,1,0:T(8,128)(2,1)S(1)} %slice_bitcast_fusion.4), channel_id=1, source_target_pairs={{0,24},{8,0},{16,8},{24,16},{1,25},{9,1},{17,9},{25,17},{2,26},{10... | collective-permute-start | bytes 589832 | tf_op jit(solution)/shard_map/ppermute | solution.py:266
  113.7 7.4 %y_near.1 = (f32[8,152,256]{2,1,0:T(8,128)S(1)}, f32[8,152,256]{2,1,0:T(8,128)S(1)}) custom-call(s32[4]{0:T(128)S(1)} %pad_add_fusion.place_ref.refs_0_, bf16[8,128,512]{2,1,0:T(8,128)(2,1)S(1)} %bitcast.71, bf16[2,3,128,256]{3,2,1,0:T(8,128)(2,1)} %collective-permute-done.12.refs_2_, bf16[2,3,128,256]{3,2,1,0:T(8,128)(2,1)} %collective-permute-done.14.refs_3_, ...), custom_call_target="tpu_custom_call" | custom-call | flops 6442450944 | bytes 1048576 | tf_op jit(solution)/shard_map/y_near/pallas_call | solution.py:176
  121.7 4.8 %d_near.1 = (f32[8,152,256]{2,1,0:T(8,128)S(1)}, f32[8,152,256]{2,1,0:T(8,128)S(1)}) custom-call(s32[4]{0:T(128)S(1)} %pad_add_fusion.place_ref.refs_0_, bf16[8,128,512]{2,1,0:T(8,128)(2,1)S(1)} %bitcast.72, bf16[3,128,256]{2,1,0:T(8,128)(2,1)S(1)} %collective-permute-done.13.refs_2_, bf16[3,128,256]{2,1,0:T(8,128)(2,1)S(1)} %collective-permute-done.15.refs_3_, ...), custom_call_target="tpu_custom_call" | custom-call | flops 3221225472 | bytes 1048576 | tf_op jit(solution)/shard_map/d_near/pallas_call | solution.py:176
  130.0 10.9 %y_far.1 = (f32[8,152,256]{2,1,0:T(8,128)S(1)}, f32[8,152,256]{2,1,0:T(8,128)S(1)}) custom-call(s32[4]{0:T(128)S(1)} %pad_add_fusion.place_ref.refs_0_, bf16[8,128,512]{2,1,0:T(8,128)(2,1)S(1)} %bitcast.73, bf16[2,5,128,256]{3,2,1,0:T(8,128)(2,1)S(1)} %collective-permute-done.8.refs_2_, bf16[2,5,128,256]{3,2,1,0:T(8,128)(2,1)S(1)} %collective-permute-done.10.refs_3_, ...), custom_call_target="tpu_custom_call" | custom-call | flops 10737418240 | bytes 1048576 | tf_op jit(solution)/shard_map/y_far/pallas_call | solution.py:176
  140.9 6.8 %d_far.1 = (f32[8,152,256]{2,1,0:T(8,128)S(1)}, f32[8,152,256]{2,1,0:T(8,128)S(1)}) custom-call(s32[4]{0:T(128)S(1)} %pad_add_fusion.place_ref.refs_0_, bf16[8,128,512]{2,1,0:T(8,128)(2,1)S(1)} %bitcast.74, bf16[5,128,256]{2,1,0:T(8,128)(2,1)S(1)} %collective-permute-done.9.refs_2_, bf16[5,128,256]{2,1,0:T(8,128)(2,1)S(1)} %collective-permute-done.11.refs_3_, ...), custom_call_target="tpu_custom_call" | custom-call | flops 5368709120 | bytes 1048576 | tf_op jit(solution)/shard_map/d_far/pallas_call | solution.py:176
  147.8 2.9 %collective-permute-done.18.b_ref = f32[8,152,256]{2,1,0:T(8,128)S(1)} collective-permute-done((f32[8,152,256]{2,1,0:T(8,128)S(1)}, f32[8,152,256]{2,1,0:T(8,128)S(1)}, u32[]{:S(2)}, u32[]{:S(2)}) %collective-permute-start.18) | collective-permute-done | bytes 1245216 | tf_op jit(solution)/shard_map/ppermute | solution.py:303
  150.7 2.6 finish.1
  153.4 96.3 %all-to-all-start.1 = ((bf16[4,64,2048]{2,1,0:T(8,128)(2,1)}), bf16[4,64,2048]{2,1,0:T(8,128)(2,1)S(1)}, u32[]{:S(2)}, u32[]{:S(2)}) async-start(bf16[4,64,2048]{2,1,0:T(8,128)(2,1)} %bitcast.26), calls=%async_computation.1 | async-start | bytes 2097152 | tf_op jit(solution)/shard_map/all_to_all | solution.py:313
  250.2 14.8 %all-to-all-done.1 = bf16[4,64,2048]{2,1,0:T(8,128)(2,1)S(1)} async-done(((bf16[4,64,2048]{2,1,0:T(8,128)(2,1)}), bf16[4,64,2048]{2,1,0:T(8,128)(2,1)S(1)}, u32[]{:S(2)}, u32[]{:S(2)}) %all-to-all-start.1) | async-done | bytes 1048608 | tf_op jit(solution)/shard_map/all_to_all | solution.py:313
  (93 shorter events, 29.0 us)
Async XLA Ops:
  0.6 29.2 %copy-start = (bf16[2048,1,512]{2,0,1:T(8,128)(2,1)S(1)}, bf16[2048,1,512]{2,0,1:T(8,128)(2,1)}, u32[]{:S(2)}) copy-start(bf16[2048,1,512]{2,0,1:T(8,128)(2,1)} %param.19) | copy-start | bytes 6291460
  2.8 19.4 %all-to-all-start = ((bf16[4,64,2048]{2,1,0:T(8,128)(2,1)}), bf16[4,64,2048]{2,1,0:T(8,128)(2,1)S(1)}, u32[]{:S(2)}, u32[]{:S(2)}) async-start(bf16[4,64,2048]{2,1,0:T(8,128)(2,1)} %broadcast_in_dim.6), calls=%async_computation | async-start | bytes 2097152 | tf_op jit(solution)/shard_map/all_to_all | solution.py:239
  12.6 10.0 %copy-start.14 = (f32[2048]{0:T(1024)S(1)}, f32[2048]{0:T(1024)}, u32[]{:S(2)}) copy-start(f32[2048]{0:T(1024)} %param.13) | copy-start | bytes 24580
  26.5 21.4 %collective-permute-start.16 = (bf16[2,1,128,256]{3,2,1,0:T(8,128)(2,1)S(1)}, bf16[2,1,128,256]{3,2,1,0:T(8,128)(2,1)S(1)}, u32[]{:S(2)}, u32[]{:S(2)}) collective-permute-start(bf16[2,1,128,256]{3,2,1,0:T(8,128)(2,1)S(1)} %pad_maximum_fusion.3.kv_ref), channel_id=1, source_target_pairs={{0,4},{4,0},{1,5},{5,1},{2,6},{6,2},{3,7},{7,3},{8,12},{12,8},{9,1... | collective-permute-start | bytes 393224 | tf_op jit(solution)/shard_map/ppermute | solution.py:274
  26.6 10.7 %collective-permute-start.1 = (bf16[2,1,128,256]{3,2,1,0:T(8,128)(2,1)S(1)}, bf16[2,1,128,256]{3,2,1,0:T(8,128)(2,1)S(1)}, u32[]{:S(2)}, u32[]{:S(2)}) collective-permute-start(bf16[2,1,128,256]{3,2,1,0:T(8,128)(2,1)S(1)} %pad_maximum_fusion.3.kv_ref), channel_id=1, source_target_pairs={{0,32},{32,64},{64,96},{96,128},{128,160},{160,192},{192,224},{224... | collective-permute-start | bytes 393224 | tf_op jit(solution)/shard_map/ppermute | solution.py:255
  26.7 10.6 %collective-permute-start.5 = (bf16[2,1,128,256]{3,2,1,0:T(8,128)(2,1)S(1)}, bf16[2,1,128,256]{3,2,1,0:T(8,128)(2,1)}, u32[]{:S(2)}, u32[]{:S(2)}) collective-permute-start(bf16[2,1,128,256]{3,2,1,0:T(8,128)(2,1)S(1)} %pad_maximum_fusion.3.kv_ref), channel_id=1, source_target_pairs={{0,224},{32,0},{64,32},{96,64},{128,96},{160,128},{192,160},{224,1... | collective-permute-start | bytes 393224 | tf_op jit(solution)/shard_map/ppermute | solution.py:257
  29.7 12.6 %collective-permute-start = (bf16[512,256]{0,1:T(8,128)(2,1)S(1)}, bf16[512,256]{0,1:T(8,128)(2,1)S(1)}, u32[]{:S(2)}, u32[]{:S(2)}) collective-permute-start(bf16[512,256]{0,1:T(8,128)(2,1)S(1)} %fusion.4), channel_id=1, source_target_pairs={{0,4},{4,0},{1,5},{5,1},{2,6},{6,2},{3,7},{7,3},{8,12},{12,8},{9,1... | collective-permute-start | bytes 786440 | tf_op jit(solution)/shard_map/ppermute | solution.py:273
  31.0 5.2 %collective-permute-start.17 = (bf16[16,512]{1,0:T(8,128)(2,1)S(1)}, bf16[16,512]{1,0:T(8,128)(2,1)S(1)}, u32[]{:S(2)}, u32[]{:S(2)}) collective-permute-start(bf16[16,512]{1,0:T(8,128)(2,1)S(1)} %slice.34), channel_id=1, source_target_pairs={{0,4},{4,8},{8,12},{12,16},{16,20},{20,24},{24,28},{28,32},{32,36}... | collective-permute-start | bytes 49160 | tf_op jit(solution)/shard_map/ppermute | solution.py:282
  39.0 53.9 %collective-permute-start.12 = (bf16[2,3,128,256]{3,2,1,0:T(8,128)(2,1)}, bf16[2,3,128,256]{3,2,1,0:T(8,128)(2,1)}, u32[]{:S(2)}, u32[]{:S(2)}) collective-permute-start(bf16[2,3,128,256]{3,2,1,0:T(8,128)(2,1)} %pad_maximum_fusion.2), channel_id=1, source_target_pairs={{0,8},{8,16},{16,24},{24,0},{1,9},{9,17},{17,25},{25,1},{2,10},{10... | collective-permute-start | bytes 1179656 | tf_op jit(solution)/shard_map/ppermute | solution.py:263
  41.3 54.4 %collective-permute-start.14 = (bf16[2,3,128,256]{3,2,1,0:T(8,128)(2,1)}, bf16[2,3,128,256]{3,2,1,0:T(8,128)(2,1)}, u32[]{:S(2)}, u32[]{:S(2)}) collective-permute-start(bf16[2,3,128,256]{3,2,1,0:T(8,128)(2,1)} %pad_maximum_fusion.2), channel_id=1, source_target_pairs={{0,24},{8,0},{16,8},{24,16},{1,25},{9,1},{17,9},{25,17},{2,26},{10... | collective-permute-start | bytes 1179656 | tf_op jit(solution)/shard_map/ppermute | solution.py:264
  41.3 11.7 %collective-permute-start.2 = (bf16[2,1,128,256]{3,2,1,0:T(8,128)(2,1)S(1)}, bf16[2,1,128,256]{3,2,1,0:T(8,128)(2,1)}, u32[]{:S(2)}, u32[]{:S(2)}) collective-permute-start(bf16[2,1,128,256]{3,2,1,0:T(8,128)(2,1)S(1)} %collective-permute-done.1.refs_2_), channel_id=1, source_target_pairs={{0,32},{32,64},{64,96},{96,128},{128,160},{160,192},{192,224},{224... | collective-permute-start | bytes 393224 | tf_op jit(solution)/shard_map/ppermute | solution.py:255
  42.3 12.9 %collective-permute-start.6 = (bf16[2,1,128,256]{3,2,1,0:T(8,128)(2,1)}, bf16[2,1,128,256]{3,2,1,0:T(8,128)(2,1)}, u32[]{:S(2)}, u32[]{:S(2)}) collective-permute-start(bf16[2,1,128,256]{3,2,1,0:T(8,128)(2,1)} %collective-permute-done.5.refs_3_), channel_id=1, source_target_pairs={{0,224},{32,0},{64,32},{96,64},{128,96},{160,128},{192,160},{224,1... | collective-permute-start | bytes 393224 | tf_op jit(solution)/shard_map/ppermute | solution.py:257
  53.0 13.3 %collective-permute-start.3 = (bf16[2,1,128,256]{3,2,1,0:T(8,128)(2,1)}, bf16[2,1,128,256]{3,2,1,0:T(8,128)(2,1)S(1)}, u32[]{:S(2)}, u32[]{:S(2)}) collective-permute-start(bf16[2,1,128,256]{3,2,1,0:T(8,128)(2,1)} %collective-permute-done.2), channel_id=1, source_target_pairs={{0,32},{32,64},{64,96},{96,128},{128,160},{160,192},{192,224},{224... | collective-permute-start | bytes 393224 | tf_op jit(solution)/shard_map/ppermute | solution.py:255
  55.3 17.0 %collective-permute-start.7 = (bf16[2,1,128,256]{3,2,1,0:T(8,128)(2,1)}, bf16[2,1,128,256]{3,2,1,0:T(8,128)(2,1)S(1)}, u32[]{:S(2)}, u32[]{:S(2)}) collective-permute-start(bf16[2,1,128,256]{3,2,1,0:T(8,128)(2,1)} %collective-permute-done.6), channel_id=1, source_target_pairs={{0,224},{32,0},{64,32},{96,64},{128,96},{160,128},{192,160},{224,1... | collective-permute-start | bytes 393224 | tf_op jit(solution)/shard_map/ppermute | solution.py:257
  66.3 5.0 %collective-permute-start.4 = (bf16[2,1,128,256]{3,2,1,0:T(8,128)(2,1)S(1)}, bf16[2,1,128,256]{3,2,1,0:T(8,128)(2,1)S(1)}, u32[]{:S(2)}, u32[]{:S(2)}) collective-permute-start(bf16[2,1,128,256]{3,2,1,0:T(8,128)(2,1)S(1)} %collective-permute-done.3), channel_id=1, source_target_pairs={{0,32},{32,64},{64,96},{96,128},{128,160},{160,192},{192,224},{224... | collective-permute-start | bytes 393224 | tf_op jit(solution)/shard_map/ppermute | solution.py:255
  72.3 54.2 %collective-permute-start.10 = (bf16[2,5,128,256]{3,2,1,0:T(8,128)(2,1)S(1)}, bf16[2,5,128,256]{3,2,1,0:T(8,128)(2,1)S(1)}, u32[]{:S(2)}, u32[]{:S(2)}) collective-permute-start(bf16[2,5,128,256]{3,2,1,0:T(8,128)(2,1)S(1)} %constant_dynamic-update-slice_fusion.refs_2_), channel_id=1, source_target_pairs={{0,24},{8,0},{16,8},{24,16},{1,25},{9,1},{17,9},{25,17},{2,26},{10... | collective-permute-start | bytes 1966088 | tf_op jit(solution)/shard_map/ppermute | solution.py:264
  73.1 54.9 %collective-permute-start.8 = (bf16[2,5,128,256]{3,2,1,0:T(8,128)(2,1)S(1)}, bf16[2,5,128,256]{3,2,1,0:T(8,128)(2,1)S(1)}, u32[]{:S(2)}, u32[]{:S(2)}) collective-permute-start(bf16[2,5,128,256]{3,2,1,0:T(8,128)(2,1)S(1)} %constant_dynamic-update-slice_fusion.refs_2_), channel_id=1, source_target_pairs={{0,8},{8,16},{16,24},{24,0},{1,9},{9,17},{17,25},{25,1},{2,10},{10... | collective-permute-start | bytes 1966088 | tf_op jit(solution)/shard_map/ppermute | solution.py:263
  93.8 27.2 %collective-permute-start.13 = (bf16[3,128,256]{2,1,0:T(8,128)(2,1)S(1)}, bf16[3,128,256]{2,1,0:T(8,128)(2,1)S(1)}, u32[]{:S(2)}, u32[]{:S(2)}) collective-permute-start(bf16[3,128,256]{2,1,0:T(8,128)(2,1)S(1)} %slice_bitcast_fusion.5), channel_id=1, source_target_pairs={{0,8},{8,16},{16,24},{24,0},{1,9},{9,17},{17,25},{25,1},{2,10},{10... | collective-permute-start | bytes 589832 | tf_op jit(solution)/shard_map/ppermute | solution.py:265
  96.7 25.0 %collective-permute-start.15 = (bf16[3,128,256]{2,1,0:T(8,128)(2,1)S(1)}, bf16[3,128,256]{2,1,0:T(8,128)(2,1)S(1)}, u32[]{:S(2)}, u32[]{:S(2)}) collective-permute-start(bf16[3,128,256]{2,1,0:T(8,128)(2,1)S(1)} %slice_bitcast_fusion.4), channel_id=1, source_target_pairs={{0,24},{8,0},{16,8},{24,16},{1,25},{9,1},{17,9},{25,17},{2,26},{10... | collective-permute-start | bytes 589832 | tf_op jit(solution)/shard_map/ppermute | solution.py:266
  126.6 14.3 %collective-permute-start.11 = (bf16[5,128,256]{2,1,0:T(8,128)(2,1)S(1)}, bf16[5,128,256]{2,1,0:T(8,128)(2,1)S(1)}, u32[]{:S(2)}, u32[]{:S(2)}) collective-permute-start(bf16[5,128,256]{2,1,0:T(8,128)(2,1)S(1)} %slice_bitcast_fusion), channel_id=1, source_target_pairs={{0,24},{8,0},{16,8},{24,16},{1,25},{9,1},{17,9},{25,17},{2,26},{10... | collective-permute-start | bytes 983048 | tf_op jit(solution)/shard_map/ppermute | solution.py:266
  128.0 12.8 %collective-permute-start.9 = (bf16[5,128,256]{2,1,0:T(8,128)(2,1)S(1)}, bf16[5,128,256]{2,1,0:T(8,128)(2,1)S(1)}, u32[]{:S(2)}, u32[]{:S(2)}) collective-permute-start(bf16[5,128,256]{2,1,0:T(8,128)(2,1)S(1)} %slice_bitcast_fusion.1), channel_id=1, source_target_pairs={{0,8},{8,16},{16,24},{24,0},{1,9},{9,17},{17,25},{25,1},{2,10},{10... | collective-permute-start | bytes 983048 | tf_op jit(solution)/shard_map/ppermute | solution.py:265
  140.9 9.9 %copy-start.1 = (bf16[512,2048]{1,0:T(8,128)(2,1)S(1)}, bf16[512,2048]{1,0:T(8,128)(2,1)}, u32[]{:S(2)}) copy-start(bf16[512,2048]{1,0:T(8,128)(2,1)} %w_ref.1) | copy-start | bytes 6291460
  147.7 3.0 %collective-permute-start.18 = (f32[8,152,256]{2,1,0:T(8,128)S(1)}, f32[8,152,256]{2,1,0:T(8,128)S(1)}, u32[]{:S(2)}, u32[]{:S(2)}) collective-permute-start(f32[8,152,256]{2,1,0:T(8,128)S(1)} %get-tuple-element.47), channel_id=1, source_target_pairs={{0,4},{4,0},{1,5},{5,1},{2,6},{6,2},{3,7},{7,3},{8,12},{12,8},{9,1... | collective-permute-start | bytes 3735560 | tf_op jit(solution)/shard_map/ppermute | solution.py:303
  153.4 111.7 %all-to-all-start.1 = ((bf16[4,64,2048]{2,1,0:T(8,128)(2,1)}), bf16[4,64,2048]{2,1,0:T(8,128)(2,1)S(1)}, u32[]{:S(2)}, u32[]{:S(2)}) async-start(bf16[4,64,2048]{2,1,0:T(8,128)(2,1)} %bitcast.26), calls=%async_computation.1 | async-start | bytes 2097152 | tf_op jit(solution)/shard_map/all_to_all | solution.py:313
  (12 other events, 56.1 us)

commit v2 on v1

--- a/solution.py
+++ b/solution.py
@@ -42,13 +42,15 @@
 
 
 def first_kernel(place_ref, kv_ref, oth_kv_ref, q_ref, own_ref, oth_ref):
-    keys = jnp.concatenate([kv_ref[0, 0, :, :HALF], kv_ref[1, 0, :, :HALF]], axis=0)
-    oth_keys = jnp.concatenate([oth_kv_ref[0, 0, :, :HALF], oth_kv_ref[1, 0, :, :HALF]], axis=0)
-    values = with_ones(kv_ref[0, 0, :, HALF:], kv_ref[1, 0, :, HALF:])
+    keys = jnp.concatenate([kv_ref[0, 0, :, :HALF], kv_ref[0, 1, :, :HALF]], axis=0)
+    oth_keys = jnp.concatenate([oth_kv_ref[0, 0, :, :HALF], oth_kv_ref[0, 1, :, :HALF]], axis=0)
+    values = with_ones(kv_ref[0, 0, :, HALF:], kv_ref[0, 1, :, HALF:])
     row = lax.broadcasted_iota(jnp.int32, (ROWS, ROWS), 0)
     col = lax.broadcasted_iota(jnp.int32, (ROWS, ROWS), 1)
     diagonal = row <= col
-    for i in range(MAPS):
+    both = place_ref[2] == 0
+
+    def one_map(i, carry):
         q_own, q_oth = q_ref[i, :, :ROWS], q_ref[i, :, ROWS:]
         s = jnp.where(diagonal, dot(keys, q_own), NEG)
         top = jnp.max(s, axis=0, keepdims=True)
@@ -56,18 +58,38 @@
         own_ref[i, 0:144] = dot(values, p)
         own_ref[i, 144:152] = jnp.broadcast_to(top, (8, ROWS))
         top = jnp.max(jnp.where(diagonal, dot(oth_keys, q_oth), NEG), axis=0, keepdims=True)
+        s = jnp.where(both, dot(keys, q_oth), NEG)
+        top = jnp.maximum(top, jnp.max(s, axis=0, keepdims=True))
+        p = jnp.exp2(s - top).astype(BF16)
+        oth_ref[i, 0:144] = dot(values, p)
         oth_ref[i, 144:152] = jnp.broadcast_to(top, (8, ROWS))
-        oth_ref[i, 0:144] = jnp.zeros((144, ROWS), F32)
-
-    @pl.when(place_ref[2] == 0)
-    def _():
-        for i in range(MAPS):
-            before = oth_ref[i, 144:145]
-            s = dot(keys, q_ref[i, :, ROWS:])
-            top = jnp.maximum(before, jnp.max(s, axis=0, keepdims=True))
-            p = jnp.exp2(s - top).astype(BF16)
-            oth_ref[i, 0:144] = dot(values, p)
-            oth_ref[i, 144:152] = jnp.broadcast_to(top, (8, ROWS))
+        return carry
+
+    lax.fori_loop(0, MAPS, one_map, 0, unroll=2)
+
+
+def front_kernel(place_ref, p0, p1a, p1b, p2a, p2b, p3a, p3b, gain_ref, w_ref, normed_ref, kv_ref):
+    x = place_ref[3]
+
+    def put(piece_ref, back, half, rows):
+        values = piece_ref[...].astype(F32)
+        scale = lax.rsqrt(jnp.mean(values * values, axis=1, keepdims=True) + NORM_EPS)
+        at = pl.multiple_of(((x - back) & 3) * 64 + half * 32, 32)
+        normed_ref[pl.ds(at, rows), :] = (values * scale * gain_ref[...]).astype(BF16)
+
+    put(p0, 0, 0, 64)
+    put(p1a, 1, 0, 32)
+    put(p1b, 1, 1, 32)
+    put(p3a, 3, 0, 32)
+    put(p3b, 3, 1, 32)
+    put(p2a, 2, 0, 32)
+    put(p2b, 2, 1, 32)
+    both = dot(normed_ref[...], w_ref[...])
+    values_t = both[:, HALF:].T.astype(BF16)
+    for half in range(2):
+        rows = slice(half * HALF, half * HALF + HALF)
+        kv_ref[0, half, :, :HALF] = both[rows, :HALF].astype(BF16)
+        kv_ref[0, half, :, HALF:] = values_t[:, rows]
 
 
 def chunk_kernel(plan, n_in, *refs):
@@ -78,8 +100,8 @@
     z, y = place_ref[0], place_ref[1]
     visible = jnp.int32(0)
     at = 0
-    for _, dy, planes in plan:
-        for dz in planes:
+    for _, offsets in plan:
+        for dz, dy in offsets:
             sees = ((z + dz) & 7) * 4 + ((y + dy) & 3) < z * 4 + y
             list_ref[visible] = at
             visible = visible + sees.astype(jnp.int32)
@@ -88,14 +110,14 @@
     def fetch(which, slot):
         at = 0
         rows = slice(slot * ROWS, slot * ROWS + HALF), slice(slot * ROWS + HALF, slot * ROWS + ROWS)
-        for pair, _, planes in plan:
-            count = len(planes)
+        for pair, offsets in plan:
+            count = len(offsets)
 
             @pl.when((which >= at) & (which < at + count))
             def _(pair=pair, at=at):
                 b = which - at
                 for half in range(2):
-                    source = ins[pair[half]].at[b] if isinstance(pair, tuple) else ins[pair].at[half, b]
+                    source = ins[pair].at[b, half]
                     keys_ref[rows[half]] = source[:, :HALF]
                     values_ref[0:HALF, rows[half]] = source[:, HALF:]
             at += count
@@ -172,7 +194,7 @@
 
 def attend_chunk(place, q, state, plan, arrays, name):
     n = len(arrays)
-    blocks = sum(len(planes) for _, _, planes in plan)
+    blocks = sum(len(offsets) for _, offsets in plan)
     return pl.pallas_call(
         functools.partial(chunk_kernel, plan, n),
         out_shape=STATE,
@@ -236,35 +258,37 @@
     width = tokens.shape[1]
     z, y, c = lax.axis_index("z"), lax.axis_index("y"), lax.axis_index("c")
     place = jnp.stack([z, y, c, lax.axis_index("x")])
-    pieces = lax.all_to_all(jnp.broadcast_to(tokens[None], (4, *tokens.shape)), "x", 0, 0, tiled=True)
+    halves = tokens[:32], tokens[32:]
+    up_a = lax.ppermute(halves[0], "x", ring(4, 1))
+    down_b = lax.ppermute(halves[1], "x", ring(4, -1))
+    up_b = lax.ppermute(halves[1], "x", ring(4, 1))
+    down_a = lax.ppermute(halves[0], "x", ring(4, -1))
+    far_a = lax.ppermute(up_a, "x", ring(4, 1))
+    far_b = lax.ppermute(down_b, "x", ring(4, -1))
     gate_w, query_w = gate_weight.reshape(width, -1), query_weight.reshape(width, -1)
-    pieces, gate_w, query_w = lax.optimization_barrier((pieces, gate_w, query_w))
-    inputs = pieces.reshape(ROWS, width).astype(F32)
-    normed = (inputs * lax.rsqrt(jnp.mean(inputs * inputs, axis=1, keepdims=True) + NORM_EPS) * norm_gain).astype(BF16)
+    kv_w = jnp.concatenate([key_weight[:, 0], value_weight[:, 0]], axis=1)
+    far_a, gate_w, query_w, kv_w = lax.optimization_barrier((far_a, gate_w, query_w, kv_w))
+    normed, kv = pl.pallas_call(
+        front_kernel,
+        out_shape=(jax.ShapeDtypeStruct((ROWS, width), BF16), jax.ShapeDtypeStruct((1, 2, HALF, 2 * HALF), BF16)),
+        in_specs=[SMEM] + [VMEM] * 9,
+        out_specs=(VMEM, VMEM),
+        compiler_params=vmem(16),
+        name="front",
+    )(place, tokens, up_a, up_b, far_a, far_b, down_a, down_b, norm_gain[None], kv_w)
 
     def project(weight):
         return dot(normed, weight.reshape(width, -1)).astype(BF16)
 
-    keys = project(key_weight)
-    values_t = lax.dot_general(value_weight.reshape(width, 128), normed, (((0,), (1,)), ((), ())), preferred_element_type=F32).astype(BF16)
-    kv = jnp.concatenate(
-        [keys.reshape(2, 1, HALF, HALF), jnp.transpose(values_t.reshape(HALF, 2, HALF), (1, 0, 2))[:, None]], axis=3
-    )
-    up, down = [kv], [kv]
-    for k in range(4):
+    beside = [lax.ppermute(kv, "y", ring(4, step)) for step in (1, -1, 2)]
+    group = jnp.concatenate([kv, *beside], axis=0)
+    columns = (0, -1, 1, 2)
+    up, down = [group], [group]
+    for k in range(3):
         up.append(lax.ppermute(up[-1], "z", ring(8, 1)))
-        if k < 3:
-            down.append(lax.ppermute(down[-1], "z", ring(8, -1)))
-    near = jnp.concatenate([kv, up[1], down[1]], axis=1)
-    far = jnp.concatenate([up[2], up[3], up[4], down[2], down[3]], axis=1)
-    near_at, far_at = (0, -1, 1), (-2, -3, -4, 2, 3)
-
-    def around_y(group):
-        low = lax.ppermute(group, "y", ring(4, 1))
-        high = lax.ppermute(group, "y", ring(4, -1))
-        a = lax.ppermute(low[0], "y", ring(4, 1))
-        b = lax.ppermute(high[1], "y", ring(4, -1))
-        return low, high, a, b
+        down.append(lax.ppermute(down[-1], "z", ring(8, -1)))
+    up.append(lax.ppermute(up[3][:2], "z", ring(8, 1)))
+    down.append(lax.ppermute(down[3][2:], "z", ring(8, -1)))
 
     scale = (query_weight.shape[2] // 2) ** -0.5 * LOG2E
     q_own = (
@@ -294,12 +318,14 @@
         first_kernel, out_shape=STATE, in_specs=[SMEM, VMEM, VMEM, VMEM], out_specs=(VMEM, VMEM), compiler_params=vmem(16), name="first"
     )(place, kv, kv_oth, in_vmem(q))
     state, keep, part = lax.optimization_barrier((state, keep, part))
-    state = attend_chunk(place, q, state, ((0, 0, (-1,)), (1, 0, (1,))), (up[1], down[1]), "z_near")
-    state = attend_chunk(place, q, state, ((0, 0, far_at),), (far,), "z_far")
-    for group, at, name in ((near, near_at, "near"), (far, far_at, "far")):
-        low, high, a, b = around_y(group)
-        state = attend_chunk(place, q, state, ((0, -1, at), (1, 1, at)), (low, high), "y_" + name)
-        state = attend_chunk(place, q, state, (((0, 1), 2, at),), (a, b), "d_" + name)
+    plan = tuple((i, ((0, dy),)) for i, dy in enumerate(columns[1:]))
+    state = attend_chunk(place, q, state, plan, beside, "chunk0")
+    for k in range(1, 5):
+        plan = (
+            (0, tuple((-k, dy) for dy in (columns if k < 4 else columns[:2]))),
+            (1, tuple((k, dy) for dy in (columns if k < 4 else columns[2:]))),
+        )
+        state = attend_chunk(place, q, state, plan, (up[k], down[k]), f"chunk{k}")
     other = lax.ppermute(state[1], "c", [(0, 1), (1, 0)])
     out, logs = pl.pallas_call(
         finish_kernel,

time: 270 us -> 235 us (0.87); the launches traced: 266 us -> 235 us
  starting transfers between devices: 138 us -> 27.3 us
  Pallas kernels: 66.9 us -> 166 us
  waiting for transfers between devices: 31.9 us -> 20 us
  local copies, waits for them, and re-layouts: 18.8 us -> 14 us
    pallas_call x6 -> x5, Pallas kernels: 58.1 us -> 156 us  [attend_chunk(): pl.pallas_call(functools.partial(chunk_kernel, plan, n), out_shape=STATE,...]
    all_to_all x1, starting transfers between devices: 96.3 us -> 3.51 us  [local(): shares = lax.all_to_all(out.reshape(4, 64, width), 'x', 0, 0, tiled=True)]
    ppermute x8 -> x11, starting transfers between devices: 27.9 us -> 15.2 us  [the longest x3 3.34 us: local(): beside = [lax.ppermute(kv, 'y', ring(4, step)) for step in (1, -1, 2)]]
    all_to_all x1 -> x0, waiting for transfers between devices: 7.76 us -> none  [local(): lax.all_to_all(jnp.broadcast_to(tokens[None], (4, *tokens.shape)), 'x', 0...]
    all_to_all x1 -> x0, starting transfers between devices: 4.29 us -> none  [local(): lax.all_to_all(jnp.broadcast_to(tokens[None], (4, *tokens.shape)), 'x', 0...]
    ppermute x4 -> x3, waiting for transfers between devices: 4.03 us -> 0.01 us  [local(): up.append(lax.ppermute(up[-1], 'z', ring(8, 1)))]
    unnamed x36 -> x35, local copies, waits for them, and re-layouts: 10.5 us -> 7.51 us
  transfers between devices with their start and end apart: 21 -> 22, of which waited for: 6 -> 4; matrix products, arithmetic and copies ran while one was open for 8% -> 7% of each run, Pallas kernels for 22% -> 60%
where the time goes in v2:
time: 235 us
  Pallas kernels  166 us (71%)
  starting transfers between devices  27.3 us (12%)
  waiting for transfers between devices  20 us (9%)
  local copies, waits for them, and re-layouts  14 us (6%)
  other arithmetic  3.26 us (1%)
  matrix products  2.75 us (1%)
    pallas_call x5, Pallas kernels, attend_chunk(): pl.pallas_call(functools.partial(chunk_kernel, plan, n), out_shape=STATE,...  156 us
    all_to_all x1, waiting for transfers between devices, local(): shares = lax.all_to_all(out.reshape(4, 64, width), 'x', 0, 0, tiled=True)  15 us
    unnamed x35, local copies, waits for them, and re-layouts  7.51 us
    ppermute x3, starting transfers between devices, local(): down.append(lax.ppermute(down[-1], 'z', ring(8, -1)))  4.93 us
    pallas_call x1, Pallas kernels, local(): pl.pallas_call(first_kernel, out_shape=STATE, in_specs=[SMEM, VMEM, VMEM,...  4.7 us
  transfers between devices with their start and end apart: 22, of which 4 were waited for; matrix products, arithmetic and copies ran while one was open for 7% of the time, Pallas kernels for 60%

profile of v2, /device:TPU:248, one launch (start us, length us, event | category | flops | bytes accessed | tf_op | source)
XLA Modules:
  0.0 234.8 jit_solution(4655450784113892045)
XLA Ops:
  0.6 1.8 fusion.6
  2.5 1.5 collective-permute-start
  4.0 1.7 collective-permute-start.3
  6.0 3.0 %collective-permute-start.5 = (bf16[32,2048]{1,0:T(8,128)(2,1)}, bf16[32,2048]{1,0:T(8,128)(2,1)}, u32[]{:S(2)}, u32[]{:S(2)}) collective-permute-start(bf16[32,2048]{1,0:T(8,128)(2,1)} %get-tuple-element.57), channel_id=1, source_target_pairs={{0,3},{1,0},{2,1},{3,2},{4,7},{5,4},{6,5},{7,6},{8,11},{9,8},{10,9... | collective-permute-start | bytes 393224 | tf_op jit(solution)/shard_map/ppermute | solution.py:265
  10.5 2.0 collective-permute-start.4
  13.8 3.5 %copy.22 = bf16[256,8,2,512]{3,1,2,0:T(8,128)(2,1)S(1)} copy(bf16[256,8,2,512]{3,2,1,0:T(2,128)(2,1)} %bitcast.50) | data formatting | bytes 8388608
  19.4 1.9 front.1
  21.8 1.8 collective-permute-start.8
  26.9 2.1 collective-permute-start.19
  30.3 1.7 collective-permute-done.19.rim_ref
  35.3 2.0 collective-permute-start.14
  38.1 2.1 copy.17
  41.6 4.7 %first.1 = (f32[8,152,256]{2,1,0:T(8,128)S(1)}, f32[8,152,256]{2,1,0:T(8,128)S(1)}) custom-call(s32[4]{0:T(128)S(1)} %pad_add_fusion.place_ref.refs_0_, bf16[1,2,128,256]{3,2,1,0:T(8,128)(2,1)S(1)} %get-tuple-element.32.kv_ref, bf16[1,2,128,256]{3,2,1,0:T(8,128)(2,1)S(1)} %collective-permute-done.18.oth_kv_ref, bf16[8,128,512]{2,1,0:T(8,128)(2,1)S(1)} %bitcast.41), custom_call_target="tpu_custom_call" | custom-call | tf_op jit(solution)/shard_map/first/pallas_call | solution.py:317
  46.3 16.5 %chunk0.1 = (f32[8,152,256]{2,1,0:T(8,128)S(1)}, f32[8,152,256]{2,1,0:T(8,128)S(1)}) custom-call(s32[4]{0:T(128)S(1)} %pad_add_fusion.place_ref.refs_0_, bf16[8,128,512]{2,1,0:T(8,128)(2,1)S(1)} %bitcast.42, bf16[1,2,128,256]{3,2,1,0:T(8,128)(2,1)S(1)} %collective-permute-done.7.refs_2_, bf16[1,2,128,256]{3,2,1,0:T(8,128)(2,1)S(1)} %copy-done.7, ...), custom_call_target="tpu_custom_call" | custom-call | flops 3221225472 | bytes 1048576 | tf_op jit(solution)/shard_map/chunk0/pallas_call | solution.py:198
  65.0 40.2 %chunk1.1 = (f32[8,152,256]{2,1,0:T(8,128)S(1)}, f32[8,152,256]{2,1,0:T(8,128)S(1)}) custom-call(s32[4]{0:T(128)S(1)} %pad_add_fusion.place_ref.refs_0_, bf16[8,128,512]{2,1,0:T(8,128)(2,1)S(1)} %bitcast.43, bf16[4,2,128,256]{3,2,1,0:T(8,128)(2,1)} %collective-permute-done.10.refs_2_, bf16[4,2,128,256]{3,2,1,0:T(8,128)(2,1)} %collective-permute-done.14.refs_3_, ...), custom_call_target="tpu_custom_call" | custom-call | flops 8589934592 | bytes 1048576 | tf_op jit(solution)/shard_map/chunk1/pallas_call | solution.py:198
  105.3 2.0 collective-permute-start.16
  107.3 39.7 %chunk2.1 = (f32[8,152,256]{2,1,0:T(8,128)S(1)}, f32[8,152,256]{2,1,0:T(8,128)S(1)}) custom-call(s32[4]{0:T(128)S(1)} %pad_add_fusion.place_ref.refs_0_, bf16[8,128,512]{2,1,0:T(8,128)(2,1)S(1)} %bitcast.44, bf16[4,2,128,256]{3,2,1,0:T(8,128)(2,1)S(1)} %collective-permute-done.11.refs_2_, bf16[4,2,128,256]{3,2,1,0:T(8,128)(2,1)S(1)} %collective-permute-done.15.refs_3_, ...), custom_call_target="tpu_custom_call" | custom-call | flops 8589934592 | bytes 1048576 | tf_op jit(solution)/shard_map/chunk2/pallas_call | solution.py:198
  147.2 2.1 collective-permute-start.17
  149.3 39.5 %chunk3.1 = (f32[8,152,256]{2,1,0:T(8,128)S(1)}, f32[8,152,256]{2,1,0:T(8,128)S(1)}) custom-call(s32[4]{0:T(128)S(1)} %pad_add_fusion.place_ref.refs_0_, bf16[8,128,512]{2,1,0:T(8,128)(2,1)S(1)} %bitcast.45, bf16[4,2,128,256]{3,2,1,0:T(8,128)(2,1)S(1)} %collective-permute-done.12.refs_2_, bf16[4,2,128,256]{3,2,1,0:T(8,128)(2,1)S(1)} %collective-permute-done.16.refs_3_, ...), custom_call_target="tpu_custom_call" | custom-call | flops 8589934592 | bytes 1048576 | tf_op jit(solution)/shard_map/chunk3/pallas_call | solution.py:198
  188.8 20.3 %chunk4.1 = (f32[8,152,256]{2,1,0:T(8,128)S(1)}, f32[8,152,256]{2,1,0:T(8,128)S(1)}) custom-call(s32[4]{0:T(128)S(1)} %pad_add_fusion.place_ref.refs_0_, bf16[8,128,512]{2,1,0:T(8,128)(2,1)S(1)} %bitcast.46, bf16[2,2,128,256]{3,2,1,0:T(8,128)(2,1)S(1)} %collective-permute-done.13.refs_2_, bf16[2,2,128,256]{3,2,1,0:T(8,128)(2,1)S(1)} %collective-permute-done.17.refs_3_, ...), custom_call_target="tpu_custom_call" | custom-call | flops 4294967296 | bytes 1048576 | tf_op jit(solution)/shard_map/chunk4/pallas_call | solution.py:198
  209.2 2.9 %collective-permute-done.20.b_ref = f32[8,152,256]{2,1,0:T(8,128)S(1)} collective-permute-done((f32[8,152,256]{2,1,0:T(8,128)S(1)}, f32[8,152,256]{2,1,0:T(8,128)S(1)}, u32[]{:S(2)}, u32[]{:S(2)}) %collective-permute-start.20) | collective-permute-done | bytes 1245216 | tf_op jit(solution)/shard_map/ppermute | solution.py:329
  212.1 2.6 %finish.1 = (bf16[256,2048]{1,0:T(8,128)(2,1)}, f32[8,256]{1,0:T(8,128)S(1)}) custom-call(f32[4]{0:T(128)S(1)} %copy-done.12, f32[8,152,256]{2,1,0:T(8,128)S(1)} %get-tuple-element.48.a_ref, f32[8,152,256]{2,1,0:T(8,128)S(1)} %collective-permute-done.20.b_ref, f32[1,128]{1,0:T(1,128)S(1)} %bitcast.49, f32[256,512]{1,0:T(8,128)S(1)} %get-tuple-element.50.keep_ref, ...), custom_call_target="tpu_custom_call" | custom-call | tf_op jit(solution)/shard_map/finish/pallas_call | solution.py:330
  214.7 3.5 %all-to-all-start = ((bf16[4,64,2048]{2,1,0:T(8,128)(2,1)}), bf16[4,64,2048]{2,1,0:T(8,128)(2,1)S(1)}, u32[]{:S(2)}, u32[]{:S(2)}) async-start(bf16[4,64,2048]{2,1,0:T(8,128)(2,1)} %bitcast.16), calls=%async_computation | async-start | bytes 2097152 | tf_op jit(solution)/shard_map/all_to_all | solution.py:339
  218.9 15.0 %all-to-all-done = bf16[4,64,2048]{2,1,0:T(8,128)(2,1)S(1)} async-done(((bf16[4,64,2048]{2,1,0:T(8,128)(2,1)}), bf16[4,64,2048]{2,1,0:T(8,128)(2,1)S(1)}, u32[]{:S(2)}, u32[]{:S(2)}) %all-to-all-start) | async-done | bytes 1048608 | tf_op jit(solution)/shard_map/all_to_all | solution.py:339
  (83 shorter events, 19.6 us)
Async XLA Ops:
  0.6 25.5 %copy-start = (bf16[2048,1,512]{2,0,1:T(8,128)(2,1)S(1)}, bf16[2048,1,512]{2,0,1:T(8,128)(2,1)}, u32[]{:S(2)}) copy-start(bf16[2048,1,512]{2,0,1:T(8,128)(2,1)} %param.19) | copy-start | bytes 6291460
  2.5 6.8 %collective-permute-start = (bf16[32,2048]{1,0:T(8,128)(2,1)}, bf16[32,2048]{1,0:T(8,128)(2,1)S(1)}, u32[]{:S(2)}, u32[]{:S(2)}) collective-permute-start(bf16[32,2048]{1,0:T(8,128)(2,1)} %get-tuple-element.57), channel_id=1, source_target_pairs={{0,1},{1,2},{2,3},{3,0},{4,5},{5,6},{6,7},{7,4},{8,9},{9,10},{10,1... | collective-permute-start | bytes 393224 | tf_op jit(solution)/shard_map/ppermute | solution.py:262
  4.0 6.6 %collective-permute-start.3 = (bf16[32,2048]{1,0:T(8,128)(2,1)}, bf16[32,2048]{1,0:T(8,128)(2,1)S(1)}, u32[]{:S(2)}, u32[]{:S(2)}) collective-permute-start(bf16[32,2048]{1,0:T(8,128)(2,1)} %get-tuple-element.56), channel_id=1, source_target_pairs={{0,3},{1,0},{2,1},{3,2},{4,7},{5,4},{6,5},{7,6},{8,11},{9,8},{10,9... | collective-permute-start | bytes 393224 | tf_op jit(solution)/shard_map/ppermute | solution.py:263
  5.7 12.1 %collective-permute-start.2 = (bf16[32,2048]{1,0:T(8,128)(2,1)}, bf16[32,2048]{1,0:T(8,128)(2,1)S(1)}, u32[]{:S(2)}, u32[]{:S(2)}) collective-permute-start(bf16[32,2048]{1,0:T(8,128)(2,1)} %get-tuple-element.56), channel_id=1, source_target_pairs={{0,1},{1,2},{2,3},{3,0},{4,5},{5,6},{6,7},{7,4},{8,9},{9,10},{10,1... | collective-permute-start | bytes 393224 | tf_op jit(solution)/shard_map/ppermute | solution.py:264
  6.0 12.5 %collective-permute-start.5 = (bf16[32,2048]{1,0:T(8,128)(2,1)}, bf16[32,2048]{1,0:T(8,128)(2,1)}, u32[]{:S(2)}, u32[]{:S(2)}) collective-permute-start(bf16[32,2048]{1,0:T(8,128)(2,1)} %get-tuple-element.57), channel_id=1, source_target_pairs={{0,3},{1,0},{2,1},{3,2},{4,7},{5,4},{6,5},{7,6},{8,11},{9,8},{10,9... | collective-permute-start | bytes 393224 | tf_op jit(solution)/shard_map/ppermute | solution.py:265
  9.3 8.6 %collective-permute-start.1 = (bf16[32,2048]{1,0:T(8,128)(2,1)S(1)}, bf16[32,2048]{1,0:T(8,128)(2,1)}, u32[]{:S(2)}, u32[]{:S(2)}) collective-permute-start(bf16[32,2048]{1,0:T(8,128)(2,1)S(1)} %collective-permute-done.p1a), channel_id=1, source_target_pairs={{0,1},{1,2},{2,3},{3,0},{4,5},{5,6},{6,7},{7,4},{8,9},{9,10},{10,1... | collective-permute-start | bytes 393224 | tf_op jit(solution)/shard_map/ppermute | solution.py:266
  10.5 8.0 %collective-permute-start.4 = (bf16[32,2048]{1,0:T(8,128)(2,1)S(1)}, bf16[32,2048]{1,0:T(8,128)(2,1)}, u32[]{:S(2)}, u32[]{:S(2)}) collective-permute-start(bf16[32,2048]{1,0:T(8,128)(2,1)S(1)} %collective-permute-done.3.p3b), channel_id=1, source_target_pairs={{0,3},{1,0},{2,1},{3,2},{4,7},{5,4},{6,5},{7,6},{8,11},{9,8},{10,9... | collective-permute-start | bytes 393224 | tf_op jit(solution)/shard_map/ppermute | solution.py:267
  21.4 20.2 %collective-permute-start.18 = (bf16[1,2,128,256]{3,2,1,0:T(8,128)(2,1)S(1)}, bf16[1,2,128,256]{3,2,1,0:T(8,128)(2,1)S(1)}, u32[]{:S(2)}, u32[]{:S(2)}) collective-permute-start(bf16[1,2,128,256]{3,2,1,0:T(8,128)(2,1)S(1)} %get-tuple-element.32.kv_ref), channel_id=1, source_target_pairs={{0,4},{4,0},{1,5},{5,1},{2,6},{6,2},{3,7},{7,3},{8,12},{12,8},{9,1... | collective-permute-start | bytes 393224 | tf_op jit(solution)/shard_map/ppermute | solution.py:298
  21.5 11.7 %collective-permute-start.7 = (bf16[1,2,128,256]{3,2,1,0:T(8,128)(2,1)S(1)}, bf16[1,2,128,256]{3,2,1,0:T(8,128)(2,1)S(1)}, u32[]{:S(2)}, u32[]{:S(2)}) collective-permute-start(bf16[1,2,128,256]{3,2,1,0:T(8,128)(2,1)S(1)} %get-tuple-element.32.kv_ref), channel_id=1, source_target_pairs={{0,8},{8,16},{16,24},{24,0},{1,9},{9,17},{17,25},{25,1},{2,10},{10... | collective-permute-start | bytes 393224 | tf_op jit(solution)/shard_map/ppermute | solution.py:283
  21.8 12.1 %collective-permute-start.8 = (bf16[1,2,128,256]{3,2,1,0:T(8,128)(2,1)S(1)}, bf16[1,2,128,256]{3,2,1,0:T(8,128)(2,1)S(1)}, u32[]{:S(2)}, u32[]{:S(2)}) collective-permute-start(bf16[1,2,128,256]{3,2,1,0:T(8,128)(2,1)S(1)} %get-tuple-element.32.kv_ref), channel_id=1, source_target_pairs={{0,24},{8,0},{16,8},{24,16},{1,25},{9,1},{17,9},{25,17},{2,26},{10... | collective-permute-start | bytes 393224 | tf_op jit(solution)/shard_map/ppermute | solution.py:283
  23.6 11.0 %collective-permute-start.9 = (bf16[1,2,128,256]{3,2,1,0:T(8,128)(2,1)S(1)}, bf16[1,2,128,256]{3,2,1,0:T(8,128)(2,1)S(1)}, u32[]{:S(2)}, u32[]{:S(2)}) collective-permute-start(bf16[1,2,128,256]{3,2,1,0:T(8,128)(2,1)S(1)} %get-tuple-element.32.kv_ref), channel_id=1, source_target_pairs={{0,16},{8,24},{16,0},{24,8},{1,17},{9,25},{17,1},{25,9},{2,18},{10... | collective-permute-start | bytes 393224 | tf_op jit(solution)/shard_map/ppermute | solution.py:283
  26.9 5.2 %collective-permute-start.19 = (bf16[16,512]{1,0:T(8,128)(2,1)S(1)}, bf16[16,512]{1,0:T(8,128)(2,1)S(1)}, u32[]{:S(2)}, u32[]{:S(2)}) collective-permute-start(bf16[16,512]{1,0:T(8,128)(2,1)S(1)} %slice.32), channel_id=1, source_target_pairs={{0,4},{4,8},{8,12},{12,16},{16,20},{20,24},{24,28},{28,32},{32,36}... | collective-permute-start | bytes 49160 | tf_op jit(solution)/shard_map/ppermute | solution.py:306
  32.1 5.2 %collective-permute-start.6 = (bf16[512,256]{0,1:T(8,128)(2,1)S(1)}, bf16[512,256]{0,1:T(8,128)(2,1)S(1)}, u32[]{:S(2)}, u32[]{:S(2)}) collective-permute-start(bf16[512,256]{0,1:T(8,128)(2,1)S(1)} %fusion.2), channel_id=1, source_target_pairs={{0,4},{4,0},{1,5},{5,1},{2,6},{6,2},{3,7},{7,3},{8,12},{12,8},{9,1... | collective-permute-start | bytes 786440 | tf_op jit(solution)/shard_map/ppermute | solution.py:297
  35.3 27.5 %collective-permute-start.10 = (bf16[4,2,128,256]{3,2,1,0:T(8,128)(2,1)}, bf16[4,2,128,256]{3,2,1,0:T(8,128)(2,1)}, u32[]{:S(2)}, u32[]{:S(2)}) collective-permute-start(bf16[4,2,128,256]{3,2,1,0:T(8,128)(2,1)} %constant_dynamic-update-slice_fusion), channel_id=1, source_target_pairs={{0,32},{32,64},{64,96},{96,128},{128,160},{160,192},{192,224},{224... | collective-permute-start | bytes 1572872 | tf_op jit(solution)/shard_map/ppermute | solution.py:288
  35.3 28.8 %collective-permute-start.14 = (bf16[4,2,128,256]{3,2,1,0:T(8,128)(2,1)}, bf16[4,2,128,256]{3,2,1,0:T(8,128)(2,1)}, u32[]{:S(2)}, u32[]{:S(2)}) collective-permute-start(bf16[4,2,128,256]{3,2,1,0:T(8,128)(2,1)} %constant_dynamic-update-slice_fusion), channel_id=1, source_target_pairs={{0,224},{32,0},{64,32},{96,64},{128,96},{160,128},{192,160},{224,1... | collective-permute-start | bytes 1572872 | tf_op jit(solution)/shard_map/ppermute | solution.py:289
  62.8 42.4 %collective-permute-start.11 = (bf16[4,2,128,256]{3,2,1,0:T(8,128)(2,1)}, bf16[4,2,128,256]{3,2,1,0:T(8,128)(2,1)S(1)}, u32[]{:S(2)}, u32[]{:S(2)}) collective-permute-start(bf16[4,2,128,256]{3,2,1,0:T(8,128)(2,1)} %collective-permute-done.10.refs_2_), channel_id=1, source_target_pairs={{0,32},{32,64},{64,96},{96,128},{128,160},{160,192},{192,224},{224... | collective-permute-start | bytes 1572872 | tf_op jit(solution)/shard_map/ppermute | solution.py:288
  64.1 41.2 %collective-permute-start.15 = (bf16[4,2,128,256]{3,2,1,0:T(8,128)(2,1)}, bf16[4,2,128,256]{3,2,1,0:T(8,128)(2,1)S(1)}, u32[]{:S(2)}, u32[]{:S(2)}) collective-permute-start(bf16[4,2,128,256]{3,2,1,0:T(8,128)(2,1)} %collective-permute-done.14.refs_3_), channel_id=1, source_target_pairs={{0,224},{32,0},{64,32},{96,64},{128,96},{160,128},{192,160},{224,1... | collective-permute-start | bytes 1572872 | tf_op jit(solution)/shard_map/ppermute | solution.py:289
  105.2 41.8 %collective-permute-start.12 = (bf16[4,2,128,256]{3,2,1,0:T(8,128)(2,1)S(1)}, bf16[4,2,128,256]{3,2,1,0:T(8,128)(2,1)S(1)}, u32[]{:S(2)}, u32[]{:S(2)}) collective-permute-start(bf16[4,2,128,256]{3,2,1,0:T(8,128)(2,1)S(1)} %collective-permute-done.11.refs_2_), channel_id=1, source_target_pairs={{0,32},{32,64},{64,96},{96,128},{128,160},{160,192},{192,224},{224... | collective-permute-start | bytes 1572872 | tf_op jit(solution)/shard_map/ppermute | solution.py:288
  105.3 41.9 %collective-permute-start.16 = (bf16[4,2,128,256]{3,2,1,0:T(8,128)(2,1)S(1)}, bf16[4,2,128,256]{3,2,1,0:T(8,128)(2,1)S(1)}, u32[]{:S(2)}, u32[]{:S(2)}) collective-permute-start(bf16[4,2,128,256]{3,2,1,0:T(8,128)(2,1)S(1)} %collective-permute-done.15.refs_3_), channel_id=1, source_target_pairs={{0,224},{32,0},{64,32},{96,64},{128,96},{160,128},{192,160},{224,1... | collective-permute-start | bytes 1572872 | tf_op jit(solution)/shard_map/ppermute | solution.py:289
  147.0 41.7 %collective-permute-start.13 = (bf16[2,2,128,256]{3,2,1,0:T(8,128)(2,1)S(1)}, bf16[2,2,128,256]{3,2,1,0:T(8,128)(2,1)S(1)}, u32[]{:S(2)}, u32[]{:S(2)}) collective-permute-start(bf16[2,2,128,256]{3,2,1,0:T(8,128)(2,1)S(1)} %slice.30), channel_id=1, source_target_pairs={{0,32},{32,64},{64,96},{96,128},{128,160},{160,192},{192,224},{224... | collective-permute-start | bytes 786440 | tf_op jit(solution)/shard_map/ppermute | solution.py:290
  147.2 41.6 %collective-permute-start.17 = (bf16[2,2,128,256]{3,2,1,0:T(8,128)(2,1)S(1)}, bf16[2,2,128,256]{3,2,1,0:T(8,128)(2,1)S(1)}, u32[]{:S(2)}, u32[]{:S(2)}) collective-permute-start(bf16[2,2,128,256]{3,2,1,0:T(8,128)(2,1)S(1)} %slice.31), channel_id=1, source_target_pairs={{0,224},{32,0},{64,32},{96,64},{128,96},{160,128},{192,160},{224,1... | collective-permute-start | bytes 786440 | tf_op jit(solution)/shard_map/ppermute | solution.py:291
  188.8 23.3 %copy-start.1 = (bf16[512,2048]{1,0:T(8,128)(2,1)S(1)}, bf16[512,2048]{1,0:T(8,128)(2,1)}, u32[]{:S(2)}) copy-start(bf16[512,2048]{1,0:T(8,128)(2,1)} %w_ref.1) | copy-start | bytes 6291460
  209.1 3.0 %collective-permute-start.20 = (f32[8,152,256]{2,1,0:T(8,128)S(1)}, f32[8,152,256]{2,1,0:T(8,128)S(1)}, u32[]{:S(2)}, u32[]{:S(2)}) collective-permute-start(f32[8,152,256]{2,1,0:T(8,128)S(1)} %get-tuple-element.49), channel_id=1, source_target_pairs={{0,4},{4,0},{1,5},{5,1},{2,6},{6,2},{3,7},{7,3},{8,12},{12,8},{9,1... | collective-permute-start | bytes 3735560 | tf_op jit(solution)/shard_map/ppermute | solution.py:329
  214.7 19.2 %all-to-all-start = ((bf16[4,64,2048]{2,1,0:T(8,128)(2,1)}), bf16[4,64,2048]{2,1,0:T(8,128)(2,1)S(1)}, u32[]{:S(2)}, u32[]{:S(2)}) async-start(bf16[4,64,2048]{2,1,0:T(8,128)(2,1)} %bitcast.16), calls=%async_computation | async-start | bytes 2097152 | tf_op jit(solution)/shard_map/all_to_all | solution.py:339
  (13 other events, 75.5 us)

commit v3 on v2

--- a/solution.py
+++ b/solution.py
@@ -41,49 +41,55 @@
     return jnp.concatenate([values, jnp.ones((16, values.shape[1]), BF16)], axis=0)
 
 
-def first_kernel(place_ref, kv_ref, oth_kv_ref, q_ref, own_ref, oth_ref):
+def first_kernel(place_ref, kv_ref, oth_kv_ref, q_own_ref, q_oth_ref, own_ref, oth_ref, q_ref, p_a, p_b):
+    for i in range(MAPS):
+        here, there = slice(i % 2 * 64, i % 2 * 64 + 64), slice(64 - i % 2 * 64, 128 - i % 2 * 64)
+        q_ref[i, here, :ROWS] = q_own_ref[i * 64 : i * 64 + 64]
+        q_ref[i, here, ROWS:] = q_oth_ref[i * 64 : i * 64 + 64]
+        q_ref[i, there] = jnp.zeros((64, 2 * ROWS), BF16)
     keys = jnp.concatenate([kv_ref[0, 0, :, :HALF], kv_ref[0, 1, :, :HALF]], axis=0)
     oth_keys = jnp.concatenate([oth_kv_ref[0, 0, :, :HALF], oth_kv_ref[0, 1, :, :HALF]], axis=0)
     values = with_ones(kv_ref[0, 0, :, HALF:], kv_ref[0, 1, :, HALF:])
-    row = lax.broadcasted_iota(jnp.int32, (ROWS, ROWS), 0)
-    col = lax.broadcasted_iota(jnp.int32, (ROWS, ROWS), 1)
-    diagonal = row <= col
-    both = place_ref[2] == 0
-
-    def one_map(i, carry):
-        q_own, q_oth = q_ref[i, :, :ROWS], q_ref[i, :, ROWS:]
-        s = jnp.where(diagonal, dot(keys, q_own), NEG)
+    row = lax.broadcasted_iota(jnp.int32, (ROWS, 2 * ROWS), 0)
+    col = lax.broadcasted_iota(jnp.int32, (ROWS, 2 * ROWS), 1)
+    seen = row <= jnp.where(col < ROWS, col, jnp.where(place_ref[2] == 0, ROWS, -1))
+    diagonal = (row <= col)[:, :ROWS]
+    probs = (p_a, p_b)
+
+    def scores(i, slot):
+        s = jnp.where(seen, dot(keys, q_ref[i]), NEG)
+        seed = jnp.max(jnp.where(diagonal, dot(oth_keys, q_ref[i, :, ROWS:]), NEG), axis=0, keepdims=True)
         top = jnp.max(s, axis=0, keepdims=True)
-        p = jnp.exp2(s - top).astype(BF16)
-        own_ref[i, 0:144] = dot(values, p)
-        own_ref[i, 144:152] = jnp.broadcast_to(top, (8, ROWS))
-        top = jnp.max(jnp.where(diagonal, dot(oth_keys, q_oth), NEG), axis=0, keepdims=True)
-        s = jnp.where(both, dot(keys, q_oth), NEG)
-        top = jnp.maximum(top, jnp.max(s, axis=0, keepdims=True))
-        p = jnp.exp2(s - top).astype(BF16)
-        oth_ref[i, 0:144] = dot(values, p)
-        oth_ref[i, 144:152] = jnp.broadcast_to(top, (8, ROWS))
+        top = jnp.concatenate([top[:, :ROWS], jnp.maximum(top[:, ROWS:], seed)], axis=1)
+        probs[slot][...] = jnp.exp2(s - top).astype(BF16)
+        own_ref[i, 144:152] = jnp.broadcast_to(top[:, :ROWS], (8, ROWS))
+        oth_ref[i, 144:152] = jnp.broadcast_to(top[:, ROWS:], (8, ROWS))
+
+    def sums(i, slot):
+        out = dot(values, probs[slot][...])
+        own_ref[i, 0:144] = out[:, :ROWS]
+        oth_ref[i, 0:144] = out[:, ROWS:]
+
+    def two_maps(h, carry):
+        scores(2 * h, 0)
+        scores(2 * h + 1, 1)
+        sums(2 * h, 0)
+        sums(2 * h + 1, 1)
         return carry
 
-    lax.fori_loop(0, MAPS, one_map, 0, unroll=2)
-
-
-def front_kernel(place_ref, p0, p1a, p1b, p2a, p2b, p3a, p3b, gain_ref, w_ref, normed_ref, kv_ref):
-    x = place_ref[3]
-
-    def put(piece_ref, back, half, rows):
-        values = piece_ref[...].astype(F32)
+    lax.fori_loop(0, MAPS // 2, two_maps, 0)
+
+
+def join_kernel(a, b, c, d, out_ref):
+    for i, ref in enumerate((a, b, c, d)):
+        out_ref[i] = ref[0]
+
+
+def front_kernel(rows_ref, gain_ref, w_ref, normed_ref, kv_ref):
+    for j in range(4):
+        values = rows_ref[j].astype(F32)
         scale = lax.rsqrt(jnp.mean(values * values, axis=1, keepdims=True) + NORM_EPS)
-        at = pl.multiple_of(((x - back) & 3) * 64 + half * 32, 32)
-        normed_ref[pl.ds(at, rows), :] = (values * scale * gain_ref[...]).astype(BF16)
-
-    put(p0, 0, 0, 64)
-    put(p1a, 1, 0, 32)
-    put(p1b, 1, 1, 32)
-    put(p3a, 3, 0, 32)
-    put(p3b, 3, 1, 32)
-    put(p2a, 2, 0, 32)
-    put(p2b, 2, 1, 32)
+        normed_ref[j * 64 : j * 64 + 64] = (values * scale * gain_ref[...]).astype(BF16)
     both = dot(normed_ref[...], w_ref[...])
     values_t = both[:, HALF:].T.astype(BF16)
     for half in range(2):
@@ -235,7 +241,9 @@
     part_ref[...] = jax.nn.sigmoid(gate_ref[:, width:].astype(F32)) * mixed
 
 
-def finish_kernel(lam_ref, a_ref, b_ref, gain_ref, keep_ref, part_ref, w_ref, out_ref, log_ref, merged_ref):
+def finish_kernel(place_ref, lam_ref, a_ref, b_ref, gain_ref, keep_ref, part_ref, w_ref, *refs):
+    own_out, up_a, up_b, far_a, far_b, down_a, down_b, log_ref, merged_ref = refs
+    x = place_ref[3]
     for h in range(MAPS // 2):
         maps = []
         for m in range(2):
@@ -249,39 +257,45 @@
         head = maps[0] - lam_ref[h] * maps[1]
         head = head * lax.rsqrt(jnp.mean(head * head, axis=0, keepdims=True) + NORM_EPS)
         cols = slice(h * 128, h * 128 + 128)
-        attended = head.T * gain_ref[...]
-        merged_ref[:, cols] = (keep_ref[:, cols] * attended + part_ref[:, cols]).astype(BF16)
-    out_ref[...] = dot(merged_ref[...], w_ref[...]).astype(BF16)
+        merged = (keep_ref[:, cols] * (head.T * gain_ref[...]) + part_ref[:, cols]).astype(BF16)
+        for j in range(4):
+            at = pl.multiple_of(((j - x) & 3) * 64, 64)
+            merged_ref[pl.ds(at, 64), cols] = merged[j * 64 : j * 64 + 64]
+    out = dot(merged_ref[...], w_ref[...]).astype(BF16)
+    own_out[...] = out[:64]
+    for i, ref in enumerate((up_a, up_b, far_a, far_b, down_a, down_b)):
+        ref[...] = out[64 + i * 32 : 96 + i * 32]
 
 
 def local(tokens, norm_gain, query_weight, key_weight, value_weight, mix_lambda, head_gain, pool_weight, pool_mix, pool_scale, gate_weight, out_weight):
     width = tokens.shape[1]
     z, y, c = lax.axis_index("z"), lax.axis_index("y"), lax.axis_index("c")
     place = jnp.stack([z, y, c, lax.axis_index("x")])
-    halves = tokens[:32], tokens[32:]
-    up_a = lax.ppermute(halves[0], "x", ring(4, 1))
-    down_b = lax.ppermute(halves[1], "x", ring(4, -1))
-    up_b = lax.ppermute(halves[1], "x", ring(4, 1))
-    down_a = lax.ppermute(halves[0], "x", ring(4, -1))
-    far_a = lax.ppermute(up_a, "x", ring(4, 1))
-    far_b = lax.ppermute(down_b, "x", ring(4, -1))
+    pieces = lax.all_to_all(jnp.broadcast_to(tokens[None], (4, *tokens.shape)), "x", 0, 0, tiled=True)
     gate_w, query_w = gate_weight.reshape(width, -1), query_weight.reshape(width, -1)
     kv_w = jnp.concatenate([key_weight[:, 0], value_weight[:, 0]], axis=1)
-    far_a, gate_w, query_w, kv_w = lax.optimization_barrier((far_a, gate_w, query_w, kv_w))
+    pieces, gate_w, query_w, kv_w = lax.optimization_barrier((pieces, gate_w, query_w, kv_w))
     normed, kv = pl.pallas_call(
         front_kernel,
         out_shape=(jax.ShapeDtypeStruct((ROWS, width), BF16), jax.ShapeDtypeStruct((1, 2, HALF, 2 * HALF), BF16)),
-        in_specs=[SMEM] + [VMEM] * 9,
+        in_specs=[VMEM] * 3,
         out_specs=(VMEM, VMEM),
         compiler_params=vmem(16),
         name="front",
-    )(place, tokens, up_a, up_b, far_a, far_b, down_a, down_b, norm_gain[None], kv_w)
+    )(pieces, norm_gain[None], kv_w)
 
     def project(weight):
         return dot(normed, weight.reshape(width, -1)).astype(BF16)
 
     beside = [lax.ppermute(kv, "y", ring(4, step)) for step in (1, -1, 2)]
-    group = jnp.concatenate([kv, *beside], axis=0)
+    group = pl.pallas_call(
+        join_kernel,
+        out_shape=jax.ShapeDtypeStruct((4, 2, HALF, 2 * HALF), BF16),
+        in_specs=[VMEM] * 4,
+        out_specs=VMEM,
+        compiler_params=vmem(8),
+        name="join",
+    )(kv, *beside)
     columns = (0, -1, 1, 2)
     up, down = [group], [group]
     for k in range(3):
@@ -296,10 +310,6 @@
     ).astype(BF16)
     q_oth = lax.ppermute(q_own, "c", [(0, 1), (1, 0)])
     kv_oth = lax.ppermute(kv, "c", [(0, 1), (1, 0)])
-    q = jnp.concatenate([q_own, q_oth], axis=1).reshape(4, 2, 64, 2 * ROWS)
-    zero = jnp.zeros((4, 64, 2 * ROWS), BF16)
-    q = jnp.stack([jnp.concatenate([q[:, 0], zero], axis=1), jnp.concatenate([zero, q[:, 1]], axis=1)], axis=1)
-    q = q.reshape(MAPS, 128, 2 * ROWS)
 
     pool_in = project(pool_weight)
     gate_pre = project(gate_w)
@@ -314,10 +324,15 @@
         name="pool",
     )(place, pool_in, rim, gate_pre, pool_mix[0], pool_scale)
 
-    state = pl.pallas_call(
-        first_kernel, out_shape=STATE, in_specs=[SMEM, VMEM, VMEM, VMEM], out_specs=(VMEM, VMEM), compiler_params=vmem(16), name="first"
-    )(place, kv, kv_oth, in_vmem(q))
-    state, keep, part = lax.optimization_barrier((state, keep, part))
+    *state, q = pl.pallas_call(
+        first_kernel,
+        out_shape=(*STATE, pltpu.VMEM((MAPS, 128, 2 * ROWS), BF16)),
+        in_specs=[SMEM] + [VMEM] * 4,
+        out_specs=(VMEM, VMEM, VMEM),
+        scratch_shapes=[pltpu.VMEM((ROWS, 2 * ROWS), BF16)] * 2,
+        compiler_params=vmem(16),
+        name="first",
+    )(place, kv, kv_oth, q_own, q_oth)
     plan = tuple((i, ((0, dy),)) for i, dy in enumerate(columns[1:]))
     state = attend_chunk(place, q, state, plan, beside, "chunk0")
     for k in range(1, 5):
@@ -326,18 +341,30 @@
             (1, tuple((k, dy) for dy in (columns if k < 4 else columns[2:]))),
         )
         state = attend_chunk(place, q, state, plan, (up[k], down[k]), f"chunk{k}")
+        if k == 1:
+            state, keep, part = lax.optimization_barrier((state, keep, part))
     other = lax.ppermute(state[1], "c", [(0, 1), (1, 0)])
-    out, logs = pl.pallas_call(
+    piece = jax.ShapeDtypeStruct((32, width), BF16)
+    own, up_a, up_b, far_a, far_b, down_a, down_b, logs = pl.pallas_call(
         finish_kernel,
-        out_shape=(jax.ShapeDtypeStruct((ROWS, width), BF16), jax.ShapeDtypeStruct((MAPS, ROWS), F32)),
-        in_specs=[SMEM] + [VMEM] * 6,
-        out_specs=(VMEM, VMEM),
+        out_shape=(jax.ShapeDtypeStruct((64, width), BF16), *[piece] * 6, jax.ShapeDtypeStruct((MAPS, ROWS), F32)),
+        in_specs=[SMEM, SMEM] + [VMEM] * 6,
+        out_specs=(VMEM,) * 8,
         scratch_shapes=[pltpu.VMEM((ROWS, 512), BF16)],
         compiler_params=vmem(24),
         name="finish",
-    )(mix_lambda, state[0], other, head_gain[None], keep, part, out_weight)
-    shares = lax.all_to_all(out.reshape(4, 64, width), "x", 0, 0, tiled=True)
-    mixed = jnp.sum(shares.astype(F32), axis=0).astype(BF16)
+    )(place, mix_lambda, state[0], other, head_gain[None], keep, part, out_weight)
+    from_far_a = lax.ppermute(far_a, "x", ring(4, 1))
+    from_far_b = lax.ppermute(far_b, "x", ring(4, -1))
+    low_b = lax.ppermute(up_b, "x", ring(4, 1))
+    high_a = lax.ppermute(down_a, "x", ring(4, -1))
+
+    def add(*arrays):
+        return sum(a.astype(F32) for a in arrays).astype(BF16)
+
+    low_a = lax.ppermute(add(up_a, from_far_a), "x", ring(4, 1))
+    high_b = lax.ppermute(add(down_b, from_far_b), "x", ring(4, -1))
+    mixed = jnp.concatenate([add(own[:32], low_a, high_a), add(own[32:], low_b, high_b)], axis=0)
     return mixed, jnp.transpose(logs.reshape(4, 2, ROWS), (1, 0, 2))
 
 

time: 235 us -> 230 us (0.979)
  starting transfers between devices: 27.3 us -> 35.2 us
  waiting for transfers between devices: 20 us -> 14.4 us
  local copies, waits for them, and re-layouts: 14 us -> 10.8 us
  Pallas kernels: 166 us -> 163 us
    all_to_all x1, waiting for transfers between devices: 15 us -> 7.18 us  [local(): lax.all_to_all(jnp.broadcast_to(tokens[None], (4, *tokens.shape)), 'x', 0...]
    ppermute x3, starting transfers between devices: 1.38 us -> 6.88 us  [local(): up.append(lax.ppermute(up[-1], 'z', ring(8, 1)))]
    ppermute x6, waiting for transfers between devices: 0.32 us -> 4.3 us  [the longest x1 2 us: local(): from_far_b = lax.ppermute(far_b, 'x', ring(4, -1))]
    ppermute x1, starting transfers between devices: 0.08 us -> 3.29 us  [local(): up.append(lax.ppermute(up[3][:2], 'z', ring(8, 1)))]
    concatenate x2 -> x0, local copies, waits for them, and re-layouts: 2.77 us -> none  [the longest x1 2.06 us: local(): q = jnp.concatenate([q_own, q_oth], axis=1).reshape(4, 2, 64, 2 * ROWS)]
    pallas_call x2 -> x3, Pallas kernels: 7.32 us -> 4.81 us  [the longest x1 3.09 us: local(): pl.pallas_call(first_kernel, out_shape=(*STATE, pltpu.VMEM((MAPS, 128, 2...]
    unnamed x35 -> x28, local copies, waits for them, and re-layouts: 7.51 us -> 7.94 us
  transfers between devices with their start and end apart: 22 -> 22, of which waited for: 4 -> 5; matrix products, arithmetic and copies ran while one was open for 7% -> 5% of each run, Pallas kernels for 60% -> 61%
where the time goes in v3:
time: 230 us; the launch traced here: 229 us
  Pallas kernels  163 us (71%)
  starting transfers between devices  35.2 us (15%)
  waiting for transfers between devices  14.4 us (6%)
  local copies, waits for them, and re-layouts  10.8 us (5%)
  matrix products  2.76 us (1%)
    pallas_call x5, Pallas kernels, attend_chunk(): pl.pallas_call(functools.partial(chunk_kernel, plan, n), out_shape=STATE,...  156 us
    unnamed x28, local copies, waits for them, and re-layouts  7.94 us
    all_to_all x1, waiting for transfers between devices, local(): lax.all_to_all(jnp.broadcast_to(tokens[None], (4, *tokens.shape)), 'x', 0...  7.18 us
    ppermute x3, starting transfers between devices, local(): up.append(lax.ppermute(up[-1], 'z', ring(8, 1)))  6.88 us
  transfers between devices with their start and end apart: 22, of which 5 were waited for; matrix products, arithmetic and copies ran while one was open for 5% of the time, Pallas kernels for 61%

profile of v3, /device:TPU:248, one launch (start us, length us, event | category | flops | bytes accessed | tf_op | source)
XLA Modules:
  0.0 229.3 jit_solution(1915658247310404523)
XLA Ops:
  0.6 2.2 broadcast_in_dim.12
  2.8 4.3 %all-to-all-start = ((bf16[4,64,2048]{2,1,0:T(8,128)(2,1)}), bf16[4,64,2048]{2,1,0:T(8,128)(2,1)S(1)}, u32[]{:S(2)}, u32[]{:S(2)}) async-start(bf16[4,64,2048]{2,1,0:T(8,128)(2,1)} %broadcast_in_dim.12), calls=%async_computation | async-start | bytes 2097152 | tf_op jit(solution)/shard_map/all_to_all | solution.py:274
  7.1 3.5 %copy.19 = bf16[256,8,4,128]{3,1,2,0:T(8,128)(2,1)} copy(bf16[256,8,4,128]{3,2,1,0:T(4,128)(2,1)} %bitcast.33) | data formatting | bytes 4194304
  10.6 3.2 %copy.15 = bf16[256,8,2,512]{3,1,2,0:T(8,128)(2,1)} copy(bf16[256,8,2,512]{3,2,1,0:T(2,128)(2,1)S(1)} %bitcast.31) | data formatting | bytes 8388608
  15.0 7.2 %all-to-all-done.rows_ref = bf16[4,64,2048]{2,1,0:T(8,128)(2,1)S(1)} async-done(((bf16[4,64,2048]{2,1,0:T(8,128)(2,1)}), bf16[4,64,2048]{2,1,0:T(8,128)(2,1)S(1)}, u32[]{:S(2)}, u32[]{:S(2)}) %all-to-all-start) | async-done | bytes 1048608 | tf_op jit(solution)/shard_map/all_to_all | solution.py:274
  25.6 3.2 %collective-permute-start.2 = (bf16[1,2,128,256]{3,2,1,0:T(8,128)(2,1)S(1)}, bf16[1,2,128,256]{3,2,1,0:T(8,128)(2,1)S(1)}, u32[]{:S(2)}, u32[]{:S(2)}) collective-permute-start(bf16[1,2,128,256]{3,2,1,0:T(8,128)(2,1)S(1)} %get-tuple-element.37.kv_ref.a), channel_id=1, source_target_pairs={{0,8},{8,16},{16,24},{24,0},{1,9},{9,17},{17,25},{25,1},{2,10},{10... | collective-permute-start | bytes 393224 | tf_op jit(solution)/shard_map/ppermute | solution.py:290
  30.3 2.5 %collective-permute-start.13 = (bf16[16,512]{1,0:T(8,128)(2,1)S(1)}, bf16[16,512]{1,0:T(8,128)(2,1)S(1)}, u32[]{:S(2)}, u32[]{:S(2)}) collective-permute-start(bf16[16,512]{1,0:T(8,128)(2,1)S(1)} %slice.22), channel_id=1, source_target_pairs={{0,4},{4,8},{8,12},{12,16},{16,20},{20,24},{24,28},{28,32},{32,36}... | collective-permute-start | bytes 49160 | tf_op jit(solution)/shard_map/ppermute | solution.py:316
  33.1 2.1 collective-permute-start.9
  38.8 3.1 %first.1 = (f32[8,152,256]{2,1,0:T(8,128)S(1)}, f32[8,152,256]{2,1,0:T(8,128)S(1)}, bf16[8,128,512]{2,1,0:T(8,128)(2,1)S(1)}) custom-call(s32[4]{0:T(128)S(1)} %pad_add_fusion.place_ref.refs_0_, bf16[1,2,128,256]{3,2,1,0:T(8,128)(2,1)S(1)} %get-tuple-element.37.kv_ref.a, bf16[1,2,128,256]{3,2,1,0:T(8,128)(2,1)S(1)} %collective-permute-done.oth_kv_ref, ...), custom_call_target="tpu_custom_call" | custom-call | tf_op jit(solution)/shard_map/first/pallas_call | solution.py:327
  41.9 16.9 %chunk0.1 = (f32[8,152,256]{2,1,0:T(8,128)S(1)}, f32[8,152,256]{2,1,0:T(8,128)S(1)}) custom-call(s32[4]{0:T(128)S(1)} %pad_add_fusion.place_ref.refs_0_, bf16[8,128,512]{2,1,0:T(8,128)(2,1)S(1)} %get-tuple-element.40.refs_1_, bf16[1,2,128,256]{3,2,1,0:T(8,128)(2,1)S(1)} %collective-permute-done.2.b.refs_2_, ...), custom_call_target="tpu_custom_call" | custom-call | flops 3221225472 | bytes 1048576 | tf_op jit(solution)/shard_map/chunk0/pallas_call | solution.py:204
  59.8 2.4 %collective-permute-start.6 = (bf16[4,2,128,256]{3,2,1,0:T(8,128)(2,1)S(1)}, bf16[4,2,128,256]{3,2,1,0:T(8,128)(2,1)S(1)}, u32[]{:S(2)}, u32[]{:S(2)}) collective-permute-start(bf16[4,2,128,256]{3,2,1,0:T(8,128)(2,1)S(1)} %collective-permute-done.5.refs_2_), channel_id=1, source_target_pairs={{0,32},{32,64},{64,96},{96,128},{128,160},{160,192},{192,224},{224... | collective-permute-start | bytes 1572872 | tf_op jit(solution)/shard_map/ppermute | solution.py:302
  62.2 39.6 %chunk1.1 = (f32[8,152,256]{2,1,0:T(8,128)S(1)}, f32[8,152,256]{2,1,0:T(8,128)S(1)}) custom-call(s32[4]{0:T(128)S(1)} %pad_add_fusion.place_ref.refs_0_, bf16[8,128,512]{2,1,0:T(8,128)(2,1)S(1)} %get-tuple-element.40.refs_1_, bf16[4,2,128,256]{3,2,1,0:T(8,128)(2,1)S(1)} %collective-permute-done.5.refs_2_, ...), custom_call_target="tpu_custom_call" | custom-call | flops 8589934592 | bytes 1048576 | tf_op jit(solution)/shard_map/chunk1/pallas_call | solution.py:204
  101.9 3.2 %collective-permute-start.7 = (bf16[4,2,128,256]{3,2,1,0:T(8,128)(2,1)S(1)}, bf16[4,2,128,256]{3,2,1,0:T(8,128)(2,1)S(1)}, u32[]{:S(2)}, u32[]{:S(2)}) collective-permute-start(bf16[4,2,128,256]{3,2,1,0:T(8,128)(2,1)S(1)} %collective-permute-done.6.refs_2_), channel_id=1, source_target_pairs={{0,32},{32,64},{64,96},{96,128},{128,160},{160,192},{192,224},{224... | collective-permute-start | bytes 1572872 | tf_op jit(solution)/shard_map/ppermute | solution.py:302
  105.1 39.6 %chunk2.1 = (f32[8,152,256]{2,1,0:T(8,128)S(1)}, f32[8,152,256]{2,1,0:T(8,128)S(1)}) custom-call(s32[4]{0:T(128)S(1)} %pad_add_fusion.place_ref.refs_0_, bf16[8,128,512]{2,1,0:T(8,128)(2,1)S(1)} %get-tuple-element.40.refs_1_, bf16[4,2,128,256]{3,2,1,0:T(8,128)(2,1)S(1)} %collective-permute-done.6.refs_2_, ...), custom_call_target="tpu_custom_call" | custom-call | flops 8589934592 | bytes 1048576 | tf_op jit(solution)/shard_map/chunk2/pallas_call | solution.py:204
  144.8 3.3 %collective-permute-start.8 = (bf16[2,2,128,256]{3,2,1,0:T(8,128)(2,1)S(1)}, bf16[2,2,128,256]{3,2,1,0:T(8,128)(2,1)S(1)}, u32[]{:S(2)}, u32[]{:S(2)}) collective-permute-start(bf16[2,2,128,256]{3,2,1,0:T(8,128)(2,1)S(1)} %slice.20), channel_id=1, source_target_pairs={{0,32},{32,64},{64,96},{96,128},{128,160},{160,192},{192,224},{224... | collective-permute-start | bytes 786440 | tf_op jit(solution)/shard_map/ppermute | solution.py:304
  148.1 39.9 %chunk3.1 = (f32[8,152,256]{2,1,0:T(8,128)S(1)}, f32[8,152,256]{2,1,0:T(8,128)S(1)}) custom-call(s32[4]{0:T(128)S(1)} %pad_add_fusion.place_ref.refs_0_, bf16[8,128,512]{2,1,0:T(8,128)(2,1)S(1)} %get-tuple-element.40.refs_1_, bf16[4,2,128,256]{3,2,1,0:T(8,128)(2,1)S(1)} %collective-permute-done.7.refs_2_, ...), custom_call_target="tpu_custom_call" | custom-call | flops 8589934592 | bytes 1048576 | tf_op jit(solution)/shard_map/chunk3/pallas_call | solution.py:204
  188.1 20.3 %chunk4.1 = (f32[8,152,256]{2,1,0:T(8,128)S(1)}, f32[8,152,256]{2,1,0:T(8,128)S(1)}) custom-call(s32[4]{0:T(128)S(1)} %pad_add_fusion.place_ref.refs_0_, bf16[8,128,512]{2,1,0:T(8,128)(2,1)S(1)} %get-tuple-element.40.refs_1_, bf16[2,2,128,256]{3,2,1,0:T(8,128)(2,1)S(1)} %collective-permute-done.8.refs_2_, ...), custom_call_target="tpu_custom_call" | custom-call | flops 4294967296 | bytes 1048576 | tf_op jit(solution)/shard_map/chunk4/pallas_call | solution.py:204
  208.5 2.9 %collective-permute-done.14.b_ref = f32[8,152,256]{2,1,0:T(8,128)S(1)} collective-permute-done((f32[8,152,256]{2,1,0:T(8,128)S(1)}, f32[8,152,256]{2,1,0:T(8,128)S(1)}, u32[]{:S(2)}, u32[]{:S(2)}) %collective-permute-start.14) | collective-permute-done | bytes 1245216 | tf_op jit(solution)/shard_map/ppermute | solution.py:346
  211.5 1.7 finish.1
  213.8 2.7 %collective-permute-start.17 = (bf16[32,2048]{1,0:T(8,128)(2,1)S(1)}, bf16[32,2048]{1,0:T(8,128)(2,1)S(1)}, u32[]{:S(2)}, u32[]{:S(2)}) collective-permute-start(bf16[32,2048]{1,0:T(8,128)(2,1)S(1)} %get-tuple-element.63), channel_id=1, source_target_pairs={{0,3},{1,0},{2,1},{3,2},{4,7},{5,4},{6,5},{7,6},{8,11},{9,8},{10,9... | collective-permute-start | bytes 393224 | tf_op jit(solution)/shard_map/ppermute | solution.py:360
  216.5 3.2 %collective-permute-start.19 = (bf16[32,2048]{1,0:T(8,128)(2,1)S(1)}, bf16[32,2048]{1,0:T(8,128)(2,1)S(1)}, u32[]{:S(2)}, u32[]{:S(2)}) collective-permute-start(bf16[32,2048]{1,0:T(8,128)(2,1)S(1)} %get-tuple-element.66), channel_id=1, source_target_pairs={{0,3},{1,0},{2,1},{3,2},{4,7},{5,4},{6,5},{7,6},{8,11},{9,8},{10,9... | collective-permute-start | bytes 393224 | tf_op jit(solution)/shard_map/ppermute | solution.py:358
  220.2 2.0 collective-permute-done.19
  222.3 3.7 %collective-permute-start.20 = (bf16[32,2048]{1,0:T(8,128)(2,1)S(1)}, bf16[32,2048]{1,0:T(8,128)(2,1)S(1)}, u32[]{:S(2)}, u32[]{:S(2)}) collective-permute-start(bf16[32,2048]{1,0:T(8,128)(2,1)S(1)} %add_convert_fusion.1), channel_id=1, source_target_pairs={{0,3},{1,0},{2,1},{3,2},{4,7},{5,4},{6,5},{7,6},{8,11},{9,8},{10,9... | collective-permute-start | bytes 393224 | tf_op jit(solution)/shard_map/ppermute | solution.py:366
  226.6 1.9 collective-permute-done.20
  (73 shorter events, 13.7 us)
Async XLA Ops:
  0.6 29.0 %copy-start = (bf16[2048,1,512]{2,0,1:T(8,128)(2,1)S(1)}, bf16[2048,1,512]{2,0,1:T(8,128)(2,1)}, u32[]{:S(2)}) copy-start(bf16[2048,1,512]{2,0,1:T(8,128)(2,1)} %param.19) | copy-start | bytes 6291460
  2.8 19.4 %all-to-all-start = ((bf16[4,64,2048]{2,1,0:T(8,128)(2,1)}), bf16[4,64,2048]{2,1,0:T(8,128)(2,1)S(1)}, u32[]{:S(2)}, u32[]{:S(2)}) async-start(bf16[4,64,2048]{2,1,0:T(8,128)(2,1)} %broadcast_in_dim.12), calls=%async_computation | async-start | bytes 2097152 | tf_op jit(solution)/shard_map/all_to_all | solution.py:274
  24.3 8.6 %collective-permute-start.4 = (bf16[1,2,128,256]{3,2,1,0:T(8,128)(2,1)S(1)}, bf16[1,2,128,256]{3,2,1,0:T(8,128)(2,1)S(1)}, u32[]{:S(2)}, u32[]{:S(2)}) collective-permute-start(bf16[1,2,128,256]{3,2,1,0:T(8,128)(2,1)S(1)} %get-tuple-element.37.kv_ref.a), channel_id=1, source_target_pairs={{0,16},{8,24},{16,0},{24,8},{1,17},{9,25},{17,1},{25,9},{2,18},{10... | collective-permute-start | bytes 393224 | tf_op jit(solution)/shard_map/ppermute | solution.py:290
  25.6 7.4 %collective-permute-start.3 = (bf16[1,2,128,256]{3,2,1,0:T(8,128)(2,1)S(1)}, bf16[1,2,128,256]{3,2,1,0:T(8,128)(2,1)S(1)}, u32[]{:S(2)}, u32[]{:S(2)}) collective-permute-start(bf16[1,2,128,256]{3,2,1,0:T(8,128)(2,1)S(1)} %get-tuple-element.37.kv_ref.a), channel_id=1, source_target_pairs={{0,24},{8,0},{16,8},{24,16},{1,25},{9,1},{17,9},{25,17},{2,26},{10... | collective-permute-start | bytes 393224 | tf_op jit(solution)/shard_map/ppermute | solution.py:290
  25.6 7.4 %collective-permute-start.2 = (bf16[1,2,128,256]{3,2,1,0:T(8,128)(2,1)S(1)}, bf16[1,2,128,256]{3,2,1,0:T(8,128)(2,1)S(1)}, u32[]{:S(2)}, u32[]{:S(2)}) collective-permute-start(bf16[1,2,128,256]{3,2,1,0:T(8,128)(2,1)S(1)} %get-tuple-element.37.kv_ref.a), channel_id=1, source_target_pairs={{0,8},{8,16},{16,24},{24,0},{1,9},{9,17},{17,25},{25,1},{2,10},{10... | collective-permute-start | bytes 393224 | tf_op jit(solution)/shard_map/ppermute | solution.py:290
  28.8 10.0 %collective-permute-start = (bf16[1,2,128,256]{3,2,1,0:T(8,128)(2,1)S(1)}, bf16[1,2,128,256]{3,2,1,0:T(8,128)(2,1)S(1)}, u32[]{:S(2)}, u32[]{:S(2)}) collective-permute-start(bf16[1,2,128,256]{3,2,1,0:T(8,128)(2,1)S(1)} %get-tuple-element.37.kv_ref.a), channel_id=1, source_target_pairs={{0,4},{4,0},{1,5},{5,1},{2,6},{6,2},{3,7},{7,3},{8,12},{12,8},{9,1... | collective-permute-start | bytes 393224 | tf_op jit(solution)/shard_map/ppermute | solution.py:312
  30.3 7.4 %collective-permute-start.13 = (bf16[16,512]{1,0:T(8,128)(2,1)S(1)}, bf16[16,512]{1,0:T(8,128)(2,1)S(1)}, u32[]{:S(2)}, u32[]{:S(2)}) collective-permute-start(bf16[16,512]{1,0:T(8,128)(2,1)S(1)} %slice.22), channel_id=1, source_target_pairs={{0,4},{4,8},{8,12},{12,16},{16,20},{20,24},{24,28},{28,32},{32,36}... | collective-permute-start | bytes 49160 | tf_op jit(solution)/shard_map/ppermute | solution.py:316
  32.9 5.9 %collective-permute-start.1 = (bf16[512,256]{1,0:T(8,128)(2,1)S(1)}, bf16[512,256]{1,0:T(8,128)(2,1)S(1)}, u32[]{:S(2)}, u32[]{:S(2)}) collective-permute-start(bf16[512,256]{1,0:T(8,128)(2,1)S(1)} %fusion.2.q_own_ref), channel_id=1, source_target_pairs={{0,4},{4,0},{1,5},{5,1},{2,6},{6,2},{3,7},{7,3},{8,12},{12,8},{9,1... | collective-permute-start | bytes 786440 | tf_op jit(solution)/shard_map/ppermute | solution.py:311
  33.1 25.8 %collective-permute-start.9 = (bf16[4,2,128,256]{3,2,1,0:T(8,128)(2,1)S(1)}, bf16[4,2,128,256]{3,2,1,0:T(8,128)(2,1)S(1)}, u32[]{:S(2)}, u32[]{:S(2)}) collective-permute-start(bf16[4,2,128,256]{3,2,1,0:T(8,128)(2,1)S(1)} %join.1), channel_id=1, source_target_pairs={{0,224},{32,0},{64,32},{96,64},{128,96},{160,128},{192,160},{224,1... | collective-permute-start | bytes 1572872 | tf_op jit(solution)/shard_map/ppermute | solution.py:303
  35.2 24.6 %collective-permute-start.5 = (bf16[4,2,128,256]{3,2,1,0:T(8,128)(2,1)S(1)}, bf16[4,2,128,256]{3,2,1,0:T(8,128)(2,1)S(1)}, u32[]{:S(2)}, u32[]{:S(2)}) collective-permute-start(bf16[4,2,128,256]{3,2,1,0:T(8,128)(2,1)S(1)} %join.1), channel_id=1, source_target_pairs={{0,32},{32,64},{64,96},{96,128},{128,160},{160,192},{192,224},{224... | collective-permute-start | bytes 1572872 | tf_op jit(solution)/shard_map/ppermute | solution.py:302
  58.9 42.9 %collective-permute-start.10 = (bf16[4,2,128,256]{3,2,1,0:T(8,128)(2,1)S(1)}, bf16[4,2,128,256]{3,2,1,0:T(8,128)(2,1)S(1)}, u32[]{:S(2)}, u32[]{:S(2)}) collective-permute-start(bf16[4,2,128,256]{3,2,1,0:T(8,128)(2,1)S(1)} %collective-permute-done.9.refs_3_), channel_id=1, source_target_pairs={{0,224},{32,0},{64,32},{96,64},{128,96},{160,128},{192,160},{224,1... | collective-permute-start | bytes 1572872 | tf_op jit(solution)/shard_map/ppermute | solution.py:303
  59.8 42.1 %collective-permute-start.6 = (bf16[4,2,128,256]{3,2,1,0:T(8,128)(2,1)S(1)}, bf16[4,2,128,256]{3,2,1,0:T(8,128)(2,1)S(1)}, u32[]{:S(2)}, u32[]{:S(2)}) collective-permute-start(bf16[4,2,128,256]{3,2,1,0:T(8,128)(2,1)S(1)} %collective-permute-done.5.refs_2_), channel_id=1, source_target_pairs={{0,32},{32,64},{64,96},{96,128},{128,160},{160,192},{192,224},{224... | collective-permute-start | bytes 1572872 | tf_op jit(solution)/shard_map/ppermute | solution.py:302
  101.8 42.9 %collective-permute-start.11 = (bf16[4,2,128,256]{3,2,1,0:T(8,128)(2,1)S(1)}, bf16[4,2,128,256]{3,2,1,0:T(8,128)(2,1)S(1)}, u32[]{:S(2)}, u32[]{:S(2)}) collective-permute-start(bf16[4,2,128,256]{3,2,1,0:T(8,128)(2,1)S(1)} %collective-permute-done.10.refs_3_), channel_id=1, source_target_pairs={{0,224},{32,0},{64,32},{96,64},{128,96},{160,128},{192,160},{224,1... | collective-permute-start | bytes 1572872 | tf_op jit(solution)/shard_map/ppermute | solution.py:303
  101.9 42.9 %collective-permute-start.7 = (bf16[4,2,128,256]{3,2,1,0:T(8,128)(2,1)S(1)}, bf16[4,2,128,256]{3,2,1,0:T(8,128)(2,1)S(1)}, u32[]{:S(2)}, u32[]{:S(2)}) collective-permute-start(bf16[4,2,128,256]{3,2,1,0:T(8,128)(2,1)S(1)} %collective-permute-done.6.refs_2_), channel_id=1, source_target_pairs={{0,32},{32,64},{64,96},{96,128},{128,160},{160,192},{192,224},{224... | collective-permute-start | bytes 1572872 | tf_op jit(solution)/shard_map/ppermute | solution.py:302
  144.7 43.3 %collective-permute-start.12 = (bf16[2,2,128,256]{3,2,1,0:T(8,128)(2,1)S(1)}, bf16[2,2,128,256]{3,2,1,0:T(8,128)(2,1)S(1)}, u32[]{:S(2)}, u32[]{:S(2)}) collective-permute-start(bf16[2,2,128,256]{3,2,1,0:T(8,128)(2,1)S(1)} %slice.21), channel_id=1, source_target_pairs={{0,224},{32,0},{64,32},{96,64},{128,96},{160,128},{192,160},{224,1... | collective-permute-start | bytes 786440 | tf_op jit(solution)/shard_map/ppermute | solution.py:305
  144.8 43.2 %collective-permute-start.8 = (bf16[2,2,128,256]{3,2,1,0:T(8,128)(2,1)S(1)}, bf16[2,2,128,256]{3,2,1,0:T(8,128)(2,1)S(1)}, u32[]{:S(2)}, u32[]{:S(2)}) collective-permute-start(bf16[2,2,128,256]{3,2,1,0:T(8,128)(2,1)S(1)} %slice.20), channel_id=1, source_target_pairs={{0,32},{32,64},{64,96},{96,128},{128,160},{160,192},{192,224},{224... | collective-permute-start | bytes 786440 | tf_op jit(solution)/shard_map/ppermute | solution.py:304
  188.0 23.4 %copy-start.2 = (bf16[512,2048]{1,0:T(8,128)(2,1)S(1)}, bf16[512,2048]{1,0:T(8,128)(2,1)}, u32[]{:S(2)}) copy-start(bf16[512,2048]{1,0:T(8,128)(2,1)} %w_ref.1) | copy-start | bytes 6291460
  208.4 3.0 %collective-permute-start.14 = (f32[8,152,256]{2,1,0:T(8,128)S(1)}, f32[8,152,256]{2,1,0:T(8,128)S(1)}, u32[]{:S(2)}, u32[]{:S(2)}) collective-permute-start(f32[8,152,256]{2,1,0:T(8,128)S(1)} %get-tuple-element.57), channel_id=1, source_target_pairs={{0,4},{4,0},{1,5},{5,1},{2,6},{6,2},{3,7},{7,3},{8,12},{12,8},{9,1... | collective-permute-start | bytes 3735560 | tf_op jit(solution)/shard_map/ppermute | solution.py:346
  213.1 6.9 %collective-permute-start.15 = (bf16[32,2048]{1,0:T(8,128)(2,1)S(1)}, bf16[32,2048]{1,0:T(8,128)(2,1)S(1)}, u32[]{:S(2)}, u32[]{:S(2)}) collective-permute-start(bf16[32,2048]{1,0:T(8,128)(2,1)S(1)} %get-tuple-element.62), channel_id=1, source_target_pairs={{0,1},{1,2},{2,3},{3,0},{4,5},{5,6},{6,7},{7,4},{8,9},{9,10},{10,1... | collective-permute-start | bytes 393224 | tf_op jit(solution)/shard_map/ppermute | solution.py:357
  213.8 12.8 %collective-permute-start.17 = (bf16[32,2048]{1,0:T(8,128)(2,1)S(1)}, bf16[32,2048]{1,0:T(8,128)(2,1)S(1)}, u32[]{:S(2)}, u32[]{:S(2)}) collective-permute-start(bf16[32,2048]{1,0:T(8,128)(2,1)S(1)} %get-tuple-element.63), channel_id=1, source_target_pairs={{0,3},{1,0},{2,1},{3,2},{4,7},{5,4},{6,5},{7,6},{8,11},{9,8},{10,9... | collective-permute-start | bytes 393224 | tf_op jit(solution)/shard_map/ppermute | solution.py:360
  216.5 10.2 %collective-permute-start.18 = (bf16[32,2048]{1,0:T(8,128)(2,1)S(1)}, bf16[32,2048]{1,0:T(8,128)(2,1)S(1)}, u32[]{:S(2)}, u32[]{:S(2)}) collective-permute-start(bf16[32,2048]{1,0:T(8,128)(2,1)S(1)} %get-tuple-element.64), channel_id=1, source_target_pairs={{0,1},{1,2},{2,3},{3,0},{4,5},{5,6},{6,7},{7,4},{8,9},{9,10},{10,1... | collective-permute-start | bytes 393224 | tf_op jit(solution)/shard_map/ppermute | solution.py:359
  216.5 5.8 %collective-permute-start.19 = (bf16[32,2048]{1,0:T(8,128)(2,1)S(1)}, bf16[32,2048]{1,0:T(8,128)(2,1)S(1)}, u32[]{:S(2)}, u32[]{:S(2)}) collective-permute-start(bf16[32,2048]{1,0:T(8,128)(2,1)S(1)} %get-tuple-element.66), channel_id=1, source_target_pairs={{0,3},{1,0},{2,1},{3,2},{4,7},{5,4},{6,5},{7,6},{8,11},{9,8},{10,9... | collective-permute-start | bytes 393224 | tf_op jit(solution)/shard_map/ppermute | solution.py:358
  220.1 6.5 %collective-permute-start.16 = (bf16[32,2048]{1,0:T(8,128)(2,1)S(1)}, bf16[32,2048]{1,0:T(8,128)(2,1)S(1)}, u32[]{:S(2)}, u32[]{:S(2)}) collective-permute-start(bf16[32,2048]{1,0:T(8,128)(2,1)S(1)} %add_convert_fusion.3), channel_id=1, source_target_pairs={{0,1},{1,2},{2,3},{3,0},{4,5},{5,6},{6,7},{7,4},{8,9},{9,10},{10,1... | collective-permute-start | bytes 393224 | tf_op jit(solution)/shard_map/ppermute | solution.py:365
  222.3 6.3 %collective-permute-start.20 = (bf16[32,2048]{1,0:T(8,128)(2,1)S(1)}, bf16[32,2048]{1,0:T(8,128)(2,1)S(1)}, u32[]{:S(2)}, u32[]{:S(2)}) collective-permute-start(bf16[32,2048]{1,0:T(8,128)(2,1)S(1)} %add_convert_fusion.1), channel_id=1, source_target_pairs={{0,3},{1,0},{2,1},{3,2},{4,7},{5,4},{6,5},{7,6},{8,11},{9,8},{10,9... | collective-permute-start | bytes 393224 | tf_op jit(solution)/shard_map/ppermute | solution.py:366
  (11 other events, 87.9 us)

commit v4 on v3

--- a/solution.py
+++ b/solution.py
@@ -128,11 +128,16 @@
                     values_ref[0:HALF, rows[half]] = source[:, HALF:]
             at += count
 
-    own_ref[...] = own_in[...]
-    oth_ref[...] = oth_in[...]
+    def keep_state():
+        own_ref[...] = own_in[...]
+        oth_ref[...] = oth_in[...]
+
+    pl.when(visible == 0)(keep_state)
 
     @pl.when(visible > 0)
     def _():
+        own_ref[:, 144:] = own_in[:, 144:]
+        oth_ref[:, 144:] = oth_in[:, 144:]
         over_ref[...] = jnp.full(over_ref.shape, NEG, F32)
         values_ref[HALF:144] = jnp.ones((16, 2 * ROWS), BF16)
 
@@ -148,7 +153,7 @@
             keys, values = keys_ref[...], values_ref[...]
 
             def scores(i):
-                top = jnp.concatenate([own_ref[i, 144:145], oth_ref[i, 144:145]], axis=1)
+                top = jnp.concatenate([own_in[i, 144:145], oth_in[i, 144:145]], axis=1)
                 s = dot(keys, q_ref[i]) - top
                 over_ref[i] = jnp.maximum(over_ref[i], jnp.max(s.reshape(-1, 8, 2 * ROWS), axis=0))
                 probs[i % 2][...] = jnp.exp2(s).astype(BF16)
@@ -158,16 +163,15 @@
                 if i + 1 < MAPS:
                     scores(i + 1)
                 out = dot(values, probs[i % 2][...])
-                own_ref[i, 0:144] = own_ref[i, 0:144] + out[:, :ROWS]
-                oth_ref[i, 0:144] = oth_ref[i, 0:144] + out[:, ROWS:]
+                own_ref[i, 0:144] = jnp.where(t == 0, own_in[i, 0:144], own_ref[i, 0:144]) + out[:, :ROWS]
+                oth_ref[i, 0:144] = jnp.where(t == 0, oth_in[i, 0:144], oth_ref[i, 0:144]) + out[:, ROWS:]
             return carry
 
         lax.fori_loop(0, (visible + 1) // 2, two_blocks, 0)
 
         @pl.when(jnp.logical_not(jnp.max(over_ref[...]) <= LIMIT))
         def _():
-            own_ref[...] = own_in[...]
-            oth_ref[...] = oth_in[...]
+            keep_state()
             values_ref[HALF:144] = jnp.ones((16, 2 * ROWS), BF16)
 
             def one_block(t, carry):
@@ -284,9 +288,6 @@
         name="front",
     )(pieces, norm_gain[None], kv_w)
 
-    def project(weight):
-        return dot(normed, weight.reshape(width, -1)).astype(BF16)
-
     beside = [lax.ppermute(kv, "y", ring(4, step)) for step in (1, -1, 2)]
     group = pl.pallas_call(
         join_kernel,
@@ -311,19 +312,6 @@
     q_oth = lax.ppermute(q_own, "c", [(0, 1), (1, 0)])
     kv_oth = lax.ppermute(kv, "c", [(0, 1), (1, 0)])
 
-    pool_in = project(pool_weight)
-    gate_pre = project(gate_w)
-    rim = lax.ppermute(pool_in[ROWS - WINDOW :], ("z", "y", "c"), [(i, i + 1) for i in range(63)])
-    part_shape = jax.ShapeDtypeStruct((ROWS, 512), F32)
-    keep, part = pl.pallas_call(
-        pool_kernel,
-        out_shape=(part_shape, part_shape),
-        in_specs=[SMEM] + [VMEM] * 5,
-        out_specs=(VMEM, VMEM),
-        compiler_params=vmem(16),
-        name="pool",
-    )(place, pool_in, rim, gate_pre, pool_mix[0], pool_scale)
-
     *state, q = pl.pallas_call(
         first_kernel,
         out_shape=(*STATE, pltpu.VMEM((MAPS, 128, 2 * ROWS), BF16)),
@@ -335,6 +323,9 @@
     )(place, kv, kv_oth, q_own, q_oth)
     plan = tuple((i, ((0, dy),)) for i, dy in enumerate(columns[1:]))
     state = attend_chunk(place, q, state, plan, beside, "chunk0")
+    normed, state = lax.optimization_barrier((normed, state))
+    pool_in = dot(normed, pool_weight[:, 0]).astype(BF16)
+    rim = lax.ppermute(pool_in[ROWS - WINDOW :], ("z", "y", "c"), [(i, i + 1) for i in range(63)])
     for k in range(1, 5):
         plan = (
             (0, tuple((-k, dy) for dy in (columns if k < 4 else columns[:2]))),
@@ -342,6 +333,19 @@
         )
         state = attend_chunk(place, q, state, plan, (up[k], down[k]), f"chunk{k}")
         if k == 1:
+            normed, state = lax.optimization_barrier((normed, state))
+            gate_pre = dot(normed, gate_w).astype(BF16)
+        if k == 2:
+            gate_pre, state = lax.optimization_barrier((gate_pre, state))
+            part_shape = jax.ShapeDtypeStruct((ROWS, 512), F32)
+            keep, part = pl.pallas_call(
+                pool_kernel,
+                out_shape=(part_shape, part_shape),
+                in_specs=[SMEM] + [VMEM] * 5,
+                out_specs=(VMEM, VMEM),
+                compiler_params=vmem(16),
+                name="pool",
+            )(place, pool_in, rim, gate_pre, pool_mix[0], pool_scale)
             state, keep, part = lax.optimization_barrier((state, keep, part))
     other = lax.ppermute(state[1], "c", [(0, 1), (1, 0)])
     piece = jax.ShapeDtypeStruct((32, width), BF16)

time: 230 us -> 232 us (level)
  Pallas kernels: 163 us -> 100 us
  starting transfers between devices: 35.2 us -> 91.2 us
  waiting for transfers between devices: 14.4 us -> 22.2 us
    pallas_call x5, Pallas kernels: 156 us -> 93.7 us  [attend_chunk(): pl.pallas_call(functools.partial(chunk_kernel, plan, n), out_shape=STATE,...]
    ppermute x1, starting transfers between devices: 3.23 us -> 54.5 us  [local(): from_far_b = lax.ppermute(far_b, 'x', ring(4, -1))]
    ppermute x3, starting transfers between devices: 3.05 us -> 14.5 us  [local(): down.append(lax.ppermute(down[-1], 'z', ring(8, -1)))]
    ppermute x3, waiting for transfers between devices: 0.01 us -> 6.5 us  [local(): beside = [lax.ppermute(kv, 'y', ring(4, step)) for step in (1, -1, 2)]]
    ppermute x3, starting transfers between devices: 6.88 us -> 2.33 us  [local(): up.append(lax.ppermute(up[-1], 'z', ring(8, 1)))]
    ppermute x1, waiting for transfers between devices: 0.01 us -> 3.77 us  [local(): low_a = lax.ppermute(add(up_a, from_far_a), 'x', ring(4, 1))]
    unnamed x28 -> x32, local copies, waits for them, and re-layouts: 7.94 us -> 9.28 us
  transfers between devices with their start and end apart: 22 -> 22, of which waited for: 5 -> 8; matrix products, arithmetic and copies ran while one was open for 5% -> 5% of each run, Pallas kernels for 61% -> 34%
where the time goes in v4:
time: 232 us
  Pallas kernels  100 us (43%)
  starting transfers between devices  91.2 us (39%)
  waiting for transfers between devices  22.2 us (10%)
  local copies, waits for them, and re-layouts  12.1 us (5%)
  matrix products  2.75 us (1%)
    pallas_call x5, Pallas kernels, attend_chunk(): pl.pallas_call(functools.partial(chunk_kernel, plan, n), out_shape=STATE,...  93.7 us
    ppermute x1, starting transfers between devices, local(): from_far_b = lax.ppermute(far_b, 'x', ring(4, -1))  54.5 us
    ppermute x3, starting transfers between devices, local(): down.append(lax.ppermute(down[-1], 'z', ring(8, -1)))  14.5 us
    unnamed x32, local copies, waits for them, and re-layouts  9.28 us
    all_to_all x1, waiting for transfers between devices, local(): lax.all_to_all(jnp.broadcast_to(tokens[None], (4, *tokens.shape)), 'x', 0...  6.69 us
    ppermute x3, waiting for transfers between devices, local(): beside = [lax.ppermute(kv, 'y', ring(4, step)) for step in (1, -1, 2)]  6.5 us
  transfers between devices with their start and end apart: 22, of which 8 were waited for; matrix products, arithmetic and copies ran while one was open for 5% of the time, Pallas kernels for 34%

profile of v4, /device:TPU:248, one launch (start us, length us, event | category | flops | bytes accessed | tf_op | source)
XLA Modules:
  0.0 231.8 jit_solution(8253740943908208790)
XLA Ops:
  0.6 2.2 broadcast_in_dim.12
  2.8 4.3 %all-to-all-start = ((bf16[4,64,2048]{2,1,0:T(8,128)(2,1)}), bf16[4,64,2048]{2,1,0:T(8,128)(2,1)S(1)}, u32[]{:S(2)}, u32[]{:S(2)}) async-start(bf16[4,64,2048]{2,1,0:T(8,128)(2,1)} %broadcast_in_dim.12), calls=%async_computation | async-start | bytes 2097152 | tf_op jit(solution)/shard_map/all_to_all | solution.py:278
  7.1 5.5 %copy.15 = bf16[256,8,2,512]{3,1,2,0:T(8,128)(2,1)} copy(bf16[256,8,2,512]{3,2,1,0:T(2,128)(2,1)} %bitcast.31) | data formatting | bytes 8388608
  12.6 1.7 copy.19
  15.5 6.7 %all-to-all-done.rows_ref = bf16[4,64,2048]{2,1,0:T(8,128)(2,1)S(1)} async-done(((bf16[4,64,2048]{2,1,0:T(8,128)(2,1)}), bf16[4,64,2048]{2,1,0:T(8,128)(2,1)S(1)}, u32[]{:S(2)}, u32[]{:S(2)}) %all-to-all-start) | async-done | bytes 1048608 | tf_op jit(solution)/shard_map/all_to_all | solution.py:278
  26.2 1.8 collective-permute-start.3
  29.3 3.0 %collective-permute-done.2.b.refs_2_ = bf16[1,2,128,256]{3,2,1,0:T(8,128)(2,1)S(1)} collective-permute-done((bf16[1,2,128,256]{3,2,1,0:T(8,128)(2,1)S(1)}, bf16[1,2,128,256]{3,2,1,0:T(8,128)(2,1)S(1)}, u32[]{:S(2)}, u32[]{:S(2)}) %collective-permute-start.2) | collective-permute-done | bytes 131104 | tf_op jit(solution)/shard_map/ppermute | solution.py:291
  32.3 3.5 %collective-permute-done.3.c.refs_3_ = bf16[1,2,128,256]{3,2,1,0:T(8,128)(2,1)S(1)} collective-permute-done((bf16[1,2,128,256]{3,2,1,0:T(8,128)(2,1)S(1)}, bf16[1,2,128,256]{3,2,1,0:T(8,128)(2,1)S(1)}, u32[]{:S(2)}, u32[]{:S(2)}) %collective-permute-start.3) | collective-permute-done | bytes 131104 | tf_op jit(solution)/shard_map/ppermute | solution.py:291
  35.9 2.0 collective-permute-start.9
  38.0 3.1 %first.1 = (f32[8,152,256]{2,1,0:T(8,128)S(1)}, f32[8,152,256]{2,1,0:T(8,128)S(1)}, bf16[8,128,512]{2,1,0:T(8,128)(2,1)S(1)}) custom-call(s32[4]{0:T(128)S(1)} %pad_add_fusion.place_ref.refs_0_, bf16[1,2,128,256]{3,2,1,0:T(8,128)(2,1)S(1)} %get-tuple-element.46.kv_ref.a, bf16[1,2,128,256]{3,2,1,0:T(8,128)(2,1)S(1)} %collective-permute-done.oth_kv_ref, ...), custom_call_target="tpu_custom_call" | custom-call | tf_op jit(solution)/shard_map/first/pallas_call | solution.py:315
  41.0 16.4 %chunk0.1 = (f32[8,152,256]{2,1,0:T(8,128)S(1)}, f32[8,152,256]{2,1,0:T(8,128)S(1)}) custom-call(s32[4]{0:T(128)S(1)} %pad_add_fusion.place_ref.refs_0_, bf16[8,128,512]{2,1,0:T(8,128)(2,1)S(1)} %get-tuple-element.49.refs_1_, bf16[1,2,128,256]{3,2,1,0:T(8,128)(2,1)S(1)} %collective-permute-done.2.b.refs_2_, ...), custom_call_target="tpu_custom_call" | custom-call | flops 3221225472 | bytes 1048576 | tf_op jit(solution)/shard_map/chunk0/pallas_call | solution.py:208
  58.3 2.2 collective-permute-start.13
  61.7 2.2 collective-permute-start.6
  64.0 8.7 %chunk1.1 = (f32[8,152,256]{2,1,0:T(8,128)S(1)}, f32[8,152,256]{2,1,0:T(8,128)S(1)}) custom-call(s32[4]{0:T(128)S(1)} %pad_add_fusion.place_ref.refs_0_, bf16[8,128,512]{2,1,0:T(8,128)(2,1)S(1)} %get-tuple-element.49.refs_1_, bf16[4,2,128,256]{3,2,1,0:T(8,128)(2,1)S(1)} %collective-permute-done.5.refs_2_, ...), custom_call_target="tpu_custom_call" | custom-call | flops 8589934592 | bytes 1048576 | tf_op jit(solution)/shard_map/chunk1/pallas_call | solution.py:208
  74.0 11.2 %collective-permute-start.11 = (bf16[4,2,128,256]{3,2,1,0:T(8,128)(2,1)S(1)}, bf16[4,2,128,256]{3,2,1,0:T(8,128)(2,1)S(1)}, u32[]{:S(2)}, u32[]{:S(2)}) collective-permute-start(bf16[4,2,128,256]{3,2,1,0:T(8,128)(2,1)S(1)} %collective-permute-done.10.refs_3_), channel_id=1, source_target_pairs={{0,224},{32,0},{64,32},{96,64},{128,96},{160,128},{192,160},{224,1... | collective-permute-start | bytes 1572872 | tf_op jit(solution)/shard_map/ppermute | solution.py:304
  85.2 39.3 %chunk2.1 = (f32[8,152,256]{2,1,0:T(8,128)S(1)}, f32[8,152,256]{2,1,0:T(8,128)S(1)}) custom-call(s32[4]{0:T(128)S(1)} %pad_add_fusion.place_ref.refs_0_, bf16[8,128,512]{2,1,0:T(8,128)(2,1)S(1)} %get-tuple-element.49.refs_1_, bf16[4,2,128,256]{3,2,1,0:T(8,128)(2,1)S(1)} %collective-permute-done.6.refs_2_, ...), custom_call_target="tpu_custom_call" | custom-call | flops 8589934592 | bytes 1048576 | tf_op jit(solution)/shard_map/chunk2/pallas_call | solution.py:208
  125.8 3.3 %collective-permute-start.8 = (bf16[2,2,128,256]{3,2,1,0:T(8,128)(2,1)S(1)}, bf16[2,2,128,256]{3,2,1,0:T(8,128)(2,1)S(1)}, u32[]{:S(2)}, u32[]{:S(2)}) collective-permute-start(bf16[2,2,128,256]{3,2,1,0:T(8,128)(2,1)S(1)} %slice.20), channel_id=1, source_target_pairs={{0,32},{32,64},{64,96},{96,128},{128,160},{160,192},{192,224},{224... | collective-permute-start | bytes 786440 | tf_op jit(solution)/shard_map/ppermute | solution.py:305
  129.1 9.1 %chunk3.1 = (f32[8,152,256]{2,1,0:T(8,128)S(1)}, f32[8,152,256]{2,1,0:T(8,128)S(1)}) custom-call(s32[4]{0:T(128)S(1)} %pad_add_fusion.place_ref.refs_0_, bf16[8,128,512]{2,1,0:T(8,128)(2,1)S(1)} %get-tuple-element.49.refs_1_, bf16[4,2,128,256]{3,2,1,0:T(8,128)(2,1)S(1)} %collective-permute-done.7.refs_2_, ...), custom_call_target="tpu_custom_call" | custom-call | flops 8589934592 | bytes 1048576 | tf_op jit(solution)/shard_map/chunk3/pallas_call | solution.py:208
  138.3 20.1 %chunk4.1 = (f32[8,152,256]{2,1,0:T(8,128)S(1)}, f32[8,152,256]{2,1,0:T(8,128)S(1)}) custom-call(s32[4]{0:T(128)S(1)} %pad_add_fusion.place_ref.refs_0_, bf16[8,128,512]{2,1,0:T(8,128)(2,1)S(1)} %get-tuple-element.49.refs_1_, bf16[2,2,128,256]{3,2,1,0:T(8,128)(2,1)S(1)} %collective-permute-done.8.refs_2_, ...), custom_call_target="tpu_custom_call" | custom-call | flops 4294967296 | bytes 1048576 | tf_op jit(solution)/shard_map/chunk4/pallas_call | solution.py:208
  158.5 2.9 %collective-permute-done.14.b_ref = f32[8,152,256]{2,1,0:T(8,128)S(1)} collective-permute-done((f32[8,152,256]{2,1,0:T(8,128)S(1)}, f32[8,152,256]{2,1,0:T(8,128)S(1)}, u32[]{:S(2)}, u32[]{:S(2)}) %collective-permute-start.14) | collective-permute-done | bytes 1245216 | tf_op jit(solution)/shard_map/ppermute | solution.py:350
  163.1 54.5 %collective-permute-start.19 = (bf16[32,2048]{1,0:T(8,128)(2,1)S(1)}, bf16[32,2048]{1,0:T(8,128)(2,1)S(1)}, u32[]{:S(2)}, u32[]{:S(2)}) collective-permute-start(bf16[32,2048]{1,0:T(8,128)(2,1)S(1)} %get-tuple-element.84), channel_id=1, source_target_pairs={{0,3},{1,0},{2,1},{3,2},{4,7},{5,4},{6,5},{7,6},{8,11},{9,8},{10,9... | collective-permute-start | bytes 393224 | tf_op jit(solution)/shard_map/ppermute | solution.py:362
  217.7 3.2 %collective-permute-start.17 = (bf16[32,2048]{1,0:T(8,128)(2,1)S(1)}, bf16[32,2048]{1,0:T(8,128)(2,1)S(1)}, u32[]{:S(2)}, u32[]{:S(2)}) collective-permute-start(bf16[32,2048]{1,0:T(8,128)(2,1)S(1)} %get-tuple-element.81), channel_id=1, source_target_pairs={{0,3},{1,0},{2,1},{3,2},{4,7},{5,4},{6,5},{7,6},{8,11},{9,8},{10,9... | collective-permute-start | bytes 393224 | tf_op jit(solution)/shard_map/ppermute | solution.py:364
  221.4 3.2 %collective-permute-start.20 = (bf16[32,2048]{1,0:T(8,128)(2,1)S(1)}, bf16[32,2048]{1,0:T(8,128)(2,1)S(1)}, u32[]{:S(2)}, u32[]{:S(2)}) collective-permute-start(bf16[32,2048]{1,0:T(8,128)(2,1)S(1)} %add_convert_fusion.1), channel_id=1, source_target_pairs={{0,3},{1,0},{2,1},{3,2},{4,7},{5,4},{6,5},{7,6},{8,11},{9,8},{10,9... | collective-permute-start | bytes 393224 | tf_op jit(solution)/shard_map/ppermute | solution.py:370
  227.2 3.8 %collective-permute-done.16 = bf16[32,2048]{1,0:T(8,128)(2,1)S(1)} collective-permute-done((bf16[32,2048]{1,0:T(8,128)(2,1)S(1)}, bf16[32,2048]{1,0:T(8,128)(2,1)S(1)}, u32[]{:S(2)}, u32[]{:S(2)}) %collective-permute-start.16) | collective-permute-done | bytes 131104 | tf_op jit(solution)/shard_map/ppermute | solution.py:369
  (77 shorter events, 16.7 us)
Async XLA Ops:
  0.6 56.9 %copy-start = (bf16[2048,1,512]{2,0,1:T(8,128)(2,1)S(1)}, bf16[2048,1,512]{2,0,1:T(8,128)(2,1)}, u32[]{:S(2)}) copy-start(bf16[2048,1,512]{2,0,1:T(8,128)(2,1)} %param.19) | copy-start | bytes 6291460
  2.8 19.4 %all-to-all-start = ((bf16[4,64,2048]{2,1,0:T(8,128)(2,1)}), bf16[4,64,2048]{2,1,0:T(8,128)(2,1)S(1)}, u32[]{:S(2)}, u32[]{:S(2)}) async-start(bf16[4,64,2048]{2,1,0:T(8,128)(2,1)} %broadcast_in_dim.12), calls=%async_computation | async-start | bytes 2097152 | tf_op jit(solution)/shard_map/all_to_all | solution.py:278
  25.8 12.2 %collective-permute-start.1 = (bf16[512,256]{1,0:T(8,128)(2,1)S(1)}, bf16[512,256]{1,0:T(8,128)(2,1)S(1)}, u32[]{:S(2)}, u32[]{:S(2)}) collective-permute-start(bf16[512,256]{1,0:T(8,128)(2,1)S(1)} %fusion.2.q_own_ref), channel_id=1, source_target_pairs={{0,4},{4,0},{1,5},{5,1},{2,6},{6,2},{3,7},{7,3},{8,12},{12,8},{9,1... | collective-permute-start | bytes 786440 | tf_op jit(solution)/shard_map/ppermute | solution.py:312
  25.9 6.4 %collective-permute-start.2 = (bf16[1,2,128,256]{3,2,1,0:T(8,128)(2,1)S(1)}, bf16[1,2,128,256]{3,2,1,0:T(8,128)(2,1)S(1)}, u32[]{:S(2)}, u32[]{:S(2)}) collective-permute-start(bf16[1,2,128,256]{3,2,1,0:T(8,128)(2,1)S(1)} %get-tuple-element.46.kv_ref.a), channel_id=1, source_target_pairs={{0,8},{8,16},{16,24},{24,0},{1,9},{9,17},{17,25},{25,1},{2,10},{10... | collective-permute-start | bytes 393224 | tf_op jit(solution)/shard_map/ppermute | solution.py:291
  26.2 9.6 %collective-permute-start.3 = (bf16[1,2,128,256]{3,2,1,0:T(8,128)(2,1)S(1)}, bf16[1,2,128,256]{3,2,1,0:T(8,128)(2,1)S(1)}, u32[]{:S(2)}, u32[]{:S(2)}) collective-permute-start(bf16[1,2,128,256]{3,2,1,0:T(8,128)(2,1)S(1)} %get-tuple-element.46.kv_ref.a), channel_id=1, source_target_pairs={{0,24},{8,0},{16,8},{24,16},{1,25},{9,1},{17,9},{25,17},{2,26},{10... | collective-permute-start | bytes 393224 | tf_op jit(solution)/shard_map/ppermute | solution.py:291
  28.0 7.8 %collective-permute-start.4 = (bf16[1,2,128,256]{3,2,1,0:T(8,128)(2,1)S(1)}, bf16[1,2,128,256]{3,2,1,0:T(8,128)(2,1)S(1)}, u32[]{:S(2)}, u32[]{:S(2)}) collective-permute-start(bf16[1,2,128,256]{3,2,1,0:T(8,128)(2,1)S(1)} %get-tuple-element.46.kv_ref.a), channel_id=1, source_target_pairs={{0,16},{8,24},{16,0},{24,8},{1,17},{9,25},{17,1},{25,9},{2,18},{10... | collective-permute-start | bytes 393224 | tf_op jit(solution)/shard_map/ppermute | solution.py:291
  29.2 8.7 %collective-permute-start = (bf16[1,2,128,256]{3,2,1,0:T(8,128)(2,1)S(1)}, bf16[1,2,128,256]{3,2,1,0:T(8,128)(2,1)S(1)}, u32[]{:S(2)}, u32[]{:S(2)}) collective-permute-start(bf16[1,2,128,256]{3,2,1,0:T(8,128)(2,1)S(1)} %get-tuple-element.46.kv_ref.a), channel_id=1, source_target_pairs={{0,4},{4,0},{1,5},{5,1},{2,6},{6,2},{3,7},{7,3},{8,12},{12,8},{9,1... | collective-permute-start | bytes 393224 | tf_op jit(solution)/shard_map/ppermute | solution.py:313
  35.9 25.9 %collective-permute-start.5 = (bf16[4,2,128,256]{3,2,1,0:T(8,128)(2,1)S(1)}, bf16[4,2,128,256]{3,2,1,0:T(8,128)(2,1)S(1)}, u32[]{:S(2)}, u32[]{:S(2)}) collective-permute-start(bf16[4,2,128,256]{3,2,1,0:T(8,128)(2,1)S(1)} %join.1), channel_id=1, source_target_pairs={{0,32},{32,64},{64,96},{96,128},{128,160},{160,192},{192,224},{224... | collective-permute-start | bytes 1572872 | tf_op jit(solution)/shard_map/ppermute | solution.py:303
  35.9 24.5 %collective-permute-start.9 = (bf16[4,2,128,256]{3,2,1,0:T(8,128)(2,1)S(1)}, bf16[4,2,128,256]{3,2,1,0:T(8,128)(2,1)S(1)}, u32[]{:S(2)}, u32[]{:S(2)}) collective-permute-start(bf16[4,2,128,256]{3,2,1,0:T(8,128)(2,1)S(1)} %join.1), channel_id=1, source_target_pairs={{0,224},{32,0},{64,32},{96,64},{128,96},{160,128},{192,160},{224,1... | collective-permute-start | bytes 1572872 | tf_op jit(solution)/shard_map/ppermute | solution.py:304
  58.3 66.3 %collective-permute-start.13 = (bf16[16,512]{1,0:T(8,128)(2,1)S(1)}, bf16[16,512]{1,0:T(8,128)(2,1)S(1)}, u32[]{:S(2)}, u32[]{:S(2)}) collective-permute-start(bf16[16,512]{1,0:T(8,128)(2,1)S(1)} %slice.22), channel_id=1, source_target_pairs={{0,4},{4,8},{8,12},{12,16},{16,20},{20,24},{24,28},{28,32},{32,36}... | collective-permute-start | bytes 49160 | tf_op jit(solution)/shard_map/ppermute | solution.py:328
  60.5 13.6 %collective-permute-start.10 = (bf16[4,2,128,256]{3,2,1,0:T(8,128)(2,1)S(1)}, bf16[4,2,128,256]{3,2,1,0:T(8,128)(2,1)S(1)}, u32[]{:S(2)}, u32[]{:S(2)}) collective-permute-start(bf16[4,2,128,256]{3,2,1,0:T(8,128)(2,1)S(1)} %collective-permute-done.9.refs_3_), channel_id=1, source_target_pairs={{0,224},{32,0},{64,32},{96,64},{128,96},{160,128},{192,160},{224,1... | collective-permute-start | bytes 1572872 | tf_op jit(solution)/shard_map/ppermute | solution.py:304
  61.7 23.5 %collective-permute-start.6 = (bf16[4,2,128,256]{3,2,1,0:T(8,128)(2,1)S(1)}, bf16[4,2,128,256]{3,2,1,0:T(8,128)(2,1)S(1)}, u32[]{:S(2)}, u32[]{:S(2)}) collective-permute-start(bf16[4,2,128,256]{3,2,1,0:T(8,128)(2,1)S(1)} %collective-permute-done.5.refs_2_), channel_id=1, source_target_pairs={{0,32},{32,64},{64,96},{96,128},{128,160},{160,192},{192,224},{224... | collective-permute-start | bytes 1572872 | tf_op jit(solution)/shard_map/ppermute | solution.py:303
  74.0 50.6 %copy-start.3 = (bf16[1,512,512]{2,1,0:T(8,128)(2,1)S(1)}, bf16[1,512,512]{2,1,0:T(8,128)(2,1)}, u32[]{:S(2)}) copy-start(bf16[1,512,512]{2,1,0:T(8,128)(2,1)} %param.20) | copy-start | bytes 1572868
  74.0 51.6 %collective-permute-start.11 = (bf16[4,2,128,256]{3,2,1,0:T(8,128)(2,1)S(1)}, bf16[4,2,128,256]{3,2,1,0:T(8,128)(2,1)S(1)}, u32[]{:S(2)}, u32[]{:S(2)}) collective-permute-start(bf16[4,2,128,256]{3,2,1,0:T(8,128)(2,1)S(1)} %collective-permute-done.10.refs_3_), channel_id=1, source_target_pairs={{0,224},{32,0},{64,32},{96,64},{128,96},{160,128},{192,160},{224,1... | collective-permute-start | bytes 1572872 | tf_op jit(solution)/shard_map/ppermute | solution.py:304
  85.2 40.6 %collective-permute-start.7 = (bf16[4,2,128,256]{3,2,1,0:T(8,128)(2,1)S(1)}, bf16[4,2,128,256]{3,2,1,0:T(8,128)(2,1)S(1)}, u32[]{:S(2)}, u32[]{:S(2)}) collective-permute-start(bf16[4,2,128,256]{3,2,1,0:T(8,128)(2,1)S(1)} %collective-permute-done.6.refs_2_), channel_id=1, source_target_pairs={{0,32},{32,64},{64,96},{96,128},{128,160},{160,192},{192,224},{224... | collective-permute-start | bytes 1572872 | tf_op jit(solution)/shard_map/ppermute | solution.py:303
  125.7 12.5 %collective-permute-start.12 = (bf16[2,2,128,256]{3,2,1,0:T(8,128)(2,1)S(1)}, bf16[2,2,128,256]{3,2,1,0:T(8,128)(2,1)S(1)}, u32[]{:S(2)}, u32[]{:S(2)}) collective-permute-start(bf16[2,2,128,256]{3,2,1,0:T(8,128)(2,1)S(1)} %slice.21), channel_id=1, source_target_pairs={{0,224},{32,0},{64,32},{96,64},{128,96},{160,128},{192,160},{224,1... | collective-permute-start | bytes 786440 | tf_op jit(solution)/shard_map/ppermute | solution.py:306
  125.8 12.4 %collective-permute-start.8 = (bf16[2,2,128,256]{3,2,1,0:T(8,128)(2,1)S(1)}, bf16[2,2,128,256]{3,2,1,0:T(8,128)(2,1)S(1)}, u32[]{:S(2)}, u32[]{:S(2)}) collective-permute-start(bf16[2,2,128,256]{3,2,1,0:T(8,128)(2,1)S(1)} %slice.20), channel_id=1, source_target_pairs={{0,32},{32,64},{64,96},{96,128},{128,160},{160,192},{192,224},{224... | collective-permute-start | bytes 786440 | tf_op jit(solution)/shard_map/ppermute | solution.py:305
  158.4 3.0 %collective-permute-start.14 = (f32[8,152,256]{2,1,0:T(8,128)S(1)}, f32[8,152,256]{2,1,0:T(8,128)S(1)}, u32[]{:S(2)}, u32[]{:S(2)}) collective-permute-start(f32[8,152,256]{2,1,0:T(8,128)S(1)} %get-tuple-element.75), channel_id=1, source_target_pairs={{0,4},{4,0},{1,5},{5,1},{2,6},{6,2},{3,7},{7,3},{8,12},{12,8},{9,1... | collective-permute-start | bytes 3735560 | tf_op jit(solution)/shard_map/ppermute | solution.py:350
  163.1 58.3 %collective-permute-start.19 = (bf16[32,2048]{1,0:T(8,128)(2,1)S(1)}, bf16[32,2048]{1,0:T(8,128)(2,1)S(1)}, u32[]{:S(2)}, u32[]{:S(2)}) collective-permute-start(bf16[32,2048]{1,0:T(8,128)(2,1)S(1)} %get-tuple-element.84), channel_id=1, source_target_pairs={{0,3},{1,0},{2,1},{3,2},{4,7},{5,4},{6,5},{7,6},{8,11},{9,8},{10,9... | collective-permute-start | bytes 393224 | tf_op jit(solution)/shard_map/ppermute | solution.py:362
  217.7 7.0 %collective-permute-start.15 = (bf16[32,2048]{1,0:T(8,128)(2,1)S(1)}, bf16[32,2048]{1,0:T(8,128)(2,1)S(1)}, u32[]{:S(2)}, u32[]{:S(2)}) collective-permute-start(bf16[32,2048]{1,0:T(8,128)(2,1)S(1)} %get-tuple-element.80), channel_id=1, source_target_pairs={{0,1},{1,2},{2,3},{3,0},{4,5},{5,6},{6,7},{7,4},{8,9},{9,10},{10,1... | collective-permute-start | bytes 393224 | tf_op jit(solution)/shard_map/ppermute | solution.py:361
  217.7 7.7 %collective-permute-start.17 = (bf16[32,2048]{1,0:T(8,128)(2,1)S(1)}, bf16[32,2048]{1,0:T(8,128)(2,1)S(1)}, u32[]{:S(2)}, u32[]{:S(2)}) collective-permute-start(bf16[32,2048]{1,0:T(8,128)(2,1)S(1)} %get-tuple-element.81), channel_id=1, source_target_pairs={{0,3},{1,0},{2,1},{3,2},{4,7},{5,4},{6,5},{7,6},{8,11},{9,8},{10,9... | collective-permute-start | bytes 393224 | tf_op jit(solution)/shard_map/ppermute | solution.py:364
  220.9 6.2 %collective-permute-start.18 = (bf16[32,2048]{1,0:T(8,128)(2,1)S(1)}, bf16[32,2048]{1,0:T(8,128)(2,1)S(1)}, u32[]{:S(2)}, u32[]{:S(2)}) collective-permute-start(bf16[32,2048]{1,0:T(8,128)(2,1)S(1)} %get-tuple-element.82), channel_id=1, source_target_pairs={{0,1},{1,2},{2,3},{3,0},{4,5},{5,6},{6,7},{7,4},{8,9},{9,10},{10,1... | collective-permute-start | bytes 393224 | tf_op jit(solution)/shard_map/ppermute | solution.py:363
  221.4 5.7 %collective-permute-start.20 = (bf16[32,2048]{1,0:T(8,128)(2,1)S(1)}, bf16[32,2048]{1,0:T(8,128)(2,1)S(1)}, u32[]{:S(2)}, u32[]{:S(2)}) collective-permute-start(bf16[32,2048]{1,0:T(8,128)(2,1)S(1)} %add_convert_fusion.1), channel_id=1, source_target_pairs={{0,3},{1,0},{2,1},{3,2},{4,7},{5,4},{6,5},{7,6},{8,11},{9,8},{10,9... | collective-permute-start | bytes 393224 | tf_op jit(solution)/shard_map/ppermute | solution.py:370
  224.7 6.3 %collective-permute-start.16 = (bf16[32,2048]{1,0:T(8,128)(2,1)S(1)}, bf16[32,2048]{1,0:T(8,128)(2,1)S(1)}, u32[]{:S(2)}, u32[]{:S(2)}) collective-permute-start(bf16[32,2048]{1,0:T(8,128)(2,1)S(1)} %add_convert_fusion.3), channel_id=1, source_target_pairs={{0,1},{1,2},{2,3},{3,0},{4,5},{5,6},{6,7},{7,4},{8,9},{9,10},{10,1... | collective-permute-start | bytes 393224 | tf_op jit(solution)/shard_map/ppermute | solution.py:369
  (13 other events, 174.5 us)

commit v5 on v4

--- a/solution.py
+++ b/solution.py
@@ -85,11 +85,22 @@
         out_ref[i] = ref[0]
 
 
-def front_kernel(rows_ref, gain_ref, w_ref, normed_ref, kv_ref):
-    for j in range(4):
-        values = rows_ref[j].astype(F32)
+def front_kernel(place_ref, p0, p1a, p1b, p2a, p2b, p3a, p3b, gain_ref, w_ref, normed_ref, kv_ref):
+    x = place_ref[3]
+
+    def put(piece_ref, back, half, rows):
+        values = piece_ref[...].astype(F32)
         scale = lax.rsqrt(jnp.mean(values * values, axis=1, keepdims=True) + NORM_EPS)
-        normed_ref[j * 64 : j * 64 + 64] = (values * scale * gain_ref[...]).astype(BF16)
+        at = pl.multiple_of(((x - back) & 3) * 64 + half * 32, 32)
+        normed_ref[pl.ds(at, rows), :] = (values * scale * gain_ref[...]).astype(BF16)
+
+    put(p0, 0, 0, 64)
+    put(p1a, 1, 0, 32)
+    put(p1b, 1, 1, 32)
+    put(p3a, 3, 0, 32)
+    put(p3b, 3, 1, 32)
+    put(p2a, 2, 0, 32)
+    put(p2b, 2, 1, 32)
     both = dot(normed_ref[...], w_ref[...])
     values_t = both[:, HALF:].T.astype(BF16)
     for half in range(2):
@@ -98,7 +109,7 @@
         kv_ref[0, half, :, HALF:] = values_t[:, rows]
 
 
-def chunk_kernel(plan, n_in, *refs):
+def chunk_kernel(plan, n_in, rolled, *refs):
     place_ref, q_ref = refs[0], refs[1]
     ins = refs[2 : 2 + n_in]
     own_in, oth_in, own_ref, oth_ref, keys_ref, values_ref, p_a, p_b, over_ref, list_ref = refs[2 + n_in :]
@@ -152,19 +163,31 @@
 
             keys, values = keys_ref[...], values_ref[...]
 
-            def scores(i):
+            def scores(i, slot):
                 top = jnp.concatenate([own_in[i, 144:145], oth_in[i, 144:145]], axis=1)
                 s = dot(keys, q_ref[i]) - top
                 over_ref[i] = jnp.maximum(over_ref[i], jnp.max(s.reshape(-1, 8, 2 * ROWS), axis=0))
-                probs[i % 2][...] = jnp.exp2(s).astype(BF16)
-
-            scores(0)
+                probs[slot][...] = jnp.exp2(s).astype(BF16)
+
+            def sums(i, slot):
+                out = dot(values, probs[slot][...])
+                own_ref[i, 0:144] = jnp.where(t == 0, own_in[i, 0:144], own_ref[i, 0:144]) + out[:, :ROWS]
+                oth_ref[i, 0:144] = jnp.where(t == 0, oth_in[i, 0:144], oth_ref[i, 0:144]) + out[:, ROWS:]
+
+            def two_maps(h, carry):
+                scores(2 * h, 0)
+                scores(2 * h + 1, 1)
+                sums(2 * h, 0)
+                sums(2 * h + 1, 1)
+                return carry
+
+            if rolled:
+                return lax.fori_loop(0, MAPS // 2, two_maps, carry)
+            scores(0, 0)
             for i in range(MAPS):
                 if i + 1 < MAPS:
-                    scores(i + 1)
-                out = dot(values, probs[i % 2][...])
-                own_ref[i, 0:144] = jnp.where(t == 0, own_in[i, 0:144], own_ref[i, 0:144]) + out[:, :ROWS]
-                oth_ref[i, 0:144] = jnp.where(t == 0, oth_in[i, 0:144], oth_ref[i, 0:144]) + out[:, ROWS:]
+                    scores(i + 1, (i + 1) % 2)
+                sums(i, i % 2)
             return carry
 
         lax.fori_loop(0, (visible + 1) // 2, two_blocks, 0)
@@ -202,11 +225,11 @@
     return pltpu.with_memory_space_constraint(array, pltpu.VMEM)
 
 
-def attend_chunk(place, q, state, plan, arrays, name):
+def attend_chunk(place, q, state, plan, arrays, name, rolled=False):
     n = len(arrays)
     blocks = sum(len(offsets) for _, offsets in plan)
     return pl.pallas_call(
-        functools.partial(chunk_kernel, plan, n),
+        functools.partial(chunk_kernel, plan, n, rolled),
         out_shape=STATE,
         in_specs=[SMEM, VMEM] + [VMEM] * n + [VMEM, VMEM],
         out_specs=(VMEM, VMEM),
@@ -275,18 +298,23 @@
     width = tokens.shape[1]
     z, y, c = lax.axis_index("z"), lax.axis_index("y"), lax.axis_index("c")
     place = jnp.stack([z, y, c, lax.axis_index("x")])
-    pieces = lax.all_to_all(jnp.broadcast_to(tokens[None], (4, *tokens.shape)), "x", 0, 0, tiled=True)
-    gate_w, query_w = gate_weight.reshape(width, -1), query_weight.reshape(width, -1)
+    halves = tokens[:32], tokens[32:]
+    up_a = lax.ppermute(halves[0], "x", ring(4, 1))
+    down_b = lax.ppermute(halves[1], "x", ring(4, -1))
+    up_b = lax.ppermute(halves[1], "x", ring(4, 1))
+    down_a = lax.ppermute(halves[0], "x", ring(4, -1))
+    far_a = lax.ppermute(up_a, "x", ring(4, 1))
+    far_b = lax.ppermute(down_b, "x", ring(4, -1))
     kv_w = jnp.concatenate([key_weight[:, 0], value_weight[:, 0]], axis=1)
-    pieces, gate_w, query_w, kv_w = lax.optimization_barrier((pieces, gate_w, query_w, kv_w))
     normed, kv = pl.pallas_call(
         front_kernel,
         out_shape=(jax.ShapeDtypeStruct((ROWS, width), BF16), jax.ShapeDtypeStruct((1, 2, HALF, 2 * HALF), BF16)),
-        in_specs=[VMEM] * 3,
+        in_specs=[SMEM] + [VMEM] * 9,
         out_specs=(VMEM, VMEM),
         compiler_params=vmem(16),
         name="front",
-    )(pieces, norm_gain[None], kv_w)
+    )(place, tokens, up_a, up_b, far_a, far_b, down_a, down_b, norm_gain[None], kv_w)
+    kv_oth = lax.ppermute(kv, "c", [(0, 1), (1, 0)])
 
     beside = [lax.ppermute(kv, "y", ring(4, step)) for step in (1, -1, 2)]
     group = pl.pallas_call(
@@ -305,12 +333,13 @@
     up.append(lax.ppermute(up[3][:2], "z", ring(8, 1)))
     down.append(lax.ppermute(down[3][2:], "z", ring(8, -1)))
 
+    normed, query_weight, kv_oth = lax.optimization_barrier((normed, query_weight, kv_oth))
+    query_w = query_weight.reshape(width, -1)
     scale = (query_weight.shape[2] // 2) ** -0.5 * LOG2E
     q_own = (
         lax.dot_general(query_w, normed, (((0,), (1,)), ((), ())), preferred_element_type=F32) * scale
     ).astype(BF16)
     q_oth = lax.ppermute(q_own, "c", [(0, 1), (1, 0)])
-    kv_oth = lax.ppermute(kv, "c", [(0, 1), (1, 0)])
 
     *state, q = pl.pallas_call(
         first_kernel,
@@ -322,8 +351,9 @@
         name="first",
     )(place, kv, kv_oth, q_own, q_oth)
     plan = tuple((i, ((0, dy),)) for i, dy in enumerate(columns[1:]))
-    state = attend_chunk(place, q, state, plan, beside, "chunk0")
-    normed, state = lax.optimization_barrier((normed, state))
+    state = attend_chunk(place, q, state, plan, beside, "chunk0", rolled=True)
+    normed, gate_weight, state = lax.optimization_barrier((normed, gate_weight, state))
+    gate_w = gate_weight.reshape(width, -1)
     pool_in = dot(normed, pool_weight[:, 0]).astype(BF16)
     rim = lax.ppermute(pool_in[ROWS - WINDOW :], ("z", "y", "c"), [(i, i + 1) for i in range(63)])
     for k in range(1, 5):
@@ -331,7 +361,7 @@
             (0, tuple((-k, dy) for dy in (columns if k < 4 else columns[:2]))),
             (1, tuple((k, dy) for dy in (columns if k < 4 else columns[2:]))),
         )
-        state = attend_chunk(place, q, state, plan, (up[k], down[k]), f"chunk{k}")
+        state = attend_chunk(place, q, state, plan, (up[k], down[k]), f"chunk{k}", rolled=k == 4)
         if k == 1:
             normed, state = lax.optimization_barrier((normed, state))
             gate_pre = dot(normed, gate_w).astype(BF16)

time: 232 us -> 227 us (0.978)
  Pallas kernels: 100 us -> 165 us
  starting transfers between devices: 91.2 us -> 30.4 us
  local copies, waits for them, and re-layouts: 12.1 us -> 3.73 us
    pallas_call x5, Pallas kernels: 93.7 us -> 157 us  [attend_chunk(): pl.pallas_call(functools.partial(chunk_kernel, plan, n, rolled), out_shap...]
    ppermute x1, starting transfers between devices: 54.5 us -> 0.08 us  [local(): from_far_b = lax.ppermute(far_b, 'x', ring(4, -1))]
    ppermute x3, starting transfers between devices: 14.5 us -> 4.74 us  [local(): down.append(lax.ppermute(down[-1], 'z', ring(8, -1)))]
    ppermute x0 -> x6, starting transfers between devices: none -> 9.66 us  [the longest x1 2.96 us: local(): down_a = lax.ppermute(halves[0], 'x', ring(4, -1))]
    unnamed x32 -> x21, local copies, waits for them, and re-layouts: 9.28 us -> 1.25 us
    all_to_all x1 -> x0, waiting for transfers between devices: 6.69 us -> none  [local(): lax.all_to_all(jnp.broadcast_to(tokens[None], (4, *tokens.shape)), 'x', 0...]
    all_to_all x1 -> x0, starting transfers between devices: 4.29 us -> none  [local(): lax.all_to_all(jnp.broadcast_to(tokens[None], (4, *tokens.shape)), 'x', 0...]
    ppermute x1, starting transfers between devices: 3.29 us -> 0.3 us  [local(): up.append(lax.ppermute(up[3][:2], 'z', ring(8, 1)))]
  transfers between devices with their start and end apart: 22 -> 27, of which waited for: 8 -> 12; matrix products, arithmetic and copies ran while one was open for 5% -> 2% of each run, Pallas kernels for 34% -> 62%
where the time goes in v5:
time: 227 us; the launch traced here: 225 us
  Pallas kernels  165 us (73%)
  starting transfers between devices  30.4 us (13%)
  waiting for transfers between devices  20.1 us (9%)
  local copies, waits for them, and re-layouts  3.73 us (2%)
  matrix products  2.82 us (1%)
  other arithmetic  2.28 us (1%)
    pallas_call x5, Pallas kernels, attend_chunk(): pl.pallas_call(functools.partial(chunk_kernel, plan, n, rolled), out_shap...  157 us
    ppermute x3, waiting for transfers between devices, local(): beside = [lax.ppermute(kv, 'y', ring(4, step)) for step in (1, -1, 2)]  6.84 us
    ppermute x3, starting transfers between devices, local(): down.append(lax.ppermute(down[-1], 'z', ring(8, -1)))  4.74 us
  transfers between devices with their start and end apart: 27, of which 12 were waited for; matrix products, arithmetic and copies ran while one was open for 2% of the time, Pallas kernels for 62%

profile of v5, /device:TPU:248, one launch (start us, length us, event | category | flops | bytes accessed | tf_op | source)
XLA Modules:
  0.0 225.1 jit_solution(8537623057322541086)
XLA Ops:
  0.7 1.8 fusion.14
  4.0 1.7 collective-permute-start.3
  6.0 3.0 %collective-permute-start.5 = (bf16[32,2048]{1,0:T(8,128)(2,1)}, bf16[32,2048]{1,0:T(8,128)(2,1)}, u32[]{:S(2)}, u32[]{:S(2)}) collective-permute-start(bf16[32,2048]{1,0:T(8,128)(2,1)} %get-tuple-element.89), channel_id=1, source_target_pairs={{0,3},{1,0},{2,1},{3,2},{4,7},{5,4},{6,5},{7,6},{8,11},{9,8},{10,9... | collective-permute-start | bytes 393224 | tf_op jit(solution)/shard_map/ppermute | solution.py:305
  10.6 1.9 collective-permute-start.4
  15.9 2.1 front.1
  21.7 2.2 collective-permute-start.8
  23.9 4.5 %collective-permute-done.10.d.refs_4_ = bf16[1,2,128,256]{3,2,1,0:T(8,128)(2,1)S(1)} collective-permute-done((bf16[1,2,128,256]{3,2,1,0:T(8,128)(2,1)S(1)}, bf16[1,2,128,256]{3,2,1,0:T(8,128)(2,1)S(1)}, u32[]{:S(2)}, u32[]{:S(2)}) %collective-permute-start.10) | collective-permute-done | bytes 131104 | tf_op jit(solution)/shard_map/ppermute | solution.py:319
  28.4 2.4 %collective-permute-done.9.c.refs_3_ = bf16[1,2,128,256]{3,2,1,0:T(8,128)(2,1)S(1)} collective-permute-done((bf16[1,2,128,256]{3,2,1,0:T(8,128)(2,1)S(1)}, bf16[1,2,128,256]{3,2,1,0:T(8,128)(2,1)S(1)}, u32[]{:S(2)}, u32[]{:S(2)}) %collective-permute-start.9) | collective-permute-done | bytes 131104 | tf_op jit(solution)/shard_map/ppermute | solution.py:319
  30.9 2.0 collective-permute-start.15
  32.9 3.1 %first.1 = (f32[8,152,256]{2,1,0:T(8,128)S(1)}, f32[8,152,256]{2,1,0:T(8,128)S(1)}, bf16[8,128,512]{2,1,0:T(8,128)(2,1)S(1)}) custom-call(s32[4]{0:T(128)S(1)} %pad_add_fusion.place_ref.refs_0_, bf16[1,2,128,256]{3,2,1,0:T(8,128)(2,1)S(1)} %get-tuple-element.44.kv_ref.a, bf16[1,2,128,256]{3,2,1,0:T(8,128)(2,1)S(1)} %collective-permute-done.6.oth_kv_ref, ...), custom_call_target="tpu_custom_call" | custom-call | tf_op jit(solution)/shard_map/first/pallas_call | solution.py:344
  36.0 17.5 %chunk0.1 = (f32[8,152,256]{2,1,0:T(8,128)S(1)}, f32[8,152,256]{2,1,0:T(8,128)S(1)}) custom-call(s32[4]{0:T(128)S(1)} %pad_add_fusion.place_ref.refs_0_, bf16[8,128,512]{2,1,0:T(8,128)(2,1)S(1)} %get-tuple-element.49.refs_1_, bf16[1,2,128,256]{3,2,1,0:T(8,128)(2,1)S(1)} %collective-permute-done.8.b.refs_2_, ...), custom_call_target="tpu_custom_call" | custom-call | flops 3221225472 | bytes 1048576 | tf_op jit(solution)/shard_map/chunk0/pallas_call | solution.py:231
  55.5 1.9 collective-permute-start.19
  59.5 39.4 %chunk1.1 = (f32[8,152,256]{2,1,0:T(8,128)S(1)}, f32[8,152,256]{2,1,0:T(8,128)S(1)}) custom-call(s32[4]{0:T(128)S(1)} %pad_add_fusion.place_ref.refs_0_, bf16[8,128,512]{2,1,0:T(8,128)(2,1)S(1)} %get-tuple-element.49.refs_1_, bf16[4,2,128,256]{3,2,1,0:T(8,128)(2,1)S(1)} %collective-permute-done.11.refs_2_, ...), custom_call_target="tpu_custom_call" | custom-call | flops 8589934592 | bytes 1048576 | tf_op jit(solution)/shard_map/chunk1/pallas_call | solution.py:231
  100.3 2.0 collective-permute-start.17
  102.3 39.3 %chunk2.1 = (f32[8,152,256]{2,1,0:T(8,128)S(1)}, f32[8,152,256]{2,1,0:T(8,128)S(1)}) custom-call(s32[4]{0:T(128)S(1)} %pad_add_fusion.place_ref.refs_0_, bf16[8,128,512]{2,1,0:T(8,128)(2,1)S(1)} %get-tuple-element.49.refs_1_, bf16[4,2,128,256]{3,2,1,0:T(8,128)(2,1)S(1)} %collective-permute-done.12.refs_2_, ...), custom_call_target="tpu_custom_call" | custom-call | flops 8589934592 | bytes 1048576 | tf_op jit(solution)/shard_map/chunk2/pallas_call | solution.py:231
  143.2 2.1 collective-permute-start.18
  145.2 39.5 %chunk3.1 = (f32[8,152,256]{2,1,0:T(8,128)S(1)}, f32[8,152,256]{2,1,0:T(8,128)S(1)}) custom-call(s32[4]{0:T(128)S(1)} %pad_add_fusion.place_ref.refs_0_, bf16[8,128,512]{2,1,0:T(8,128)(2,1)S(1)} %get-tuple-element.49.refs_1_, bf16[4,2,128,256]{3,2,1,0:T(8,128)(2,1)S(1)} %collective-permute-done.13.refs_2_, ...), custom_call_target="tpu_custom_call" | custom-call | flops 8589934592 | bytes 1048576 | tf_op jit(solution)/shard_map/chunk3/pallas_call | solution.py:231
  184.7 21.1 %chunk4.1 = (f32[8,152,256]{2,1,0:T(8,128)S(1)}, f32[8,152,256]{2,1,0:T(8,128)S(1)}) custom-call(s32[4]{0:T(128)S(1)} %pad_add_fusion.place_ref.refs_0_, bf16[8,128,512]{2,1,0:T(8,128)(2,1)S(1)} %get-tuple-element.49.refs_1_, bf16[2,2,128,256]{3,2,1,0:T(8,128)(2,1)S(1)} %collective-permute-done.14.refs_2_, ...), custom_call_target="tpu_custom_call" | custom-call | flops 4294967296 | bytes 1048576 | tf_op jit(solution)/shard_map/chunk4/pallas_call | solution.py:231
  206.0 2.9 %collective-permute-done.20.b_ref = f32[8,152,256]{2,1,0:T(8,128)S(1)} collective-permute-done((f32[8,152,256]{2,1,0:T(8,128)S(1)}, f32[8,152,256]{2,1,0:T(8,128)S(1)}, u32[]{:S(2)}, u32[]{:S(2)}) %collective-permute-start.20) | collective-permute-done | bytes 1245216 | tf_op jit(solution)/shard_map/ppermute | solution.py:380
  208.9 1.7 finish.1
  210.7 2.0 collective-permute-start.21
  214.7 2.3 %collective-permute-done.25 = bf16[32,2048]{1,0:T(8,128)(2,1)S(1)} collective-permute-done((bf16[32,2048]{1,0:T(8,128)(2,1)S(1)}, bf16[32,2048]{1,0:T(8,128)(2,1)S(1)}, u32[]{:S(2)}, u32[]{:S(2)}) %collective-permute-start.25) | collective-permute-done | bytes 131104 | tf_op jit(solution)/shard_map/ppermute | solution.py:392
  220.3 1.8 collective-permute-done.26
  222.1 2.1 collective-permute-done.22
  (76 shorter events, 23.8 us)
Async XLA Ops:
  2.5 6.8 %collective-permute-start = (bf16[32,2048]{1,0:T(8,128)(2,1)}, bf16[32,2048]{1,0:T(8,128)(2,1)S(1)}, u32[]{:S(2)}, u32[]{:S(2)}) collective-permute-start(bf16[32,2048]{1,0:T(8,128)(2,1)} %get-tuple-element.89), channel_id=1, source_target_pairs={{0,1},{1,2},{2,3},{3,0},{4,5},{5,6},{6,7},{7,4},{8,9},{9,10},{10,1... | collective-permute-start | bytes 393224 | tf_op jit(solution)/shard_map/ppermute | solution.py:302
  4.0 6.6 %collective-permute-start.3 = (bf16[32,2048]{1,0:T(8,128)(2,1)}, bf16[32,2048]{1,0:T(8,128)(2,1)}, u32[]{:S(2)}, u32[]{:S(2)}) collective-permute-start(bf16[32,2048]{1,0:T(8,128)(2,1)} %get-tuple-element.88), channel_id=1, source_target_pairs={{0,3},{1,0},{2,1},{3,2},{4,7},{5,4},{6,5},{7,6},{8,11},{9,8},{10,9... | collective-permute-start | bytes 393224 | tf_op jit(solution)/shard_map/ppermute | solution.py:303
  5.7 8.2 %collective-permute-start.1 = (bf16[32,2048]{1,0:T(8,128)(2,1)}, bf16[32,2048]{1,0:T(8,128)(2,1)}, u32[]{:S(2)}, u32[]{:S(2)}) collective-permute-start(bf16[32,2048]{1,0:T(8,128)(2,1)} %get-tuple-element.88), channel_id=1, source_target_pairs={{0,1},{1,2},{2,3},{3,0},{4,5},{5,6},{6,7},{7,4},{8,9},{9,10},{10,1... | collective-permute-start | bytes 393224 | tf_op jit(solution)/shard_map/ppermute | solution.py:304
  6.0 7.9 %collective-permute-start.5 = (bf16[32,2048]{1,0:T(8,128)(2,1)}, bf16[32,2048]{1,0:T(8,128)(2,1)}, u32[]{:S(2)}, u32[]{:S(2)}) collective-permute-start(bf16[32,2048]{1,0:T(8,128)(2,1)} %get-tuple-element.89), channel_id=1, source_target_pairs={{0,3},{1,0},{2,1},{3,2},{4,7},{5,4},{6,5},{7,6},{8,11},{9,8},{10,9... | collective-permute-start | bytes 393224 | tf_op jit(solution)/shard_map/ppermute | solution.py:305
  9.3 6.3 %collective-permute-start.2 = (bf16[32,2048]{1,0:T(8,128)(2,1)S(1)}, bf16[32,2048]{1,0:T(8,128)(2,1)}, u32[]{:S(2)}, u32[]{:S(2)}) collective-permute-start(bf16[32,2048]{1,0:T(8,128)(2,1)S(1)} %collective-permute-done.p1a), channel_id=1, source_target_pairs={{0,1},{1,2},{2,3},{3,0},{4,5},{5,6},{6,7},{7,4},{8,9},{9,10},{10,1... | collective-permute-start | bytes 393224 | tf_op jit(solution)/shard_map/ppermute | solution.py:306
  10.6 5.3 %collective-permute-start.4 = (bf16[32,2048]{1,0:T(8,128)(2,1)}, bf16[32,2048]{1,0:T(8,128)(2,1)}, u32[]{:S(2)}, u32[]{:S(2)}) collective-permute-start(bf16[32,2048]{1,0:T(8,128)(2,1)} %collective-permute-done.3.p3b), channel_id=1, source_target_pairs={{0,3},{1,0},{2,1},{3,2},{4,7},{5,4},{6,5},{7,6},{8,11},{9,8},{10,9... | collective-permute-start | bytes 393224 | tf_op jit(solution)/shard_map/ppermute | solution.py:307
  20.2 12.6 %collective-permute-start.7 = (bf16[512,256]{1,0:T(8,128)(2,1)S(1)}, bf16[512,256]{1,0:T(8,128)(2,1)S(1)}, u32[]{:S(2)}, u32[]{:S(2)}) collective-permute-start(bf16[512,256]{1,0:T(8,128)(2,1)S(1)} %fusion.8.q_own_ref), channel_id=1, source_target_pairs={{0,4},{4,0},{1,5},{5,1},{2,6},{6,2},{3,7},{7,3},{8,12},{12,8},{9,1... | collective-permute-start | bytes 786440 | tf_op jit(solution)/shard_map/ppermute | solution.py:342
  20.5 7.9 %collective-permute-start.10 = (bf16[1,2,128,256]{3,2,1,0:T(8,128)(2,1)S(1)}, bf16[1,2,128,256]{3,2,1,0:T(8,128)(2,1)S(1)}, u32[]{:S(2)}, u32[]{:S(2)}) collective-permute-start(bf16[1,2,128,256]{3,2,1,0:T(8,128)(2,1)S(1)} %get-tuple-element.44.kv_ref.a), channel_id=1, source_target_pairs={{0,16},{8,24},{16,0},{24,8},{1,17},{9,25},{17,1},{25,9},{2,18},{10... | collective-permute-start | bytes 393224 | tf_op jit(solution)/shard_map/ppermute | solution.py:319
  21.7 6.6 %collective-permute-start.8 = (bf16[1,2,128,256]{3,2,1,0:T(8,128)(2,1)S(1)}, bf16[1,2,128,256]{3,2,1,0:T(8,128)(2,1)S(1)}, u32[]{:S(2)}, u32[]{:S(2)}) collective-permute-start(bf16[1,2,128,256]{3,2,1,0:T(8,128)(2,1)S(1)} %get-tuple-element.44.kv_ref.a), channel_id=1, source_target_pairs={{0,8},{8,16},{16,24},{24,0},{1,9},{9,17},{17,25},{25,1},{2,10},{10... | collective-permute-start | bytes 393224 | tf_op jit(solution)/shard_map/ppermute | solution.py:319
  23.9 6.8 %collective-permute-start.9 = (bf16[1,2,128,256]{3,2,1,0:T(8,128)(2,1)S(1)}, bf16[1,2,128,256]{3,2,1,0:T(8,128)(2,1)S(1)}, u32[]{:S(2)}, u32[]{:S(2)}) collective-permute-start(bf16[1,2,128,256]{3,2,1,0:T(8,128)(2,1)S(1)} %get-tuple-element.44.kv_ref.a), channel_id=1, source_target_pairs={{0,24},{8,0},{16,8},{24,16},{1,25},{9,1},{17,9},{25,17},{2,26},{10... | collective-permute-start | bytes 393224 | tf_op jit(solution)/shard_map/ppermute | solution.py:319
  30.8 26.6 %collective-permute-start.11 = (bf16[4,2,128,256]{3,2,1,0:T(8,128)(2,1)S(1)}, bf16[4,2,128,256]{3,2,1,0:T(8,128)(2,1)S(1)}, u32[]{:S(2)}, u32[]{:S(2)}) collective-permute-start(bf16[4,2,128,256]{3,2,1,0:T(8,128)(2,1)S(1)} %join.1), channel_id=1, source_target_pairs={{0,32},{32,64},{64,96},{96,128},{128,160},{160,192},{192,224},{224... | collective-permute-start | bytes 1572872 | tf_op jit(solution)/shard_map/ppermute | solution.py:331
  30.9 27.9 %collective-permute-start.15 = (bf16[4,2,128,256]{3,2,1,0:T(8,128)(2,1)S(1)}, bf16[4,2,128,256]{3,2,1,0:T(8,128)(2,1)S(1)}, u32[]{:S(2)}, u32[]{:S(2)}) collective-permute-start(bf16[4,2,128,256]{3,2,1,0:T(8,128)(2,1)S(1)} %join.1), channel_id=1, source_target_pairs={{0,224},{32,0},{64,32},{96,64},{128,96},{160,128},{192,160},{224,1... | collective-permute-start | bytes 1572872 | tf_op jit(solution)/shard_map/ppermute | solution.py:332
  55.5 86.2 %collective-permute-start.19 = (bf16[16,512]{1,0:T(8,128)(2,1)S(1)}, bf16[16,512]{1,0:T(8,128)(2,1)S(1)}, u32[]{:S(2)}, u32[]{:S(2)}) collective-permute-start(bf16[16,512]{1,0:T(8,128)(2,1)S(1)} %slice.30), channel_id=1, source_target_pairs={{0,4},{4,8},{8,12},{12,16},{16,20},{20,24},{24,28},{28,32},{32,36}... | collective-permute-start | bytes 49160 | tf_op jit(solution)/shard_map/ppermute | solution.py:358
  57.4 42.8 %collective-permute-start.12 = (bf16[4,2,128,256]{3,2,1,0:T(8,128)(2,1)S(1)}, bf16[4,2,128,256]{3,2,1,0:T(8,128)(2,1)S(1)}, u32[]{:S(2)}, u32[]{:S(2)}) collective-permute-start(bf16[4,2,128,256]{3,2,1,0:T(8,128)(2,1)S(1)} %collective-permute-done.11.refs_2_), channel_id=1, source_target_pairs={{0,32},{32,64},{64,96},{96,128},{128,160},{160,192},{192,224},{224... | collective-permute-start | bytes 1572872 | tf_op jit(solution)/shard_map/ppermute | solution.py:331
  58.8 41.5 %collective-permute-start.16 = (bf16[4,2,128,256]{3,2,1,0:T(8,128)(2,1)S(1)}, bf16[4,2,128,256]{3,2,1,0:T(8,128)(2,1)S(1)}, u32[]{:S(2)}, u32[]{:S(2)}) collective-permute-start(bf16[4,2,128,256]{3,2,1,0:T(8,128)(2,1)S(1)} %collective-permute-done.15.refs_3_), channel_id=1, source_target_pairs={{0,224},{32,0},{64,32},{96,64},{128,96},{160,128},{192,160},{224,1... | collective-permute-start | bytes 1572872 | tf_op jit(solution)/shard_map/ppermute | solution.py:332
  100.2 42.6 %collective-permute-start.13 = (bf16[4,2,128,256]{3,2,1,0:T(8,128)(2,1)S(1)}, bf16[4,2,128,256]{3,2,1,0:T(8,128)(2,1)S(1)}, u32[]{:S(2)}, u32[]{:S(2)}) collective-permute-start(bf16[4,2,128,256]{3,2,1,0:T(8,128)(2,1)S(1)} %collective-permute-done.12.refs_2_), channel_id=1, source_target_pairs={{0,32},{32,64},{64,96},{96,128},{128,160},{160,192},{192,224},{224... | collective-permute-start | bytes 1572872 | tf_op jit(solution)/shard_map/ppermute | solution.py:331
  100.3 42.8 %collective-permute-start.17 = (bf16[4,2,128,256]{3,2,1,0:T(8,128)(2,1)S(1)}, bf16[4,2,128,256]{3,2,1,0:T(8,128)(2,1)S(1)}, u32[]{:S(2)}, u32[]{:S(2)}) collective-permute-start(bf16[4,2,128,256]{3,2,1,0:T(8,128)(2,1)S(1)} %collective-permute-done.16.refs_3_), channel_id=1, source_target_pairs={{0,224},{32,0},{64,32},{96,64},{128,96},{160,128},{192,160},{224,1... | collective-permute-start | bytes 1572872 | tf_op jit(solution)/shard_map/ppermute | solution.py:332
  142.8 41.9 %collective-permute-start.14 = (bf16[2,2,128,256]{3,2,1,0:T(8,128)(2,1)S(1)}, bf16[2,2,128,256]{3,2,1,0:T(8,128)(2,1)S(1)}, u32[]{:S(2)}, u32[]{:S(2)}) collective-permute-start(bf16[2,2,128,256]{3,2,1,0:T(8,128)(2,1)S(1)} %slice.28), channel_id=1, source_target_pairs={{0,32},{32,64},{64,96},{96,128},{128,160},{160,192},{192,224},{224... | collective-permute-start | bytes 786440 | tf_op jit(solution)/shard_map/ppermute | solution.py:333
  143.2 41.5 %collective-permute-start.18 = (bf16[2,2,128,256]{3,2,1,0:T(8,128)(2,1)S(1)}, bf16[2,2,128,256]{3,2,1,0:T(8,128)(2,1)S(1)}, u32[]{:S(2)}, u32[]{:S(2)}) collective-permute-start(bf16[2,2,128,256]{3,2,1,0:T(8,128)(2,1)S(1)} %slice.29), channel_id=1, source_target_pairs={{0,224},{32,0},{64,32},{96,64},{128,96},{160,128},{192,160},{224,1... | collective-permute-start | bytes 786440 | tf_op jit(solution)/shard_map/ppermute | solution.py:334
  210.6 6.4 %collective-permute-start.25 = (bf16[32,2048]{1,0:T(8,128)(2,1)S(1)}, bf16[32,2048]{1,0:T(8,128)(2,1)S(1)}, u32[]{:S(2)}, u32[]{:S(2)}) collective-permute-start(bf16[32,2048]{1,0:T(8,128)(2,1)S(1)} %get-tuple-element.84), channel_id=1, source_target_pairs={{0,3},{1,0},{2,1},{3,2},{4,7},{5,4},{6,5},{7,6},{8,11},{9,8},{10,9... | collective-permute-start | bytes 393224 | tf_op jit(solution)/shard_map/ppermute | solution.py:392
  210.7 7.3 %collective-permute-start.21 = (bf16[32,2048]{1,0:T(8,128)(2,1)S(1)}, bf16[32,2048]{1,0:T(8,128)(2,1)S(1)}, u32[]{:S(2)}, u32[]{:S(2)}) collective-permute-start(bf16[32,2048]{1,0:T(8,128)(2,1)S(1)} %get-tuple-element.80), channel_id=1, source_target_pairs={{0,1},{1,2},{2,3},{3,0},{4,5},{5,6},{6,7},{7,4},{8,9},{9,10},{10,1... | collective-permute-start | bytes 393224 | tf_op jit(solution)/shard_map/ppermute | solution.py:391
  212.7 7.2 %collective-permute-start.23 = (bf16[32,2048]{1,0:T(8,128)(2,1)S(1)}, bf16[32,2048]{1,0:T(8,128)(2,1)S(1)}, u32[]{:S(2)}, u32[]{:S(2)}) collective-permute-start(bf16[32,2048]{1,0:T(8,128)(2,1)S(1)} %get-tuple-element.81), channel_id=1, source_target_pairs={{0,3},{1,0},{2,1},{3,2},{4,7},{5,4},{6,5},{7,6},{8,11},{9,8},{10,9... | collective-permute-start | bytes 393224 | tf_op jit(solution)/shard_map/ppermute | solution.py:394
  214.0 6.3 %collective-permute-start.24 = (bf16[32,2048]{1,0:T(8,128)(2,1)S(1)}, bf16[32,2048]{1,0:T(8,128)(2,1)S(1)}, u32[]{:S(2)}, u32[]{:S(2)}) collective-permute-start(bf16[32,2048]{1,0:T(8,128)(2,1)S(1)} %get-tuple-element.82), channel_id=1, source_target_pairs={{0,1},{1,2},{2,3},{3,0},{4,5},{5,6},{6,7},{7,4},{8,9},{9,10},{10,1... | collective-permute-start | bytes 393224 | tf_op jit(solution)/shard_map/ppermute | solution.py:393
  218.0 6.3 %collective-permute-start.22 = (bf16[32,2048]{1,0:T(8,128)(2,1)S(1)}, bf16[32,2048]{1,0:T(8,128)(2,1)S(1)}, u32[]{:S(2)}, u32[]{:S(2)}) collective-permute-start(bf16[32,2048]{1,0:T(8,128)(2,1)S(1)} %add_convert_fusion.3), channel_id=1, source_target_pairs={{0,1},{1,2},{2,3},{3,0},{4,5},{5,6},{6,7},{7,4},{8,9},{9,10},{10,1... | collective-permute-start | bytes 393224 | tf_op jit(solution)/shard_map/ppermute | solution.py:399
  (13 other events, 272.8 us)

commit v6 on v5

--- a/solution.py
+++ b/solution.py
@@ -8,6 +8,7 @@
 from jax.experimental.pallas import tpu as pltpu
 from jax.sharding import Mesh
 from jax.sharding import PartitionSpec as P
+
 
 NORM_EPS = 1e-06
 WINDOW = 16
@@ -137,6 +138,7 @@
                     source = ins[pair].at[b, half]
                     keys_ref[rows[half]] = source[:, :HALF]
                     values_ref[0:HALF, rows[half]] = source[:, HALF:]
+
             at += count
 
     def keep_state():
@@ -225,7 +227,7 @@
     return pltpu.with_memory_space_constraint(array, pltpu.VMEM)
 
 
-def attend_chunk(place, q, state, plan, arrays, name, rolled=False):
+def attend_chunk(place, q, state, plan, arrays, rolled=False):
     n = len(arrays)
     blocks = sum(len(offsets) for _, offsets in plan)
     return pl.pallas_call(
@@ -245,7 +247,6 @@
             flops=blocks * MAPS * 2 * 256 * 512 * 512, transcendentals=blocks * MAPS * 256 * 512, bytes_accessed=1 << 20
         ),
         compiler_params=vmem(20),
-        name=name,
     )(place, in_vmem(q), *arrays, in_vmem(state[0]), in_vmem(state[1]))
 
 
@@ -316,7 +317,9 @@
     )(place, tokens, up_a, up_b, far_a, far_b, down_a, down_b, norm_gain[None], kv_w)
     kv_oth = lax.ppermute(kv, "c", [(0, 1), (1, 0)])
 
-    beside = [lax.ppermute(kv, "y", ring(4, step)) for step in (1, -1, 2)]
+    beside = []
+    for step in (1, -1, 2):
+        beside.append(lax.ppermute(kv, "y", ring(4, step)))
     group = pl.pallas_call(
         join_kernel,
         out_shape=jax.ShapeDtypeStruct((4, 2, HALF, 2 * HALF), BF16),
@@ -333,9 +336,8 @@
     up.append(lax.ppermute(up[3][:2], "z", ring(8, 1)))
     down.append(lax.ppermute(down[3][2:], "z", ring(8, -1)))
 
-    normed, query_weight, kv_oth = lax.optimization_barrier((normed, query_weight, kv_oth))
+    scale = (query_weight.shape[2] // 2) ** -0.5 * LOG2E
     query_w = query_weight.reshape(width, -1)
-    scale = (query_weight.shape[2] // 2) ** -0.5 * LOG2E
     q_own = (
         lax.dot_general(query_w, normed, (((0,), (1,)), ((), ())), preferred_element_type=F32) * scale
     ).astype(BF16)
@@ -351,7 +353,7 @@
         name="first",
     )(place, kv, kv_oth, q_own, q_oth)
     plan = tuple((i, ((0, dy),)) for i, dy in enumerate(columns[1:]))
-    state = attend_chunk(place, q, state, plan, beside, "chunk0", rolled=True)
+    state = attend_chunk(place, q, state, plan, beside, rolled=True)
     normed, gate_weight, state = lax.optimization_barrier((normed, gate_weight, state))
     gate_w = gate_weight.reshape(width, -1)
     pool_in = dot(normed, pool_weight[:, 0]).astype(BF16)
@@ -361,7 +363,7 @@
             (0, tuple((-k, dy) for dy in (columns if k < 4 else columns[:2]))),
             (1, tuple((k, dy) for dy in (columns if k < 4 else columns[2:]))),
         )
-        state = attend_chunk(place, q, state, plan, (up[k], down[k]), f"chunk{k}", rolled=k == 4)
+        state = attend_chunk(place, q, state, plan, (up[k], down[k]), rolled=k == 4)
         if k == 1:
             normed, state = lax.optimization_barrier((normed, state))
             gate_pre = dot(normed, gate_w).astype(BF16)

time: 227 us -> 227 us (level)
  starting transfers between devices: 30.4 us -> 34.1 us
  waiting for transfers between devices: 20.1 us -> 17.7 us
    ppermute x1, starting transfers between devices: 0.08 us -> 3.17 us  [local(): from_far_b = lax.ppermute(far_b, 'x', ring(4, -1))]
    ppermute x1, starting transfers between devices: 0.89 us -> 3.7 us  [local(): high_b = lax.ppermute(add(down_b, from_far_b), 'x', ring(4, -1))]
    ppermute x1, waiting for transfers between devices: 2.32 us -> 0.01 us  [local(): from_far_b = lax.ppermute(far_b, 'x', ring(4, -1))]
  transfers between devices with their start and end apart: 27 -> 27, of which waited for: 12 -> 10; matrix products, arithmetic and copies ran while one was open for 2% -> 2% of each run, Pallas kernels for 62% -> 62%
where the time goes in v6:
time: 227 us
  Pallas kernels  165 us (73%)
  starting transfers between devices  34.1 us (15%)
  waiting for transfers between devices  17.7 us (8%)
  local copies, waits for them, and re-layouts  3.73 us (2%)
  matrix products  3 us (1%)
  other arithmetic  2.28 us (1%)
    pallas_call x5, Pallas kernels, attend_chunk(): pl.pallas_call(functools.partial(chunk_kernel, plan, n, rolled), out_shap...  157 us
    ppermute x3, waiting for transfers between devices, local(): beside.append(lax.ppermute(kv, 'y', ring(4, step)))  6.86 us
    ppermute x3, starting transfers between devices, local(): down.append(lax.ppermute(down[-1], 'z', ring(8, -1)))  4.74 us
  transfers between devices with their start and end apart: 27, of which 10 were waited for; matrix products, arithmetic and copies ran while one was open for 2% of the time, Pallas kernels for 62%

profile of v6, /device:TPU:248, one launch (start us, length us, event | category | flops | bytes accessed | tf_op | source)
XLA Modules:
  0.0 226.6 jit_solution(4196997062890345179)
XLA Ops:
  0.7 1.8 fusion.17
  4.0 1.7 collective-permute-start.3
  6.0 3.0 %collective-permute-start.5 = (bf16[32,2048]{1,0:T(8,128)(2,1)}, bf16[32,2048]{1,0:T(8,128)(2,1)}, u32[]{:S(2)}, u32[]{:S(2)}) collective-permute-start(bf16[32,2048]{1,0:T(8,128)(2,1)} %get-tuple-element.83), channel_id=1, source_target_pairs={{0,3},{1,0},{2,1},{3,2},{4,7},{5,4},{6,5},{7,6},{8,11},{9,8},{10,9... | collective-permute-start | bytes 393224 | tf_op jit(solution)/shard_map/ppermute | solution.py:306
  10.6 1.9 collective-permute-start.4
  15.9 2.1 front.1
  20.4 2.2 collective-permute-start.8
  22.6 4.4 %collective-permute-done.10.d.refs_4_ = bf16[1,2,128,256]{3,2,1,0:T(8,128)(2,1)S(1)} collective-permute-done((bf16[1,2,128,256]{3,2,1,0:T(8,128)(2,1)S(1)}, bf16[1,2,128,256]{3,2,1,0:T(8,128)(2,1)S(1)}, u32[]{:S(2)}, u32[]{:S(2)}) %collective-permute-start.10) | collective-permute-done | bytes 131104 | tf_op jit(solution)/shard_map/ppermute | solution.py:322
  27.1 2.4 %collective-permute-done.9.c.refs_3_ = bf16[1,2,128,256]{3,2,1,0:T(8,128)(2,1)S(1)} collective-permute-done((bf16[1,2,128,256]{3,2,1,0:T(8,128)(2,1)S(1)}, bf16[1,2,128,256]{3,2,1,0:T(8,128)(2,1)S(1)}, u32[]{:S(2)}, u32[]{:S(2)}) %collective-permute-start.9) | collective-permute-done | bytes 131104 | tf_op jit(solution)/shard_map/ppermute | solution.py:322
  29.6 2.0 collective-permute-start.15
  31.6 3.1 %first.1 = (f32[8,152,256]{2,1,0:T(8,128)S(1)}, f32[8,152,256]{2,1,0:T(8,128)S(1)}, bf16[8,128,512]{2,1,0:T(8,128)(2,1)S(1)}) custom-call(s32[4]{0:T(128)S(1)} %pad_add_fusion.place_ref.refs_0_, bf16[1,2,128,256]{3,2,1,0:T(8,128)(2,1)S(1)} %get-tuple-element.41.kv_ref.a, bf16[1,2,128,256]{3,2,1,0:T(8,128)(2,1)S(1)} %collective-permute-done.6.oth_kv_ref, ...), custom_call_target="tpu_custom_call" | custom-call | tf_op jit(solution)/shard_map/first/pallas_call | solution.py:346
  34.7 17.5 %shard_map.131 = (f32[8,152,256]{2,1,0:T(8,128)S(1)}, f32[8,152,256]{2,1,0:T(8,128)S(1)}) custom-call(s32[4]{0:T(128)S(1)} %pad_add_fusion.place_ref.refs_0_, bf16[8,128,512]{2,1,0:T(8,128)(2,1)S(1)} %get-tuple-element.43.refs_1_, bf16[1,2,128,256]{3,2,1,0:T(8,128)(2,1)S(1)} %collective-permute-done.8.b.refs_2_, ...), custom_call_target="tpu_custom_call" | custom-call | flops 3221225472 | bytes 1048576 | tf_op jit(solution)/shard_map/pallas_call | solution.py:233
  54.2 1.9 collective-permute-start.19
  58.2 39.4 %shard_map.132 = (f32[8,152,256]{2,1,0:T(8,128)S(1)}, f32[8,152,256]{2,1,0:T(8,128)S(1)}) custom-call(s32[4]{0:T(128)S(1)} %pad_add_fusion.place_ref.refs_0_, bf16[8,128,512]{2,1,0:T(8,128)(2,1)S(1)} %get-tuple-element.43.refs_1_, bf16[4,2,128,256]{3,2,1,0:T(8,128)(2,1)S(1)} %collective-permute-done.11.refs_2_, ...), custom_call_target="tpu_custom_call" | custom-call | flops 8589934592 | bytes 1048576 | tf_op jit(solution)/shard_map/pallas_call | solution.py:233
  99.0 2.0 collective-permute-start.17
  101.0 39.3 %shard_map.133 = (f32[8,152,256]{2,1,0:T(8,128)S(1)}, f32[8,152,256]{2,1,0:T(8,128)S(1)}) custom-call(s32[4]{0:T(128)S(1)} %pad_add_fusion.place_ref.refs_0_, bf16[8,128,512]{2,1,0:T(8,128)(2,1)S(1)} %get-tuple-element.43.refs_1_, bf16[4,2,128,256]{3,2,1,0:T(8,128)(2,1)S(1)} %collective-permute-done.12.refs_2_, ...), custom_call_target="tpu_custom_call" | custom-call | flops 8589934592 | bytes 1048576 | tf_op jit(solution)/shard_map/pallas_call | solution.py:233
  141.9 2.1 collective-permute-start.18
  144.0 39.5 %shard_map.134 = (f32[8,152,256]{2,1,0:T(8,128)S(1)}, f32[8,152,256]{2,1,0:T(8,128)S(1)}) custom-call(s32[4]{0:T(128)S(1)} %pad_add_fusion.place_ref.refs_0_, bf16[8,128,512]{2,1,0:T(8,128)(2,1)S(1)} %get-tuple-element.43.refs_1_, bf16[4,2,128,256]{3,2,1,0:T(8,128)(2,1)S(1)} %collective-permute-done.13.refs_2_, ...), custom_call_target="tpu_custom_call" | custom-call | flops 8589934592 | bytes 1048576 | tf_op jit(solution)/shard_map/pallas_call | solution.py:233
  183.5 21.1 %shard_map.135 = (f32[8,152,256]{2,1,0:T(8,128)S(1)}, f32[8,152,256]{2,1,0:T(8,128)S(1)}) custom-call(s32[4]{0:T(128)S(1)} %pad_add_fusion.place_ref.refs_0_, bf16[8,128,512]{2,1,0:T(8,128)(2,1)S(1)} %get-tuple-element.43.refs_1_, bf16[2,2,128,256]{3,2,1,0:T(8,128)(2,1)S(1)} %collective-permute-done.14.refs_2_, ...), custom_call_target="tpu_custom_call" | custom-call | flops 4294967296 | bytes 1048576 | tf_op jit(solution)/shard_map/pallas_call | solution.py:233
  204.7 2.9 %collective-permute-done.20.b_ref = f32[8,152,256]{2,1,0:T(8,128)S(1)} collective-permute-done((f32[8,152,256]{2,1,0:T(8,128)S(1)}, f32[8,152,256]{2,1,0:T(8,128)S(1)}, u32[]{:S(2)}, u32[]{:S(2)}) %collective-permute-start.20) | collective-permute-done | bytes 1245216 | tf_op jit(solution)/shard_map/ppermute | solution.py:382
  209.3 3.2 %collective-permute-start.25 = (bf16[32,2048]{1,0:T(8,128)(2,1)S(1)}, bf16[32,2048]{1,0:T(8,128)(2,1)S(1)}, u32[]{:S(2)}, u32[]{:S(2)}) collective-permute-start(bf16[32,2048]{1,0:T(8,128)(2,1)S(1)} %get-tuple-element.78), channel_id=1, source_target_pairs={{0,3},{1,0},{2,1},{3,2},{4,7},{5,4},{6,5},{7,6},{8,11},{9,8},{10,9... | collective-permute-start | bytes 393224 | tf_op jit(solution)/shard_map/ppermute | solution.py:394
  212.5 3.2 %collective-permute-start.23 = (bf16[32,2048]{1,0:T(8,128)(2,1)S(1)}, bf16[32,2048]{1,0:T(8,128)(2,1)S(1)}, u32[]{:S(2)}, u32[]{:S(2)}) collective-permute-start(bf16[32,2048]{1,0:T(8,128)(2,1)S(1)} %get-tuple-element.75), channel_id=1, source_target_pairs={{0,3},{1,0},{2,1},{3,2},{4,7},{5,4},{6,5},{7,6},{8,11},{9,8},{10,9... | collective-permute-start | bytes 393224 | tf_op jit(solution)/shard_map/ppermute | solution.py:396
  215.8 3.7 %collective-permute-start.26 = (bf16[32,2048]{1,0:T(8,128)(2,1)S(1)}, bf16[32,2048]{1,0:T(8,128)(2,1)S(1)}, u32[]{:S(2)}, u32[]{:S(2)}) collective-permute-start(bf16[32,2048]{1,0:T(8,128)(2,1)S(1)} %add_convert_fusion.1), channel_id=1, source_target_pairs={{0,3},{1,0},{2,1},{3,2},{4,7},{5,4},{6,5},{7,6},{8,11},{9,8},{10,9... | collective-permute-start | bytes 393224 | tf_op jit(solution)/shard_map/ppermute | solution.py:402
  220.2 1.7 collective-permute-done.24
  222.0 3.8 %collective-permute-done.22 = bf16[32,2048]{1,0:T(8,128)(2,1)S(1)} collective-permute-done((bf16[32,2048]{1,0:T(8,128)(2,1)S(1)}, bf16[32,2048]{1,0:T(8,128)(2,1)S(1)}, u32[]{:S(2)}, u32[]{:S(2)}) %collective-permute-start.22) | collective-permute-done | bytes 131104 | tf_op jit(solution)/shard_map/ppermute | solution.py:401
  (76 shorter events, 19.6 us)
Async XLA Ops:
  2.5 6.8 %collective-permute-start = (bf16[32,2048]{1,0:T(8,128)(2,1)}, bf16[32,2048]{1,0:T(8,128)(2,1)S(1)}, u32[]{:S(2)}, u32[]{:S(2)}) collective-permute-start(bf16[32,2048]{1,0:T(8,128)(2,1)} %get-tuple-element.83), channel_id=1, source_target_pairs={{0,1},{1,2},{2,3},{3,0},{4,5},{5,6},{6,7},{7,4},{8,9},{9,10},{10,1... | collective-permute-start | bytes 393224 | tf_op jit(solution)/shard_map/ppermute | solution.py:303
  4.0 6.6 %collective-permute-start.3 = (bf16[32,2048]{1,0:T(8,128)(2,1)}, bf16[32,2048]{1,0:T(8,128)(2,1)}, u32[]{:S(2)}, u32[]{:S(2)}) collective-permute-start(bf16[32,2048]{1,0:T(8,128)(2,1)} %get-tuple-element.82), channel_id=1, source_target_pairs={{0,3},{1,0},{2,1},{3,2},{4,7},{5,4},{6,5},{7,6},{8,11},{9,8},{10,9... | collective-permute-start | bytes 393224 | tf_op jit(solution)/shard_map/ppermute | solution.py:304
  5.7 8.2 %collective-permute-start.1 = (bf16[32,2048]{1,0:T(8,128)(2,1)}, bf16[32,2048]{1,0:T(8,128)(2,1)}, u32[]{:S(2)}, u32[]{:S(2)}) collective-permute-start(bf16[32,2048]{1,0:T(8,128)(2,1)} %get-tuple-element.82), channel_id=1, source_target_pairs={{0,1},{1,2},{2,3},{3,0},{4,5},{5,6},{6,7},{7,4},{8,9},{9,10},{10,1... | collective-permute-start | bytes 393224 | tf_op jit(solution)/shard_map/ppermute | solution.py:305
  6.0 7.9 %collective-permute-start.5 = (bf16[32,2048]{1,0:T(8,128)(2,1)}, bf16[32,2048]{1,0:T(8,128)(2,1)}, u32[]{:S(2)}, u32[]{:S(2)}) collective-permute-start(bf16[32,2048]{1,0:T(8,128)(2,1)} %get-tuple-element.83), channel_id=1, source_target_pairs={{0,3},{1,0},{2,1},{3,2},{4,7},{5,4},{6,5},{7,6},{8,11},{9,8},{10,9... | collective-permute-start | bytes 393224 | tf_op jit(solution)/shard_map/ppermute | solution.py:306
  9.3 6.3 %collective-permute-start.2 = (bf16[32,2048]{1,0:T(8,128)(2,1)S(1)}, bf16[32,2048]{1,0:T(8,128)(2,1)}, u32[]{:S(2)}, u32[]{:S(2)}) collective-permute-start(bf16[32,2048]{1,0:T(8,128)(2,1)S(1)} %collective-permute-done.p1a), channel_id=1, source_target_pairs={{0,1},{1,2},{2,3},{3,0},{4,5},{5,6},{6,7},{7,4},{8,9},{9,10},{10,1... | collective-permute-start | bytes 393224 | tf_op jit(solution)/shard_map/ppermute | solution.py:307
  19.0 12.6 %collective-permute-start.7 = (bf16[512,256]{1,0:T(8,128)(2,1)S(1)}, bf16[512,256]{1,0:T(8,128)(2,1)S(1)}, u32[]{:S(2)}, u32[]{:S(2)}) collective-permute-start(bf16[512,256]{1,0:T(8,128)(2,1)S(1)} %fusion.14.q_own_ref), channel_id=1, source_target_pairs={{0,4},{4,0},{1,5},{5,1},{2,6},{6,2},{3,7},{7,3},{8,12},{12,8},{9,1... | collective-permute-start | bytes 786440 | tf_op jit(solution)/shard_map/ppermute | solution.py:344
  19.1 8.0 %collective-permute-start.10 = (bf16[1,2,128,256]{3,2,1,0:T(8,128)(2,1)S(1)}, bf16[1,2,128,256]{3,2,1,0:T(8,128)(2,1)S(1)}, u32[]{:S(2)}, u32[]{:S(2)}) collective-permute-start(bf16[1,2,128,256]{3,2,1,0:T(8,128)(2,1)S(1)} %get-tuple-element.41.kv_ref.a), channel_id=1, source_target_pairs={{0,16},{8,24},{16,0},{24,8},{1,17},{9,25},{17,1},{25,9},{2,18},{10... | collective-permute-start | bytes 393224 | tf_op jit(solution)/shard_map/ppermute | solution.py:322
  20.4 6.6 %collective-permute-start.8 = (bf16[1,2,128,256]{3,2,1,0:T(8,128)(2,1)S(1)}, bf16[1,2,128,256]{3,2,1,0:T(8,128)(2,1)S(1)}, u32[]{:S(2)}, u32[]{:S(2)}) collective-permute-start(bf16[1,2,128,256]{3,2,1,0:T(8,128)(2,1)S(1)} %get-tuple-element.41.kv_ref.a), channel_id=1, source_target_pairs={{0,8},{8,16},{16,24},{24,0},{1,9},{9,17},{17,25},{25,1},{2,10},{10... | collective-permute-start | bytes 393224 | tf_op jit(solution)/shard_map/ppermute | solution.py:322
  22.6 6.9 %collective-permute-start.9 = (bf16[1,2,128,256]{3,2,1,0:T(8,128)(2,1)S(1)}, bf16[1,2,128,256]{3,2,1,0:T(8,128)(2,1)S(1)}, u32[]{:S(2)}, u32[]{:S(2)}) collective-permute-start(bf16[1,2,128,256]{3,2,1,0:T(8,128)(2,1)S(1)} %get-tuple-element.41.kv_ref.a), channel_id=1, source_target_pairs={{0,24},{8,0},{16,8},{24,16},{1,25},{9,1},{17,9},{25,17},{2,26},{10... | collective-permute-start | bytes 393224 | tf_op jit(solution)/shard_map/ppermute | solution.py:322
  22.6 9.0 %collective-permute-start.6 = (bf16[1,2,128,256]{3,2,1,0:T(8,128)(2,1)S(1)}, bf16[1,2,128,256]{3,2,1,0:T(8,128)(2,1)S(1)}, u32[]{:S(2)}, u32[]{:S(2)}) collective-permute-start(bf16[1,2,128,256]{3,2,1,0:T(8,128)(2,1)S(1)} %get-tuple-element.41.kv_ref.a), channel_id=1, source_target_pairs={{0,4},{4,0},{1,5},{5,1},{2,6},{6,2},{3,7},{7,3},{8,12},{12,8},{9,1... | collective-permute-start | bytes 393224 | tf_op jit(solution)/shard_map/ppermute | solution.py:318
  29.5 26.6 %collective-permute-start.11 = (bf16[4,2,128,256]{3,2,1,0:T(8,128)(2,1)S(1)}, bf16[4,2,128,256]{3,2,1,0:T(8,128)(2,1)S(1)}, u32[]{:S(2)}, u32[]{:S(2)}) collective-permute-start(bf16[4,2,128,256]{3,2,1,0:T(8,128)(2,1)S(1)} %join.1), channel_id=1, source_target_pairs={{0,32},{32,64},{64,96},{96,128},{128,160},{160,192},{192,224},{224... | collective-permute-start | bytes 1572872 | tf_op jit(solution)/shard_map/ppermute | solution.py:334
  29.6 27.9 %collective-permute-start.15 = (bf16[4,2,128,256]{3,2,1,0:T(8,128)(2,1)S(1)}, bf16[4,2,128,256]{3,2,1,0:T(8,128)(2,1)S(1)}, u32[]{:S(2)}, u32[]{:S(2)}) collective-permute-start(bf16[4,2,128,256]{3,2,1,0:T(8,128)(2,1)S(1)} %join.1), channel_id=1, source_target_pairs={{0,224},{32,0},{64,32},{96,64},{128,96},{160,128},{192,160},{224,1... | collective-permute-start | bytes 1572872 | tf_op jit(solution)/shard_map/ppermute | solution.py:335
  54.2 86.2 %collective-permute-start.19 = (bf16[16,512]{1,0:T(8,128)(2,1)S(1)}, bf16[16,512]{1,0:T(8,128)(2,1)S(1)}, u32[]{:S(2)}, u32[]{:S(2)}) collective-permute-start(bf16[16,512]{1,0:T(8,128)(2,1)S(1)} %slice.30), channel_id=1, source_target_pairs={{0,4},{4,8},{8,12},{12,16},{16,20},{20,24},{24,28},{28,32},{32,36}... | collective-permute-start | bytes 49160 | tf_op jit(solution)/shard_map/ppermute | solution.py:360
  56.1 42.8 %collective-permute-start.12 = (bf16[4,2,128,256]{3,2,1,0:T(8,128)(2,1)S(1)}, bf16[4,2,128,256]{3,2,1,0:T(8,128)(2,1)S(1)}, u32[]{:S(2)}, u32[]{:S(2)}) collective-permute-start(bf16[4,2,128,256]{3,2,1,0:T(8,128)(2,1)S(1)} %collective-permute-done.11.refs_2_), channel_id=1, source_target_pairs={{0,32},{32,64},{64,96},{96,128},{128,160},{160,192},{192,224},{224... | collective-permute-start | bytes 1572872 | tf_op jit(solution)/shard_map/ppermute | solution.py:334
  57.5 41.5 %collective-permute-start.16 = (bf16[4,2,128,256]{3,2,1,0:T(8,128)(2,1)S(1)}, bf16[4,2,128,256]{3,2,1,0:T(8,128)(2,1)S(1)}, u32[]{:S(2)}, u32[]{:S(2)}) collective-permute-start(bf16[4,2,128,256]{3,2,1,0:T(8,128)(2,1)S(1)} %collective-permute-done.15.refs_3_), channel_id=1, source_target_pairs={{0,224},{32,0},{64,32},{96,64},{128,96},{160,128},{192,160},{224,1... | collective-permute-start | bytes 1572872 | tf_op jit(solution)/shard_map/ppermute | solution.py:335
  98.9 42.6 %collective-permute-start.13 = (bf16[4,2,128,256]{3,2,1,0:T(8,128)(2,1)S(1)}, bf16[4,2,128,256]{3,2,1,0:T(8,128)(2,1)S(1)}, u32[]{:S(2)}, u32[]{:S(2)}) collective-permute-start(bf16[4,2,128,256]{3,2,1,0:T(8,128)(2,1)S(1)} %collective-permute-done.12.refs_2_), channel_id=1, source_target_pairs={{0,32},{32,64},{64,96},{96,128},{128,160},{160,192},{192,224},{224... | collective-permute-start | bytes 1572872 | tf_op jit(solution)/shard_map/ppermute | solution.py:334
  99.0 42.8 %collective-permute-start.17 = (bf16[4,2,128,256]{3,2,1,0:T(8,128)(2,1)S(1)}, bf16[4,2,128,256]{3,2,1,0:T(8,128)(2,1)S(1)}, u32[]{:S(2)}, u32[]{:S(2)}) collective-permute-start(bf16[4,2,128,256]{3,2,1,0:T(8,128)(2,1)S(1)} %collective-permute-done.16.refs_3_), channel_id=1, source_target_pairs={{0,224},{32,0},{64,32},{96,64},{128,96},{160,128},{192,160},{224,1... | collective-permute-start | bytes 1572872 | tf_op jit(solution)/shard_map/ppermute | solution.py:335
  141.5 41.9 %collective-permute-start.14 = (bf16[2,2,128,256]{3,2,1,0:T(8,128)(2,1)S(1)}, bf16[2,2,128,256]{3,2,1,0:T(8,128)(2,1)S(1)}, u32[]{:S(2)}, u32[]{:S(2)}) collective-permute-start(bf16[2,2,128,256]{3,2,1,0:T(8,128)(2,1)S(1)} %slice.28), channel_id=1, source_target_pairs={{0,32},{32,64},{64,96},{96,128},{128,160},{160,192},{192,224},{224... | collective-permute-start | bytes 786440 | tf_op jit(solution)/shard_map/ppermute | solution.py:336
  141.9 41.5 %collective-permute-start.18 = (bf16[2,2,128,256]{3,2,1,0:T(8,128)(2,1)S(1)}, bf16[2,2,128,256]{3,2,1,0:T(8,128)(2,1)S(1)}, u32[]{:S(2)}, u32[]{:S(2)}) collective-permute-start(bf16[2,2,128,256]{3,2,1,0:T(8,128)(2,1)S(1)} %slice.29), channel_id=1, source_target_pairs={{0,224},{32,0},{64,32},{96,64},{128,96},{160,128},{192,160},{224,1... | collective-permute-start | bytes 786440 | tf_op jit(solution)/shard_map/ppermute | solution.py:337
  209.3 6.4 %collective-permute-start.25 = (bf16[32,2048]{1,0:T(8,128)(2,1)S(1)}, bf16[32,2048]{1,0:T(8,128)(2,1)S(1)}, u32[]{:S(2)}, u32[]{:S(2)}) collective-permute-start(bf16[32,2048]{1,0:T(8,128)(2,1)S(1)} %get-tuple-element.78), channel_id=1, source_target_pairs={{0,3},{1,0},{2,1},{3,2},{4,7},{5,4},{6,5},{7,6},{8,11},{9,8},{10,9... | collective-permute-start | bytes 393224 | tf_op jit(solution)/shard_map/ppermute | solution.py:394
  212.5 7.0 %collective-permute-start.21 = (bf16[32,2048]{1,0:T(8,128)(2,1)S(1)}, bf16[32,2048]{1,0:T(8,128)(2,1)S(1)}, u32[]{:S(2)}, u32[]{:S(2)}) collective-permute-start(bf16[32,2048]{1,0:T(8,128)(2,1)S(1)} %get-tuple-element.74), channel_id=1, source_target_pairs={{0,1},{1,2},{2,3},{3,0},{4,5},{5,6},{6,7},{7,4},{8,9},{9,10},{10,1... | collective-permute-start | bytes 393224 | tf_op jit(solution)/shard_map/ppermute | solution.py:393
  212.5 7.7 %collective-permute-start.23 = (bf16[32,2048]{1,0:T(8,128)(2,1)S(1)}, bf16[32,2048]{1,0:T(8,128)(2,1)S(1)}, u32[]{:S(2)}, u32[]{:S(2)}) collective-permute-start(bf16[32,2048]{1,0:T(8,128)(2,1)S(1)} %get-tuple-element.75), channel_id=1, source_target_pairs={{0,3},{1,0},{2,1},{3,2},{4,7},{5,4},{6,5},{7,6},{8,11},{9,8},{10,9... | collective-permute-start | bytes 393224 | tf_op jit(solution)/shard_map/ppermute | solution.py:396
  215.8 6.2 %collective-permute-start.26 = (bf16[32,2048]{1,0:T(8,128)(2,1)S(1)}, bf16[32,2048]{1,0:T(8,128)(2,1)S(1)}, u32[]{:S(2)}, u32[]{:S(2)}) collective-permute-start(bf16[32,2048]{1,0:T(8,128)(2,1)S(1)} %add_convert_fusion.1), channel_id=1, source_target_pairs={{0,3},{1,0},{2,1},{3,2},{4,7},{5,4},{6,5},{7,6},{8,11},{9,8},{10,9... | collective-permute-start | bytes 393224 | tf_op jit(solution)/shard_map/ppermute | solution.py:402
  219.5 6.3 %collective-permute-start.22 = (bf16[32,2048]{1,0:T(8,128)(2,1)S(1)}, bf16[32,2048]{1,0:T(8,128)(2,1)S(1)}, u32[]{:S(2)}, u32[]{:S(2)}) collective-permute-start(bf16[32,2048]{1,0:T(8,128)(2,1)S(1)} %add_convert_fusion.3), channel_id=1, source_target_pairs={{0,1},{1,2},{2,3},{3,0},{4,5},{5,6},{6,7},{7,4},{8,9},{9,10},{10,1... | collective-permute-start | bytes 393224 | tf_op jit(solution)/shard_map/ppermute | solution.py:401
  (13 other events, 275.1 us)

commit v7 on v6

--- a/solution.py
+++ b/solution.py
@@ -343,6 +343,12 @@
     ).astype(BF16)
     q_oth = lax.ppermute(q_own, "c", [(0, 1), (1, 0)])
 
+    pool_in = dot(normed, pool_weight[:, 0]).astype(BF16)
+    rim = lax.ppermute(pool_in[ROWS - WINDOW :], ("z", "y", "c"), [(i, i + 1) for i in range(63)])
+    gate_weight, pool_in = lax.optimization_barrier((gate_weight, pool_in))
+    gate_w = gate_weight.reshape(width, -1)
+    q_own, gate_w = lax.optimization_barrier((q_own, gate_w))
+
     *state, q = pl.pallas_call(
         first_kernel,
         out_shape=(*STATE, pltpu.VMEM((MAPS, 128, 2 * ROWS), BF16)),
@@ -354,32 +360,24 @@
     )(place, kv, kv_oth, q_own, q_oth)
     plan = tuple((i, ((0, dy),)) for i, dy in enumerate(columns[1:]))
     state = attend_chunk(place, q, state, plan, beside, rolled=True)
-    normed, gate_weight, state = lax.optimization_barrier((normed, gate_weight, state))
-    gate_w = gate_weight.reshape(width, -1)
-    pool_in = dot(normed, pool_weight[:, 0]).astype(BF16)
-    rim = lax.ppermute(pool_in[ROWS - WINDOW :], ("z", "y", "c"), [(i, i + 1) for i in range(63)])
     for k in range(1, 5):
         plan = (
             (0, tuple((-k, dy) for dy in (columns if k < 4 else columns[:2]))),
             (1, tuple((k, dy) for dy in (columns if k < 4 else columns[2:]))),
         )
-        state = attend_chunk(place, q, state, plan, (up[k], down[k]), rolled=k == 4)
-        if k == 1:
-            normed, state = lax.optimization_barrier((normed, state))
-            gate_pre = dot(normed, gate_w).astype(BF16)
-        if k == 2:
-            gate_pre, state = lax.optimization_barrier((gate_pre, state))
-            part_shape = jax.ShapeDtypeStruct((ROWS, 512), F32)
-            keep, part = pl.pallas_call(
-                pool_kernel,
-                out_shape=(part_shape, part_shape),
-                in_specs=[SMEM] + [VMEM] * 5,
-                out_specs=(VMEM, VMEM),
-                compiler_params=vmem(16),
-                name="pool",
-            )(place, pool_in, rim, gate_pre, pool_mix[0], pool_scale)
-            state, keep, part = lax.optimization_barrier((state, keep, part))
+        state = attend_chunk(place, q, state, plan, (up[k], down[k]))
     other = lax.ppermute(state[1], "c", [(0, 1), (1, 0)])
+    normed, mine = lax.optimization_barrier((normed, state[0]))
+    gate_pre = dot(normed, gate_w).astype(BF16)
+    part_shape = jax.ShapeDtypeStruct((ROWS, 512), F32)
+    keep, part = pl.pallas_call(
+        pool_kernel,
+        out_shape=(part_shape, part_shape),
+        in_specs=[SMEM] + [VMEM] * 5,
+        out_specs=(VMEM, VMEM),
+        compiler_params=vmem(16),
+        name="pool",
+    )(place, pool_in, rim, gate_pre, pool_mix[0], pool_scale)
     piece = jax.ShapeDtypeStruct((32, width), BF16)
     own, up_a, up_b, far_a, far_b, down_a, down_b, logs = pl.pallas_call(
         finish_kernel,
@@ -389,18 +387,16 @@
         scratch_shapes=[pltpu.VMEM((ROWS, 512), BF16)],
         compiler_params=vmem(24),
         name="finish",
-    )(place, mix_lambda, state[0], other, head_gain[None], keep, part, out_weight)
+    )(place, mix_lambda, mine, other, head_gain[None], keep, part, out_weight)
     from_far_a = lax.ppermute(far_a, "x", ring(4, 1))
     from_far_b = lax.ppermute(far_b, "x", ring(4, -1))
-    low_b = lax.ppermute(up_b, "x", ring(4, 1))
-    high_a = lax.ppermute(down_a, "x", ring(4, -1))
 
     def add(*arrays):
         return sum(a.astype(F32) for a in arrays).astype(BF16)
 
-    low_a = lax.ppermute(add(up_a, from_far_a), "x", ring(4, 1))
-    high_b = lax.ppermute(add(down_b, from_far_b), "x", ring(4, -1))
-    mixed = jnp.concatenate([add(own[:32], low_a, high_a), add(own[32:], low_b, high_b)], axis=0)
+    low = lax.ppermute(jnp.concatenate([add(up_a, from_far_a), up_b], axis=0), "x", ring(4, 1))
+    high = lax.ppermute(jnp.concatenate([down_a, add(down_b, from_far_b)], axis=0), "x", ring(4, -1))
+    mixed = add(own, low, high)
     return mixed, jnp.transpose(logs.reshape(4, 2, ROWS), (1, 0, 2))
 
 

time: 227 us -> 222 us (0.978)
  starting transfers between devices: 34.1 us -> 31.2 us
    ppermute x4 -> x2, starting transfers between devices: 7.02 us -> 3.39 us  [the longest x1 3.03 us: local(): lax.ppermute(jnp.concatenate([down_a, add(down_b, from_far_b)], axis=0),...]
    ppermute x1, waiting for transfers between devices: 0.01 us -> 2.94 us  [local(): from_far_a = lax.ppermute(far_a, 'x', ring(4, 1))]
    ppermute x1, waiting for transfers between devices: 2.93 us -> 0.01 us  [local(): other = lax.ppermute(state[1], 'c', [(0, 1), (1, 0)])]
    ppermute x4 -> x2, waiting for transfers between devices: 5.55 us -> 3.59 us  [the longest x1 3.59 us: local(): lax.ppermute(jnp.concatenate([add(up_a, from_far_a), up_b], axis=0), 'x',...]
  transfers between devices with their start and end apart: 27 -> 25, of which waited for: 10 -> 9; matrix products, arithmetic and copies ran while one was open for 2% -> 3% of each run, Pallas kernels for 62% -> 63%
where the time goes in v7:
time: 222 us; the launch traced here: 221 us
  Pallas kernels  163 us (73%)
  starting transfers between devices  31.2 us (14%)
  waiting for transfers between devices  16 us (7%)
  local copies, waits for them, and re-layouts  3.74 us (2%)
  matrix products  2.99 us (1%)
  other arithmetic  2.3 us (1%)
    pallas_call x5, Pallas kernels, attend_chunk(): pl.pallas_call(functools.partial(chunk_kernel, plan, n, rolled), out_shap...  156 us
    ppermute x3, waiting for transfers between devices, local(): beside.append(lax.ppermute(kv, 'y', ring(4, step)))  5.76 us
    ppermute x3, starting transfers between devices, local(): down.append(lax.ppermute(down[-1], 'z', ring(8, -1)))  4.57 us
  transfers between devices with their start and end apart: 25, of which 9 were waited for; matrix products, arithmetic and copies ran while one was open for 3% of the time, Pallas kernels for 63%

profile of v7, /device:TPU:248, one launch (start us, length us, event | category | flops | bytes accessed | tf_op | source)
XLA Modules:
  0.0 220.7 jit_solution(6994016253230164344)
XLA Ops:
  0.7 1.8 fusion.17
  4.0 1.7 collective-permute-start.3
  6.0 3.0 %collective-permute-start.5 = (bf16[32,2048]{1,0:T(8,128)(2,1)}, bf16[32,2048]{1,0:T(8,128)(2,1)}, u32[]{:S(2)}, u32[]{:S(2)}) collective-permute-start(bf16[32,2048]{1,0:T(8,128)(2,1)} %get-tuple-element.65), channel_id=1, source_target_pairs={{0,3},{1,0},{2,1},{3,2},{4,7},{5,4},{6,5},{7,6},{8,11},{9,8},{10,9... | collective-permute-start | bytes 393224 | tf_op jit(solution)/shard_map/ppermute | solution.py:306
  10.6 1.9 collective-permute-start.4
  13.9 1.6 collective-permute-done.2.p2a
  15.9 2.1 front.1
  19.4 2.2 collective-permute-start.8
  22.7 3.3 %collective-permute-done.10.d.refs_4_ = bf16[1,2,128,256]{3,2,1,0:T(8,128)(2,1)S(1)} collective-permute-done((bf16[1,2,128,256]{3,2,1,0:T(8,128)(2,1)S(1)}, bf16[1,2,128,256]{3,2,1,0:T(8,128)(2,1)S(1)}, u32[]{:S(2)}, u32[]{:S(2)}) %collective-permute-start.10) | collective-permute-done | bytes 131104 | tf_op jit(solution)/shard_map/ppermute | solution.py:322
  26.0 2.4 %collective-permute-done.9.c.refs_3_ = bf16[1,2,128,256]{3,2,1,0:T(8,128)(2,1)S(1)} collective-permute-done((bf16[1,2,128,256]{3,2,1,0:T(8,128)(2,1)S(1)}, bf16[1,2,128,256]{3,2,1,0:T(8,128)(2,1)S(1)}, u32[]{:S(2)}, u32[]{:S(2)}) %collective-permute-start.9) | collective-permute-done | bytes 131104 | tf_op jit(solution)/shard_map/ppermute | solution.py:322
  28.6 2.0 collective-permute-start.15
  32.6 3.1 %first.1 = (f32[8,152,256]{2,1,0:T(8,128)S(1)}, f32[8,152,256]{2,1,0:T(8,128)S(1)}, bf16[8,128,512]{2,1,0:T(8,128)(2,1)S(1)}) custom-call(s32[4]{0:T(128)S(1)} %pad_add_fusion.place_ref.refs_0_, bf16[1,2,128,256]{3,2,1,0:T(8,128)(2,1)S(1)} %get-tuple-element.34.kv_ref.a, bf16[1,2,128,256]{3,2,1,0:T(8,128)(2,1)S(1)} %collective-permute-done.6.oth_kv_ref, ...), custom_call_target="tpu_custom_call" | custom-call | tf_op jit(solution)/shard_map/first/pallas_call | solution.py:352
  35.6 17.3 %shard_map.131 = (f32[8,152,256]{2,1,0:T(8,128)S(1)}, f32[8,152,256]{2,1,0:T(8,128)S(1)}) custom-call(s32[4]{0:T(128)S(1)} %pad_add_fusion.place_ref.refs_0_, bf16[8,128,512]{2,1,0:T(8,128)(2,1)S(1)} %get-tuple-element.37.refs_1_, bf16[1,2,128,256]{3,2,1,0:T(8,128)(2,1)S(1)} %collective-permute-done.8.b.refs_2_, ...), custom_call_target="tpu_custom_call" | custom-call | flops 3221225472 | bytes 1048576 | tf_op jit(solution)/shard_map/pallas_call | solution.py:233
  55.1 39.4 %shard_map.132 = (f32[8,152,256]{2,1,0:T(8,128)S(1)}, f32[8,152,256]{2,1,0:T(8,128)S(1)}) custom-call(s32[4]{0:T(128)S(1)} %pad_add_fusion.place_ref.refs_0_, bf16[8,128,512]{2,1,0:T(8,128)(2,1)S(1)} %get-tuple-element.37.refs_1_, bf16[4,2,128,256]{3,2,1,0:T(8,128)(2,1)S(1)} %collective-permute-done.11.refs_2_, ...), custom_call_target="tpu_custom_call" | custom-call | flops 8589934592 | bytes 1048576 | tf_op jit(solution)/shard_map/pallas_call | solution.py:233
  94.6 2.0 collective-permute-start.17
  96.6 39.4 %shard_map.133 = (f32[8,152,256]{2,1,0:T(8,128)S(1)}, f32[8,152,256]{2,1,0:T(8,128)S(1)}) custom-call(s32[4]{0:T(128)S(1)} %pad_add_fusion.place_ref.refs_0_, bf16[8,128,512]{2,1,0:T(8,128)(2,1)S(1)} %get-tuple-element.37.refs_1_, bf16[4,2,128,256]{3,2,1,0:T(8,128)(2,1)S(1)} %collective-permute-done.12.refs_2_, ...), custom_call_target="tpu_custom_call" | custom-call | flops 8589934592 | bytes 1048576 | tf_op jit(solution)/shard_map/pallas_call | solution.py:233
  136.3 2.1 collective-permute-start.18
  138.4 39.4 %shard_map.134 = (f32[8,152,256]{2,1,0:T(8,128)S(1)}, f32[8,152,256]{2,1,0:T(8,128)S(1)}) custom-call(s32[4]{0:T(128)S(1)} %pad_add_fusion.place_ref.refs_0_, bf16[8,128,512]{2,1,0:T(8,128)(2,1)S(1)} %get-tuple-element.37.refs_1_, bf16[4,2,128,256]{3,2,1,0:T(8,128)(2,1)S(1)} %collective-permute-done.13.refs_2_, ...), custom_call_target="tpu_custom_call" | custom-call | flops 8589934592 | bytes 1048576 | tf_op jit(solution)/shard_map/pallas_call | solution.py:233
  177.8 20.1 %shard_map.135 = (f32[8,152,256]{2,1,0:T(8,128)S(1)}, f32[8,152,256]{2,1,0:T(8,128)S(1)}) custom-call(s32[4]{0:T(128)S(1)} %pad_add_fusion.place_ref.refs_0_, bf16[8,128,512]{2,1,0:T(8,128)(2,1)S(1)} %get-tuple-element.37.refs_1_, bf16[2,2,128,256]{3,2,1,0:T(8,128)(2,1)S(1)} %collective-permute-done.14.refs_2_, ...), custom_call_target="tpu_custom_call" | custom-call | flops 4294967296 | bytes 1048576 | tf_op jit(solution)/shard_map/pallas_call | solution.py:233
  198.0 2.4 %collective-permute-start.20 = (bf16[16,512]{1,0:T(8,128)(2,1)S(1)}, bf16[16,512]{1,0:T(8,128)(2,1)S(1)}, u32[]{:S(2)}, u32[]{:S(2)}) collective-permute-start(bf16[16,512]{1,0:T(8,128)(2,1)S(1)} %slice.22), channel_id=1, source_target_pairs={{0,4},{4,8},{8,12},{12,16},{16,20},{20,24},{24,28},{28,32},{32,36}... | collective-permute-start | bytes 49160 | tf_op jit(solution)/shard_map/ppermute | solution.py:347
  204.2 1.7 finish.1
  207.5 1.7 collective-permute-start.23
  209.2 2.9 %collective-permute-done.21 = bf16[32,2048]{1,0:T(8,128)(2,1)S(1)} collective-permute-done((bf16[32,2048]{1,0:T(8,128)(2,1)S(1)}, bf16[32,2048]{1,0:T(8,128)(2,1)S(1)}, u32[]{:S(2)}, u32[]{:S(2)}) %collective-permute-start.21) | collective-permute-done | bytes 131104 | tf_op jit(solution)/shard_map/ppermute | solution.py:391
  212.6 3.0 %collective-permute-start.24 = (bf16[64,2048]{1,0:T(8,128)(2,1)S(1)}, bf16[64,2048]{1,0:T(8,128)(2,1)S(1)}, u32[]{:S(2)}, u32[]{:S(2)}) collective-permute-start(bf16[64,2048]{1,0:T(8,128)(2,1)S(1)} %pad_maximum_fusion.2), channel_id=1, source_target_pairs={{0,3},{1,0},{2,1},{3,2},{4,7},{5,4},{6,5},{7,6},{8,11},{9,8},{10,9... | collective-permute-start | bytes 786440 | tf_op jit(solution)/shard_map/ppermute | solution.py:398
  216.3 3.6 %collective-permute-done.22 = bf16[64,2048]{1,0:T(8,128)(2,1)S(1)} collective-permute-done((bf16[64,2048]{1,0:T(8,128)(2,1)S(1)}, bf16[64,2048]{1,0:T(8,128)(2,1)S(1)}, u32[]{:S(2)}, u32[]{:S(2)}) %collective-permute-start.22) | collective-permute-done | bytes 262176 | tf_op jit(solution)/shard_map/ppermute | solution.py:397
  (73 shorter events, 19.5 us)
Async XLA Ops:
  2.5 6.8 %collective-permute-start = (bf16[32,2048]{1,0:T(8,128)(2,1)}, bf16[32,2048]{1,0:T(8,128)(2,1)S(1)}, u32[]{:S(2)}, u32[]{:S(2)}) collective-permute-start(bf16[32,2048]{1,0:T(8,128)(2,1)} %get-tuple-element.65), channel_id=1, source_target_pairs={{0,1},{1,2},{2,3},{3,0},{4,5},{5,6},{6,7},{7,4},{8,9},{9,10},{10,1... | collective-permute-start | bytes 393224 | tf_op jit(solution)/shard_map/ppermute | solution.py:303
  4.0 6.6 %collective-permute-start.3 = (bf16[32,2048]{1,0:T(8,128)(2,1)}, bf16[32,2048]{1,0:T(8,128)(2,1)}, u32[]{:S(2)}, u32[]{:S(2)}) collective-permute-start(bf16[32,2048]{1,0:T(8,128)(2,1)} %get-tuple-element.64), channel_id=1, source_target_pairs={{0,3},{1,0},{2,1},{3,2},{4,7},{5,4},{6,5},{7,6},{8,11},{9,8},{10,9... | collective-permute-start | bytes 393224 | tf_op jit(solution)/shard_map/ppermute | solution.py:304
  5.7 8.2 %collective-permute-start.1 = (bf16[32,2048]{1,0:T(8,128)(2,1)}, bf16[32,2048]{1,0:T(8,128)(2,1)}, u32[]{:S(2)}, u32[]{:S(2)}) collective-permute-start(bf16[32,2048]{1,0:T(8,128)(2,1)} %get-tuple-element.64), channel_id=1, source_target_pairs={{0,1},{1,2},{2,3},{3,0},{4,5},{5,6},{6,7},{7,4},{8,9},{9,10},{10,1... | collective-permute-start | bytes 393224 | tf_op jit(solution)/shard_map/ppermute | solution.py:305
  6.0 7.9 %collective-permute-start.5 = (bf16[32,2048]{1,0:T(8,128)(2,1)}, bf16[32,2048]{1,0:T(8,128)(2,1)}, u32[]{:S(2)}, u32[]{:S(2)}) collective-permute-start(bf16[32,2048]{1,0:T(8,128)(2,1)} %get-tuple-element.65), channel_id=1, source_target_pairs={{0,3},{1,0},{2,1},{3,2},{4,7},{5,4},{6,5},{7,6},{8,11},{9,8},{10,9... | collective-permute-start | bytes 393224 | tf_op jit(solution)/shard_map/ppermute | solution.py:306
  9.3 6.3 %collective-permute-start.2 = (bf16[32,2048]{1,0:T(8,128)(2,1)S(1)}, bf16[32,2048]{1,0:T(8,128)(2,1)}, u32[]{:S(2)}, u32[]{:S(2)}) collective-permute-start(bf16[32,2048]{1,0:T(8,128)(2,1)S(1)} %collective-permute-done.p1a), channel_id=1, source_target_pairs={{0,1},{1,2},{2,3},{3,0},{4,5},{5,6},{6,7},{7,4},{8,9},{9,10},{10,1... | collective-permute-start | bytes 393224 | tf_op jit(solution)/shard_map/ppermute | solution.py:307
  10.6 5.3 %collective-permute-start.4 = (bf16[32,2048]{1,0:T(8,128)(2,1)}, bf16[32,2048]{1,0:T(8,128)(2,1)}, u32[]{:S(2)}, u32[]{:S(2)}) collective-permute-start(bf16[32,2048]{1,0:T(8,128)(2,1)} %collective-permute-done.3.p3b), channel_id=1, source_target_pairs={{0,3},{1,0},{2,1},{3,2},{4,7},{5,4},{6,5},{7,6},{8,11},{9,8},{10,9... | collective-permute-start | bytes 393224 | tf_op jit(solution)/shard_map/ppermute | solution.py:308
  18.0 14.6 %collective-permute-start.6 = (bf16[1,2,128,256]{3,2,1,0:T(8,128)(2,1)S(1)}, bf16[1,2,128,256]{3,2,1,0:T(8,128)(2,1)S(1)}, u32[]{:S(2)}, u32[]{:S(2)}) collective-permute-start(bf16[1,2,128,256]{3,2,1,0:T(8,128)(2,1)S(1)} %get-tuple-element.34.kv_ref.a), channel_id=1, source_target_pairs={{0,4},{4,0},{1,5},{5,1},{2,6},{6,2},{3,7},{7,3},{8,12},{12,8},{9,1... | collective-permute-start | bytes 393224 | tf_op jit(solution)/shard_map/ppermute | solution.py:318
  18.1 8.0 %collective-permute-start.10 = (bf16[1,2,128,256]{3,2,1,0:T(8,128)(2,1)S(1)}, bf16[1,2,128,256]{3,2,1,0:T(8,128)(2,1)S(1)}, u32[]{:S(2)}, u32[]{:S(2)}) collective-permute-start(bf16[1,2,128,256]{3,2,1,0:T(8,128)(2,1)S(1)} %get-tuple-element.34.kv_ref.a), channel_id=1, source_target_pairs={{0,16},{8,24},{16,0},{24,8},{1,17},{9,25},{17,1},{25,9},{2,18},{10... | collective-permute-start | bytes 393224 | tf_op jit(solution)/shard_map/ppermute | solution.py:322
  19.4 6.6 %collective-permute-start.8 = (bf16[1,2,128,256]{3,2,1,0:T(8,128)(2,1)S(1)}, bf16[1,2,128,256]{3,2,1,0:T(8,128)(2,1)S(1)}, u32[]{:S(2)}, u32[]{:S(2)}) collective-permute-start(bf16[1,2,128,256]{3,2,1,0:T(8,128)(2,1)S(1)} %get-tuple-element.34.kv_ref.a), channel_id=1, source_target_pairs={{0,8},{8,16},{16,24},{24,0},{1,9},{9,17},{17,25},{25,1},{2,10},{10... | collective-permute-start | bytes 393224 | tf_op jit(solution)/shard_map/ppermute | solution.py:322
  21.6 6.9 %collective-permute-start.9 = (bf16[1,2,128,256]{3,2,1,0:T(8,128)(2,1)S(1)}, bf16[1,2,128,256]{3,2,1,0:T(8,128)(2,1)S(1)}, u32[]{:S(2)}, u32[]{:S(2)}) collective-permute-start(bf16[1,2,128,256]{3,2,1,0:T(8,128)(2,1)S(1)} %get-tuple-element.34.kv_ref.a), channel_id=1, source_target_pairs={{0,24},{8,0},{16,8},{24,16},{1,25},{9,1},{17,9},{25,17},{2,26},{10... | collective-permute-start | bytes 393224 | tf_op jit(solution)/shard_map/ppermute | solution.py:322
  22.6 10.0 %collective-permute-start.7 = (bf16[512,256]{1,0:T(8,128)(2,1)S(1)}, bf16[512,256]{1,0:T(8,128)(2,1)S(1)}, u32[]{:S(2)}, u32[]{:S(2)}) collective-permute-start(bf16[512,256]{1,0:T(8,128)(2,1)S(1)} %fusion.14.q_own_ref), channel_id=1, source_target_pairs={{0,4},{4,0},{1,5},{5,1},{2,6},{6,2},{3,7},{7,3},{8,12},{12,8},{9,1... | collective-permute-start | bytes 786440 | tf_op jit(solution)/shard_map/ppermute | solution.py:344
  28.5 24.5 %collective-permute-start.11 = (bf16[4,2,128,256]{3,2,1,0:T(8,128)(2,1)S(1)}, bf16[4,2,128,256]{3,2,1,0:T(8,128)(2,1)S(1)}, u32[]{:S(2)}, u32[]{:S(2)}) collective-permute-start(bf16[4,2,128,256]{3,2,1,0:T(8,128)(2,1)S(1)} %join.1), channel_id=1, source_target_pairs={{0,32},{32,64},{64,96},{96,128},{128,160},{160,192},{192,224},{224... | collective-permute-start | bytes 1572872 | tf_op jit(solution)/shard_map/ppermute | solution.py:334
  28.6 26.0 %collective-permute-start.15 = (bf16[4,2,128,256]{3,2,1,0:T(8,128)(2,1)S(1)}, bf16[4,2,128,256]{3,2,1,0:T(8,128)(2,1)S(1)}, u32[]{:S(2)}, u32[]{:S(2)}) collective-permute-start(bf16[4,2,128,256]{3,2,1,0:T(8,128)(2,1)S(1)} %join.1), channel_id=1, source_target_pairs={{0,224},{32,0},{64,32},{96,64},{128,96},{160,128},{192,160},{224,1... | collective-permute-start | bytes 1572872 | tf_op jit(solution)/shard_map/ppermute | solution.py:335
  53.0 41.5 %collective-permute-start.12 = (bf16[4,2,128,256]{3,2,1,0:T(8,128)(2,1)S(1)}, bf16[4,2,128,256]{3,2,1,0:T(8,128)(2,1)S(1)}, u32[]{:S(2)}, u32[]{:S(2)}) collective-permute-start(bf16[4,2,128,256]{3,2,1,0:T(8,128)(2,1)S(1)} %collective-permute-done.11.refs_2_), channel_id=1, source_target_pairs={{0,32},{32,64},{64,96},{96,128},{128,160},{160,192},{192,224},{224... | collective-permute-start | bytes 1572872 | tf_op jit(solution)/shard_map/ppermute | solution.py:334
  54.5 40.0 %collective-permute-start.16 = (bf16[4,2,128,256]{3,2,1,0:T(8,128)(2,1)S(1)}, bf16[4,2,128,256]{3,2,1,0:T(8,128)(2,1)S(1)}, u32[]{:S(2)}, u32[]{:S(2)}) collective-permute-start(bf16[4,2,128,256]{3,2,1,0:T(8,128)(2,1)S(1)} %collective-permute-done.15.refs_3_), channel_id=1, source_target_pairs={{0,224},{32,0},{64,32},{96,64},{128,96},{160,128},{192,160},{224,1... | collective-permute-start | bytes 1572872 | tf_op jit(solution)/shard_map/ppermute | solution.py:335
  94.5 41.5 %collective-permute-start.13 = (bf16[4,2,128,256]{3,2,1,0:T(8,128)(2,1)S(1)}, bf16[4,2,128,256]{3,2,1,0:T(8,128)(2,1)S(1)}, u32[]{:S(2)}, u32[]{:S(2)}) collective-permute-start(bf16[4,2,128,256]{3,2,1,0:T(8,128)(2,1)S(1)} %collective-permute-done.12.refs_2_), channel_id=1, source_target_pairs={{0,32},{32,64},{64,96},{96,128},{128,160},{160,192},{192,224},{224... | collective-permute-start | bytes 1572872 | tf_op jit(solution)/shard_map/ppermute | solution.py:334
  94.6 41.7 %collective-permute-start.17 = (bf16[4,2,128,256]{3,2,1,0:T(8,128)(2,1)S(1)}, bf16[4,2,128,256]{3,2,1,0:T(8,128)(2,1)S(1)}, u32[]{:S(2)}, u32[]{:S(2)}) collective-permute-start(bf16[4,2,128,256]{3,2,1,0:T(8,128)(2,1)S(1)} %collective-permute-done.16.refs_3_), channel_id=1, source_target_pairs={{0,224},{32,0},{64,32},{96,64},{128,96},{160,128},{192,160},{224,1... | collective-permute-start | bytes 1572872 | tf_op jit(solution)/shard_map/ppermute | solution.py:335
  136.0 41.8 %collective-permute-start.14 = (bf16[2,2,128,256]{3,2,1,0:T(8,128)(2,1)S(1)}, bf16[2,2,128,256]{3,2,1,0:T(8,128)(2,1)S(1)}, u32[]{:S(2)}, u32[]{:S(2)}) collective-permute-start(bf16[2,2,128,256]{3,2,1,0:T(8,128)(2,1)S(1)} %slice.20), channel_id=1, source_target_pairs={{0,32},{32,64},{64,96},{96,128},{128,160},{160,192},{192,224},{224... | collective-permute-start | bytes 786440 | tf_op jit(solution)/shard_map/ppermute | solution.py:336
  136.3 41.5 %collective-permute-start.18 = (bf16[2,2,128,256]{3,2,1,0:T(8,128)(2,1)S(1)}, bf16[2,2,128,256]{3,2,1,0:T(8,128)(2,1)S(1)}, u32[]{:S(2)}, u32[]{:S(2)}) collective-permute-start(bf16[2,2,128,256]{3,2,1,0:T(8,128)(2,1)S(1)} %slice.21), channel_id=1, source_target_pairs={{0,224},{32,0},{64,32},{96,64},{128,96},{160,128},{192,160},{224,1... | collective-permute-start | bytes 786440 | tf_op jit(solution)/shard_map/ppermute | solution.py:337
  197.9 6.3 %collective-permute-start.19 = (f32[8,152,256]{2,1,0:T(8,128)S(1)}, f32[8,152,256]{2,1,0:T(8,128)S(1)}, u32[]{:S(2)}, u32[]{:S(2)}) collective-permute-start(f32[8,152,256]{2,1,0:T(8,128)S(1)} %get-tuple-element.50), channel_id=1, source_target_pairs={{0,4},{4,0},{1,5},{5,1},{2,6},{6,2},{3,7},{7,3},{8,12},{12,8},{9,1... | collective-permute-start | bytes 3735560 | tf_op jit(solution)/shard_map/ppermute | solution.py:369
  205.9 6.3 %collective-permute-start.21 = (bf16[32,2048]{1,0:T(8,128)(2,1)S(1)}, bf16[32,2048]{1,0:T(8,128)(2,1)S(1)}, u32[]{:S(2)}, u32[]{:S(2)}) collective-permute-start(bf16[32,2048]{1,0:T(8,128)(2,1)S(1)} %get-tuple-element.58), channel_id=1, source_target_pairs={{0,1},{1,2},{2,3},{3,0},{4,5},{5,6},{6,7},{7,4},{8,9},{9,10},{10,1... | collective-permute-start | bytes 393224 | tf_op jit(solution)/shard_map/ppermute | solution.py:391
  207.5 5.1 %collective-permute-start.23 = (bf16[32,2048]{1,0:T(8,128)(2,1)S(1)}, bf16[32,2048]{1,0:T(8,128)(2,1)S(1)}, u32[]{:S(2)}, u32[]{:S(2)}) collective-permute-start(bf16[32,2048]{1,0:T(8,128)(2,1)S(1)} %get-tuple-element.62), channel_id=1, source_target_pairs={{0,3},{1,0},{2,1},{3,2},{4,7},{5,4},{6,5},{7,6},{8,11},{9,8},{10,9... | collective-permute-start | bytes 393224 | tf_op jit(solution)/shard_map/ppermute | solution.py:392
  212.2 7.7 %collective-permute-start.22 = (bf16[64,2048]{1,0:T(8,128)(2,1)S(1)}, bf16[64,2048]{1,0:T(8,128)(2,1)S(1)}, u32[]{:S(2)}, u32[]{:S(2)}) collective-permute-start(bf16[64,2048]{1,0:T(8,128)(2,1)S(1)} %pad_maximum_fusion.1), channel_id=1, source_target_pairs={{0,1},{1,2},{2,3},{3,0},{4,5},{5,6},{6,7},{7,4},{8,9},{9,10},{10,1... | collective-permute-start | bytes 786440 | tf_op jit(solution)/shard_map/ppermute | solution.py:397
  212.6 7.2 %collective-permute-start.24 = (bf16[64,2048]{1,0:T(8,128)(2,1)S(1)}, bf16[64,2048]{1,0:T(8,128)(2,1)S(1)}, u32[]{:S(2)}, u32[]{:S(2)}) collective-permute-start(bf16[64,2048]{1,0:T(8,128)(2,1)S(1)} %pad_maximum_fusion.2), channel_id=1, source_target_pairs={{0,3},{1,0},{2,1},{3,2},{4,7},{5,4},{6,5},{7,6},{8,11},{9,8},{10,9... | collective-permute-start | bytes 786440 | tf_op jit(solution)/shard_map/ppermute | solution.py:398
  (11 other events, 92.7 us)

commit v8 on v7

--- a/solution.py
+++ b/solution.py
@@ -86,22 +86,33 @@
         out_ref[i] = ref[0]
 
 
-def front_kernel(place_ref, p0, p1a, p1b, p2a, p2b, p3a, p3b, gain_ref, w_ref, normed_ref, kv_ref):
+def split_kernel(rows_ref, a_ref, b_ref):
+    a_ref[...] = rows_ref[:32]
+    b_ref[...] = rows_ref[32:]
+
+
+def weights_kernel(key_ref, value_ref, out_ref):
+    out_ref[:, :HALF] = key_ref[...]
+    out_ref[:, HALF:] = value_ref[...]
+
+
+def front_kernel(place_ref, p0a, p0b, p1a, p1b, p2a, p2b, p3a, p3b, gain_ref, w_ref, normed_ref, kv_ref):
     x = place_ref[3]
 
-    def put(piece_ref, back, half, rows):
+    def put(piece_ref, back, half):
         values = piece_ref[...].astype(F32)
         scale = lax.rsqrt(jnp.mean(values * values, axis=1, keepdims=True) + NORM_EPS)
         at = pl.multiple_of(((x - back) & 3) * 64 + half * 32, 32)
-        normed_ref[pl.ds(at, rows), :] = (values * scale * gain_ref[...]).astype(BF16)
-
-    put(p0, 0, 0, 64)
-    put(p1a, 1, 0, 32)
-    put(p1b, 1, 1, 32)
-    put(p3a, 3, 0, 32)
-    put(p3b, 3, 1, 32)
-    put(p2a, 2, 0, 32)
-    put(p2b, 2, 1, 32)
+        normed_ref[pl.ds(at, 32), :] = (values * scale * gain_ref[...]).astype(BF16)
+
+    put(p0a, 0, 0)
+    put(p0b, 0, 1)
+    put(p1a, 1, 0)
+    put(p1b, 1, 1)
+    put(p3a, 3, 0)
+    put(p3b, 3, 1)
+    put(p2a, 2, 0)
+    put(p2b, 2, 1)
     both = dot(normed_ref[...], w_ref[...])
     values_t = both[:, HALF:].T.astype(BF16)
     for half in range(2):
@@ -299,22 +310,36 @@
     width = tokens.shape[1]
     z, y, c = lax.axis_index("z"), lax.axis_index("y"), lax.axis_index("c")
     place = jnp.stack([z, y, c, lax.axis_index("x")])
-    halves = tokens[:32], tokens[32:]
+    halves = pl.pallas_call(
+        split_kernel,
+        out_shape=(pltpu.VMEM((32, width), BF16),) * 2,
+        in_specs=[VMEM],
+        out_specs=(VMEM, VMEM),
+        compiler_params=vmem(4),
+        name="split",
+    )(tokens)
     up_a = lax.ppermute(halves[0], "x", ring(4, 1))
     down_b = lax.ppermute(halves[1], "x", ring(4, -1))
     up_b = lax.ppermute(halves[1], "x", ring(4, 1))
     down_a = lax.ppermute(halves[0], "x", ring(4, -1))
     far_a = lax.ppermute(up_a, "x", ring(4, 1))
     far_b = lax.ppermute(down_b, "x", ring(4, -1))
-    kv_w = jnp.concatenate([key_weight[:, 0], value_weight[:, 0]], axis=1)
+    kv_w = pl.pallas_call(
+        weights_kernel,
+        out_shape=pltpu.VMEM((width, 2 * HALF), BF16),
+        in_specs=[VMEM] * 2,
+        out_specs=VMEM,
+        compiler_params=vmem(6),
+        name="weights",
+    )(key_weight[:, 0], value_weight[:, 0])
     normed, kv = pl.pallas_call(
         front_kernel,
         out_shape=(jax.ShapeDtypeStruct((ROWS, width), BF16), jax.ShapeDtypeStruct((1, 2, HALF, 2 * HALF), BF16)),
-        in_specs=[SMEM] + [VMEM] * 9,
+        in_specs=[SMEM] + [VMEM] * 10,
         out_specs=(VMEM, VMEM),
         compiler_params=vmem(16),
         name="front",
-    )(place, tokens, up_a, up_b, far_a, far_b, down_a, down_b, norm_gain[None], kv_w)
+    )(place, *map(in_vmem, (*halves, up_a, up_b, far_a, far_b, down_a, down_b)), norm_gain[None], in_vmem(kv_w))
     kv_oth = lax.ppermute(kv, "c", [(0, 1), (1, 0)])
 
     beside = []

time: 222 us -> 220 us (level)
    unnamed x21 -> x25, local copies, waits for them, and re-layouts: 1.26 us -> 4.42 us
  transfers between devices with their start and end apart: 25 -> 25, of which waited for: 9 -> 8; matrix products, arithmetic and copies ran while one was open for 3% -> 2% of each run, Pallas kernels for 63% -> 64%
where the time goes in v8:
time: 220 us; the launch traced here: 219 us
  Pallas kernels  163 us (74%)
  starting transfers between devices  31.3 us (14%)
  waiting for transfers between devices  14.4 us (7%)
  local copies, waits for them, and re-layouts  5.08 us (2%)
  matrix products  2.99 us (1%)
    pallas_call x5, Pallas kernels, attend_chunk(): pl.pallas_call(functools.partial(chunk_kernel, plan, n, rolled), out_shap...  156 us
    ppermute x3, waiting for transfers between devices, local(): beside.append(lax.ppermute(kv, 'y', ring(4, step)))  5.76 us
    ppermute x3, starting transfers between devices, local(): down.append(lax.ppermute(down[-1], 'z', ring(8, -1)))  4.57 us
    unnamed x25, local copies, waits for them, and re-layouts  4.42 us
  transfers between devices with their start and end apart: 25, of which 8 were waited for; matrix products, arithmetic and copies ran while one was open for 2% of the time, Pallas kernels for 64%

profile of v8, /device:TPU:248, one launch (start us, length us, event | category | flops | bytes accessed | tf_op | source)
XLA Modules:
  0.0 218.8 jit_solution(8959682668339023464)
XLA Ops:
  1.8 1.6 collective-permute-start
  3.3 1.7 collective-permute-start.3
  5.4 3.0 %collective-permute-start.5 = (bf16[32,2048]{1,0:T(8,128)(2,1)S(1)}, bf16[32,2048]{1,0:T(8,128)(2,1)S(1)}, u32[]{:S(2)}, u32[]{:S(2)}) collective-permute-start(bf16[32,2048]{1,0:T(8,128)(2,1)S(1)} %get-tuple-element.35.p0a), channel_id=1, source_target_pairs={{0,3},{1,0},{2,1},{3,2},{4,7},{5,4},{6,5},{7,6},{8,11},{9,8},{10,9... | collective-permute-start | bytes 393224 | tf_op jit(solution)/shard_map/ppermute | solution.py:324
  9.7 2.0 collective-permute-start.4
  17.5 2.2 collective-permute-start.8
  20.8 3.3 %collective-permute-done.10.d.refs_4_ = bf16[1,2,128,256]{3,2,1,0:T(8,128)(2,1)S(1)} collective-permute-done((bf16[1,2,128,256]{3,2,1,0:T(8,128)(2,1)S(1)}, bf16[1,2,128,256]{3,2,1,0:T(8,128)(2,1)S(1)}, u32[]{:S(2)}, u32[]{:S(2)}) %collective-permute-start.10) | collective-permute-done | bytes 131104 | tf_op jit(solution)/shard_map/ppermute | solution.py:347
  24.2 2.4 %collective-permute-done.9.c.refs_3_ = bf16[1,2,128,256]{3,2,1,0:T(8,128)(2,1)S(1)} collective-permute-done((bf16[1,2,128,256]{3,2,1,0:T(8,128)(2,1)S(1)}, bf16[1,2,128,256]{3,2,1,0:T(8,128)(2,1)S(1)}, u32[]{:S(2)}, u32[]{:S(2)}) %collective-permute-start.9) | collective-permute-done | bytes 131104 | tf_op jit(solution)/shard_map/ppermute | solution.py:347
  26.7 2.0 collective-permute-start.15
  30.7 3.1 %first.1 = (f32[8,152,256]{2,1,0:T(8,128)S(1)}, f32[8,152,256]{2,1,0:T(8,128)S(1)}, bf16[8,128,512]{2,1,0:T(8,128)(2,1)S(1)}) custom-call(s32[4]{0:T(128)S(1)} %pad_add_fusion.place_ref.refs_0_, bf16[1,2,128,256]{3,2,1,0:T(8,128)(2,1)S(1)} %get-tuple-element.38.kv_ref.a, bf16[1,2,128,256]{3,2,1,0:T(8,128)(2,1)S(1)} %collective-permute-done.6.oth_kv_ref, ...), custom_call_target="tpu_custom_call" | custom-call | tf_op jit(solution)/shard_map/first/pallas_call | solution.py:377
  33.8 17.3 %shard_map.131 = (f32[8,152,256]{2,1,0:T(8,128)S(1)}, f32[8,152,256]{2,1,0:T(8,128)S(1)}) custom-call(s32[4]{0:T(128)S(1)} %pad_add_fusion.place_ref.refs_0_, bf16[8,128,512]{2,1,0:T(8,128)(2,1)S(1)} %get-tuple-element.41.refs_1_, bf16[1,2,128,256]{3,2,1,0:T(8,128)(2,1)S(1)} %collective-permute-done.8.b.refs_2_, ...), custom_call_target="tpu_custom_call" | custom-call | flops 3221225472 | bytes 1048576 | tf_op jit(solution)/shard_map/pallas_call | solution.py:244
  51.1 1.6 collective-permute-start.12
  53.2 39.4 %shard_map.132 = (f32[8,152,256]{2,1,0:T(8,128)S(1)}, f32[8,152,256]{2,1,0:T(8,128)S(1)}) custom-call(s32[4]{0:T(128)S(1)} %pad_add_fusion.place_ref.refs_0_, bf16[8,128,512]{2,1,0:T(8,128)(2,1)S(1)} %get-tuple-element.41.refs_1_, bf16[4,2,128,256]{3,2,1,0:T(8,128)(2,1)S(1)} %collective-permute-done.11.refs_2_, ...), custom_call_target="tpu_custom_call" | custom-call | flops 8589934592 | bytes 1048576 | tf_op jit(solution)/shard_map/pallas_call | solution.py:244
  92.7 2.0 collective-permute-start.17
  94.7 39.4 %shard_map.133 = (f32[8,152,256]{2,1,0:T(8,128)S(1)}, f32[8,152,256]{2,1,0:T(8,128)S(1)}) custom-call(s32[4]{0:T(128)S(1)} %pad_add_fusion.place_ref.refs_0_, bf16[8,128,512]{2,1,0:T(8,128)(2,1)S(1)} %get-tuple-element.41.refs_1_, bf16[4,2,128,256]{3,2,1,0:T(8,128)(2,1)S(1)} %collective-permute-done.12.refs_2_, ...), custom_call_target="tpu_custom_call" | custom-call | flops 8589934592 | bytes 1048576 | tf_op jit(solution)/shard_map/pallas_call | solution.py:244
  134.5 2.1 collective-permute-start.18
  136.5 39.4 %shard_map.134 = (f32[8,152,256]{2,1,0:T(8,128)S(1)}, f32[8,152,256]{2,1,0:T(8,128)S(1)}) custom-call(s32[4]{0:T(128)S(1)} %pad_add_fusion.place_ref.refs_0_, bf16[8,128,512]{2,1,0:T(8,128)(2,1)S(1)} %get-tuple-element.41.refs_1_, bf16[4,2,128,256]{3,2,1,0:T(8,128)(2,1)S(1)} %collective-permute-done.13.refs_2_, ...), custom_call_target="tpu_custom_call" | custom-call | flops 8589934592 | bytes 1048576 | tf_op jit(solution)/shard_map/pallas_call | solution.py:244
  175.9 20.1 %shard_map.135 = (f32[8,152,256]{2,1,0:T(8,128)S(1)}, f32[8,152,256]{2,1,0:T(8,128)S(1)}) custom-call(s32[4]{0:T(128)S(1)} %pad_add_fusion.place_ref.refs_0_, bf16[8,128,512]{2,1,0:T(8,128)(2,1)S(1)} %get-tuple-element.41.refs_1_, bf16[2,2,128,256]{3,2,1,0:T(8,128)(2,1)S(1)} %collective-permute-done.14.refs_2_, ...), custom_call_target="tpu_custom_call" | custom-call | flops 4294967296 | bytes 1048576 | tf_op jit(solution)/shard_map/pallas_call | solution.py:244
  196.2 2.4 %collective-permute-start.20 = (bf16[16,512]{1,0:T(8,128)(2,1)S(1)}, bf16[16,512]{1,0:T(8,128)(2,1)S(1)}, u32[]{:S(2)}, u32[]{:S(2)}) collective-permute-start(bf16[16,512]{1,0:T(8,128)(2,1)S(1)} %slice.14), channel_id=1, source_target_pairs={{0,4},{4,8},{8,12},{12,16},{16,20},{20,24},{24,28},{28,32},{32,36}... | collective-permute-start | bytes 49160 | tf_op jit(solution)/shard_map/ppermute | solution.py:372
  202.4 1.7 finish.1
  204.0 1.6 collective-permute-start.21
  205.6 1.8 collective-permute-start.23
  207.4 2.9 %collective-permute-done.21 = bf16[32,2048]{1,0:T(8,128)(2,1)S(1)} collective-permute-done((bf16[32,2048]{1,0:T(8,128)(2,1)S(1)}, bf16[32,2048]{1,0:T(8,128)(2,1)S(1)}, u32[]{:S(2)}, u32[]{:S(2)}) %collective-permute-start.21) | collective-permute-done | bytes 131104 | tf_op jit(solution)/shard_map/ppermute | solution.py:416
  210.8 3.0 %collective-permute-start.24 = (bf16[64,2048]{1,0:T(8,128)(2,1)S(1)}, bf16[64,2048]{1,0:T(8,128)(2,1)S(1)}, u32[]{:S(2)}, u32[]{:S(2)}) collective-permute-start(bf16[64,2048]{1,0:T(8,128)(2,1)S(1)} %pad_maximum_fusion.1), channel_id=1, source_target_pairs={{0,3},{1,0},{2,1},{3,2},{4,7},{5,4},{6,5},{7,6},{8,11},{9,8},{10,9... | collective-permute-start | bytes 786440 | tf_op jit(solution)/shard_map/ppermute | solution.py:423
  214.4 3.6 %collective-permute-done.22 = bf16[64,2048]{1,0:T(8,128)(2,1)S(1)} collective-permute-done((bf16[64,2048]{1,0:T(8,128)(2,1)S(1)}, bf16[64,2048]{1,0:T(8,128)(2,1)S(1)}, u32[]{:S(2)}, u32[]{:S(2)}) %collective-permute-start.22) | collective-permute-done | bytes 262176 | tf_op jit(solution)/shard_map/ppermute | solution.py:422
  (77 shorter events, 18.4 us)
Async XLA Ops:
  1.8 6.7 %collective-permute-start = (bf16[32,2048]{1,0:T(8,128)(2,1)S(1)}, bf16[32,2048]{1,0:T(8,128)(2,1)S(1)}, u32[]{:S(2)}, u32[]{:S(2)}) collective-permute-start(bf16[32,2048]{1,0:T(8,128)(2,1)S(1)} %get-tuple-element.35.p0a), channel_id=1, source_target_pairs={{0,1},{1,2},{2,3},{3,0},{4,5},{5,6},{6,7},{7,4},{8,9},{9,10},{10,1... | collective-permute-start | bytes 393224 | tf_op jit(solution)/shard_map/ppermute | solution.py:321
  3.3 6.4 %collective-permute-start.3 = (bf16[32,2048]{1,0:T(8,128)(2,1)S(1)}, bf16[32,2048]{1,0:T(8,128)(2,1)S(1)}, u32[]{:S(2)}, u32[]{:S(2)}) collective-permute-start(bf16[32,2048]{1,0:T(8,128)(2,1)S(1)} %get-tuple-element.36.p0b), channel_id=1, source_target_pairs={{0,3},{1,0},{2,1},{3,2},{4,7},{5,4},{6,5},{7,6},{8,11},{9,8},{10,9... | collective-permute-start | bytes 393224 | tf_op jit(solution)/shard_map/ppermute | solution.py:322
  5.1 8.9 %collective-permute-start.1 = (bf16[32,2048]{1,0:T(8,128)(2,1)S(1)}, bf16[32,2048]{1,0:T(8,128)(2,1)S(1)}, u32[]{:S(2)}, u32[]{:S(2)}) collective-permute-start(bf16[32,2048]{1,0:T(8,128)(2,1)S(1)} %get-tuple-element.36.p0b), channel_id=1, source_target_pairs={{0,1},{1,2},{2,3},{3,0},{4,5},{5,6},{6,7},{7,4},{8,9},{9,10},{10,1... | collective-permute-start | bytes 393224 | tf_op jit(solution)/shard_map/ppermute | solution.py:323
  5.4 8.7 %collective-permute-start.5 = (bf16[32,2048]{1,0:T(8,128)(2,1)S(1)}, bf16[32,2048]{1,0:T(8,128)(2,1)S(1)}, u32[]{:S(2)}, u32[]{:S(2)}) collective-permute-start(bf16[32,2048]{1,0:T(8,128)(2,1)S(1)} %get-tuple-element.35.p0a), channel_id=1, source_target_pairs={{0,3},{1,0},{2,1},{3,2},{4,7},{5,4},{6,5},{7,6},{8,11},{9,8},{10,9... | collective-permute-start | bytes 393224 | tf_op jit(solution)/shard_map/ppermute | solution.py:324
  8.4 6.2 %collective-permute-start.2 = (bf16[32,2048]{1,0:T(8,128)(2,1)S(1)}, bf16[32,2048]{1,0:T(8,128)(2,1)S(1)}, u32[]{:S(2)}, u32[]{:S(2)}) collective-permute-start(bf16[32,2048]{1,0:T(8,128)(2,1)S(1)} %collective-permute-done.p1a), channel_id=1, source_target_pairs={{0,1},{1,2},{2,3},{3,0},{4,5},{5,6},{6,7},{7,4},{8,9},{9,10},{10,1... | collective-permute-start | bytes 393224 | tf_op jit(solution)/shard_map/ppermute | solution.py:325
  16.1 14.6 %collective-permute-start.6 = (bf16[1,2,128,256]{3,2,1,0:T(8,128)(2,1)S(1)}, bf16[1,2,128,256]{3,2,1,0:T(8,128)(2,1)S(1)}, u32[]{:S(2)}, u32[]{:S(2)}) collective-permute-start(bf16[1,2,128,256]{3,2,1,0:T(8,128)(2,1)S(1)} %get-tuple-element.38.kv_ref.a), channel_id=1, source_target_pairs={{0,4},{4,0},{1,5},{5,1},{2,6},{6,2},{3,7},{7,3},{8,12},{12,8},{9,1... | collective-permute-start | bytes 393224 | tf_op jit(solution)/shard_map/ppermute | solution.py:343
  16.2 8.0 %collective-permute-start.10 = (bf16[1,2,128,256]{3,2,1,0:T(8,128)(2,1)S(1)}, bf16[1,2,128,256]{3,2,1,0:T(8,128)(2,1)S(1)}, u32[]{:S(2)}, u32[]{:S(2)}) collective-permute-start(bf16[1,2,128,256]{3,2,1,0:T(8,128)(2,1)S(1)} %get-tuple-element.38.kv_ref.a), channel_id=1, source_target_pairs={{0,16},{8,24},{16,0},{24,8},{1,17},{9,25},{17,1},{25,9},{2,18},{10... | collective-permute-start | bytes 393224 | tf_op jit(solution)/shard_map/ppermute | solution.py:347
  17.5 6.6 %collective-permute-start.8 = (bf16[1,2,128,256]{3,2,1,0:T(8,128)(2,1)S(1)}, bf16[1,2,128,256]{3,2,1,0:T(8,128)(2,1)S(1)}, u32[]{:S(2)}, u32[]{:S(2)}) collective-permute-start(bf16[1,2,128,256]{3,2,1,0:T(8,128)(2,1)S(1)} %get-tuple-element.38.kv_ref.a), channel_id=1, source_target_pairs={{0,8},{8,16},{16,24},{24,0},{1,9},{9,17},{17,25},{25,1},{2,10},{10... | collective-permute-start | bytes 393224 | tf_op jit(solution)/shard_map/ppermute | solution.py:347
  19.7 6.9 %collective-permute-start.9 = (bf16[1,2,128,256]{3,2,1,0:T(8,128)(2,1)S(1)}, bf16[1,2,128,256]{3,2,1,0:T(8,128)(2,1)S(1)}, u32[]{:S(2)}, u32[]{:S(2)}) collective-permute-start(bf16[1,2,128,256]{3,2,1,0:T(8,128)(2,1)S(1)} %get-tuple-element.38.kv_ref.a), channel_id=1, source_target_pairs={{0,24},{8,0},{16,8},{24,16},{1,25},{9,1},{17,9},{25,17},{2,26},{10... | collective-permute-start | bytes 393224 | tf_op jit(solution)/shard_map/ppermute | solution.py:347
  20.7 10.0 %collective-permute-start.7 = (bf16[512,256]{1,0:T(8,128)(2,1)S(1)}, bf16[512,256]{1,0:T(8,128)(2,1)S(1)}, u32[]{:S(2)}, u32[]{:S(2)}) collective-permute-start(bf16[512,256]{1,0:T(8,128)(2,1)S(1)} %fusion.14.q_own_ref), channel_id=1, source_target_pairs={{0,4},{4,0},{1,5},{5,1},{2,6},{6,2},{3,7},{7,3},{8,12},{12,8},{9,1... | collective-permute-start | bytes 786440 | tf_op jit(solution)/shard_map/ppermute | solution.py:369
  26.6 24.5 %collective-permute-start.11 = (bf16[4,2,128,256]{3,2,1,0:T(8,128)(2,1)S(1)}, bf16[4,2,128,256]{3,2,1,0:T(8,128)(2,1)S(1)}, u32[]{:S(2)}, u32[]{:S(2)}) collective-permute-start(bf16[4,2,128,256]{3,2,1,0:T(8,128)(2,1)S(1)} %join.1), channel_id=1, source_target_pairs={{0,32},{32,64},{64,96},{96,128},{128,160},{160,192},{192,224},{224... | collective-permute-start | bytes 1572872 | tf_op jit(solution)/shard_map/ppermute | solution.py:359
  26.7 26.0 %collective-permute-start.15 = (bf16[4,2,128,256]{3,2,1,0:T(8,128)(2,1)S(1)}, bf16[4,2,128,256]{3,2,1,0:T(8,128)(2,1)S(1)}, u32[]{:S(2)}, u32[]{:S(2)}) collective-permute-start(bf16[4,2,128,256]{3,2,1,0:T(8,128)(2,1)S(1)} %join.1), channel_id=1, source_target_pairs={{0,224},{32,0},{64,32},{96,64},{128,96},{160,128},{192,160},{224,1... | collective-permute-start | bytes 1572872 | tf_op jit(solution)/shard_map/ppermute | solution.py:360
  51.1 41.5 %collective-permute-start.12 = (bf16[4,2,128,256]{3,2,1,0:T(8,128)(2,1)S(1)}, bf16[4,2,128,256]{3,2,1,0:T(8,128)(2,1)S(1)}, u32[]{:S(2)}, u32[]{:S(2)}) collective-permute-start(bf16[4,2,128,256]{3,2,1,0:T(8,128)(2,1)S(1)} %collective-permute-done.11.refs_2_), channel_id=1, source_target_pairs={{0,32},{32,64},{64,96},{96,128},{128,160},{160,192},{192,224},{224... | collective-permute-start | bytes 1572872 | tf_op jit(solution)/shard_map/ppermute | solution.py:359
  52.7 40.0 %collective-permute-start.16 = (bf16[4,2,128,256]{3,2,1,0:T(8,128)(2,1)S(1)}, bf16[4,2,128,256]{3,2,1,0:T(8,128)(2,1)S(1)}, u32[]{:S(2)}, u32[]{:S(2)}) collective-permute-start(bf16[4,2,128,256]{3,2,1,0:T(8,128)(2,1)S(1)} %collective-permute-done.15.refs_3_), channel_id=1, source_target_pairs={{0,224},{32,0},{64,32},{96,64},{128,96},{160,128},{192,160},{224,1... | collective-permute-start | bytes 1572872 | tf_op jit(solution)/shard_map/ppermute | solution.py:360
  92.6 41.5 %collective-permute-start.13 = (bf16[4,2,128,256]{3,2,1,0:T(8,128)(2,1)S(1)}, bf16[4,2,128,256]{3,2,1,0:T(8,128)(2,1)S(1)}, u32[]{:S(2)}, u32[]{:S(2)}) collective-permute-start(bf16[4,2,128,256]{3,2,1,0:T(8,128)(2,1)S(1)} %collective-permute-done.12.refs_2_), channel_id=1, source_target_pairs={{0,32},{32,64},{64,96},{96,128},{128,160},{160,192},{192,224},{224... | collective-permute-start | bytes 1572872 | tf_op jit(solution)/shard_map/ppermute | solution.py:359
  92.7 41.7 %collective-permute-start.17 = (bf16[4,2,128,256]{3,2,1,0:T(8,128)(2,1)S(1)}, bf16[4,2,128,256]{3,2,1,0:T(8,128)(2,1)S(1)}, u32[]{:S(2)}, u32[]{:S(2)}) collective-permute-start(bf16[4,2,128,256]{3,2,1,0:T(8,128)(2,1)S(1)} %collective-permute-done.16.refs_3_), channel_id=1, source_target_pairs={{0,224},{32,0},{64,32},{96,64},{128,96},{160,128},{192,160},{224,1... | collective-permute-start | bytes 1572872 | tf_op jit(solution)/shard_map/ppermute | solution.py:360
  134.1 41.8 %collective-permute-start.14 = (bf16[2,2,128,256]{3,2,1,0:T(8,128)(2,1)S(1)}, bf16[2,2,128,256]{3,2,1,0:T(8,128)(2,1)S(1)}, u32[]{:S(2)}, u32[]{:S(2)}) collective-permute-start(bf16[2,2,128,256]{3,2,1,0:T(8,128)(2,1)S(1)} %slice.12), channel_id=1, source_target_pairs={{0,32},{32,64},{64,96},{96,128},{128,160},{160,192},{192,224},{224... | collective-permute-start | bytes 786440 | tf_op jit(solution)/shard_map/ppermute | solution.py:361
  134.5 41.5 %collective-permute-start.18 = (bf16[2,2,128,256]{3,2,1,0:T(8,128)(2,1)S(1)}, bf16[2,2,128,256]{3,2,1,0:T(8,128)(2,1)S(1)}, u32[]{:S(2)}, u32[]{:S(2)}) collective-permute-start(bf16[2,2,128,256]{3,2,1,0:T(8,128)(2,1)S(1)} %slice.13), channel_id=1, source_target_pairs={{0,224},{32,0},{64,32},{96,64},{128,96},{160,128},{192,160},{224,1... | collective-permute-start | bytes 786440 | tf_op jit(solution)/shard_map/ppermute | solution.py:362
  196.1 6.3 %collective-permute-start.19 = (f32[8,152,256]{2,1,0:T(8,128)S(1)}, f32[8,152,256]{2,1,0:T(8,128)S(1)}, u32[]{:S(2)}, u32[]{:S(2)}) collective-permute-start(f32[8,152,256]{2,1,0:T(8,128)S(1)} %get-tuple-element.54), channel_id=1, source_target_pairs={{0,4},{4,0},{1,5},{5,1},{2,6},{6,2},{3,7},{7,3},{8,12},{12,8},{9,1... | collective-permute-start | bytes 3735560 | tf_op jit(solution)/shard_map/ppermute | solution.py:394
  196.2 5.1 %collective-permute-start.20 = (bf16[16,512]{1,0:T(8,128)(2,1)S(1)}, bf16[16,512]{1,0:T(8,128)(2,1)S(1)}, u32[]{:S(2)}, u32[]{:S(2)}) collective-permute-start(bf16[16,512]{1,0:T(8,128)(2,1)S(1)} %slice.14), channel_id=1, source_target_pairs={{0,4},{4,8},{8,12},{12,16},{16,20},{20,24},{24,28},{28,32},{32,36}... | collective-permute-start | bytes 49160 | tf_op jit(solution)/shard_map/ppermute | solution.py:372
  204.0 6.3 %collective-permute-start.21 = (bf16[32,2048]{1,0:T(8,128)(2,1)S(1)}, bf16[32,2048]{1,0:T(8,128)(2,1)S(1)}, u32[]{:S(2)}, u32[]{:S(2)}) collective-permute-start(bf16[32,2048]{1,0:T(8,128)(2,1)S(1)} %get-tuple-element.62), channel_id=1, source_target_pairs={{0,1},{1,2},{2,3},{3,0},{4,5},{5,6},{6,7},{7,4},{8,9},{9,10},{10,1... | collective-permute-start | bytes 393224 | tf_op jit(solution)/shard_map/ppermute | solution.py:416
  205.6 5.1 %collective-permute-start.23 = (bf16[32,2048]{1,0:T(8,128)(2,1)S(1)}, bf16[32,2048]{1,0:T(8,128)(2,1)S(1)}, u32[]{:S(2)}, u32[]{:S(2)}) collective-permute-start(bf16[32,2048]{1,0:T(8,128)(2,1)S(1)} %get-tuple-element.66), channel_id=1, source_target_pairs={{0,3},{1,0},{2,1},{3,2},{4,7},{5,4},{6,5},{7,6},{8,11},{9,8},{10,9... | collective-permute-start | bytes 393224 | tf_op jit(solution)/shard_map/ppermute | solution.py:417
  210.4 7.7 %collective-permute-start.22 = (bf16[64,2048]{1,0:T(8,128)(2,1)S(1)}, bf16[64,2048]{1,0:T(8,128)(2,1)S(1)}, u32[]{:S(2)}, u32[]{:S(2)}) collective-permute-start(bf16[64,2048]{1,0:T(8,128)(2,1)S(1)} %pad_maximum_fusion), channel_id=1, source_target_pairs={{0,1},{1,2},{2,3},{3,0},{4,5},{5,6},{6,7},{7,4},{8,9},{9,10},{10,1... | collective-permute-start | bytes 786440 | tf_op jit(solution)/shard_map/ppermute | solution.py:422
  210.8 7.2 %collective-permute-start.24 = (bf16[64,2048]{1,0:T(8,128)(2,1)S(1)}, bf16[64,2048]{1,0:T(8,128)(2,1)S(1)}, u32[]{:S(2)}, u32[]{:S(2)}) collective-permute-start(bf16[64,2048]{1,0:T(8,128)(2,1)S(1)} %pad_maximum_fusion.1), channel_id=1, source_target_pairs={{0,3},{1,0},{2,1},{3,2},{4,7},{5,4},{6,5},{7,6},{8,11},{9,8},{10,9... | collective-permute-start | bytes 786440 | tf_op jit(solution)/shard_map/ppermute | solution.py:423
  (13 other events, 74.6 us)

commit v9 on v8

--- a/solution.py
+++ b/solution.py
@@ -58,8 +58,8 @@
     probs = (p_a, p_b)
 
     def scores(i, slot):
-        s = jnp.where(seen, dot(keys, q_ref[i]), NEG)
-        seed = jnp.max(jnp.where(diagonal, dot(oth_keys, q_ref[i, :, ROWS:]), NEG), axis=0, keepdims=True)
+        s = jnp.where(seen, dot(keys, q_ref[i]) * LOG2E, NEG)
+        seed = jnp.max(jnp.where(diagonal, dot(oth_keys, q_ref[i, :, ROWS:]) * LOG2E, NEG), axis=0, keepdims=True)
         top = jnp.max(s, axis=0, keepdims=True)
         top = jnp.concatenate([top[:, :ROWS], jnp.maximum(top[:, ROWS:], seed)], axis=1)
         probs[slot][...] = jnp.exp2(s - top).astype(BF16)
@@ -153,8 +153,12 @@
             at += count
 
     def keep_state():
-        own_ref[...] = own_in[...]
-        oth_ref[...] = oth_in[...]
+        def one_map(i, carry):
+            own_ref[i] = own_in[i]
+            oth_ref[i] = oth_in[i]
+            return carry
+
+        lax.fori_loop(0, MAPS, one_map, 0)
 
     pl.when(visible == 0)(keep_state)
 
@@ -178,7 +182,7 @@
 
             def scores(i, slot):
                 top = jnp.concatenate([own_in[i, 144:145], oth_in[i, 144:145]], axis=1)
-                s = dot(keys, q_ref[i]) - top
+                s = dot(keys, q_ref[i]) * LOG2E - top
                 over_ref[i] = jnp.maximum(over_ref[i], jnp.max(s.reshape(-1, 8, 2 * ROWS), axis=0))
                 probs[slot][...] = jnp.exp2(s).astype(BF16)
 
@@ -215,7 +219,7 @@
 
                 def one_map(i, carry):
                     before = jnp.concatenate([own_ref[i, 144:145], oth_ref[i, 144:145]], axis=1)
-                    s = dot(keys_ref[:ROWS], q_ref[i])
+                    s = dot(keys_ref[:ROWS], q_ref[i]) * LOG2E
                     top = jnp.maximum(before, jnp.max(s, axis=0, keepdims=True))
                     scale = jnp.exp2(before - top)
                     out = dot(values_ref[:, :ROWS], jnp.exp2(s - top).astype(BF16))
@@ -361,7 +365,7 @@
     up.append(lax.ppermute(up[3][:2], "z", ring(8, 1)))
     down.append(lax.ppermute(down[3][2:], "z", ring(8, -1)))
 
-    scale = (query_weight.shape[2] // 2) ** -0.5 * LOG2E
+    scale = (query_weight.shape[2] // 2) ** -0.5
     query_w = query_weight.reshape(width, -1)
     q_own = (
         lax.dot_general(query_w, normed, (((0,), (1,)), ((), ())), preferred_element_type=F32) * scale

time: 220 us -> 222 us (level)
  no operation moved by 1% of the time
where the time goes in v9:
time: 222 us; the launch traced here: 221 us
  Pallas kernels  165 us (74%)
  starting transfers between devices  31.3 us (14%)
  waiting for transfers between devices  14.4 us (6%)
  local copies, waits for them, and re-layouts  5.08 us (2%)
  matrix products  2.99 us (1%)
    pallas_call x5, Pallas kernels, attend_chunk(): pl.pallas_call(functools.partial(chunk_kernel, plan, n, rolled), out_shap...  157 us
    ppermute x3, waiting for transfers between devices, local(): beside.append(lax.ppermute(kv, 'y', ring(4, step)))  5.76 us
    ppermute x3, starting transfers between devices, local(): down.append(lax.ppermute(down[-1], 'z', ring(8, -1)))  4.57 us
  transfers between devices with their start and end apart: 25, of which 8 were waited for; matrix products, arithmetic and copies ran while one was open for 2% of the time, Pallas kernels for 64%

profile of v9, /device:TPU:248, one launch (start us, length us, event | category | flops | bytes accessed | tf_op | source)
XLA Modules:
  0.0 220.8 jit_solution(936283448824443061)
XLA Ops:
  1.8 1.6 collective-permute-start
  3.3 1.7 collective-permute-start.3
  5.4 3.0 %collective-permute-start.5 = (bf16[32,2048]{1,0:T(8,128)(2,1)S(1)}, bf16[32,2048]{1,0:T(8,128)(2,1)S(1)}, u32[]{:S(2)}, u32[]{:S(2)}) collective-permute-start(bf16[32,2048]{1,0:T(8,128)(2,1)S(1)} %get-tuple-element.35.p0a), channel_id=1, source_target_pairs={{0,3},{1,0},{2,1},{3,2},{4,7},{5,4},{6,5},{7,6},{8,11},{9,8},{10,9... | collective-permute-start | bytes 393224 | tf_op jit(solution)/shard_map/ppermute | solution.py:328
  9.7 2.0 collective-permute-start.4
  17.5 2.2 collective-permute-start.8
  20.8 3.3 %collective-permute-done.10.d.refs_4_ = bf16[1,2,128,256]{3,2,1,0:T(8,128)(2,1)S(1)} collective-permute-done((bf16[1,2,128,256]{3,2,1,0:T(8,128)(2,1)S(1)}, bf16[1,2,128,256]{3,2,1,0:T(8,128)(2,1)S(1)}, u32[]{:S(2)}, u32[]{:S(2)}) %collective-permute-start.10) | collective-permute-done | bytes 131104 | tf_op jit(solution)/shard_map/ppermute | solution.py:351
  24.2 2.4 %collective-permute-done.9.c.refs_3_ = bf16[1,2,128,256]{3,2,1,0:T(8,128)(2,1)S(1)} collective-permute-done((bf16[1,2,128,256]{3,2,1,0:T(8,128)(2,1)S(1)}, bf16[1,2,128,256]{3,2,1,0:T(8,128)(2,1)S(1)}, u32[]{:S(2)}, u32[]{:S(2)}) %collective-permute-start.9) | collective-permute-done | bytes 131104 | tf_op jit(solution)/shard_map/ppermute | solution.py:351
  26.7 2.0 collective-permute-start.15
  30.7 3.2 %first.1 = (f32[8,152,256]{2,1,0:T(8,128)S(1)}, f32[8,152,256]{2,1,0:T(8,128)S(1)}, bf16[8,128,512]{2,1,0:T(8,128)(2,1)S(1)}) custom-call(s32[4]{0:T(128)S(1)} %pad_add_fusion.place_ref.refs_0_, bf16[1,2,128,256]{3,2,1,0:T(8,128)(2,1)S(1)} %get-tuple-element.38.kv_ref.a, bf16[1,2,128,256]{3,2,1,0:T(8,128)(2,1)S(1)} %collective-permute-done.6.oth_kv_ref, ...), custom_call_target="tpu_custom_call" | custom-call | tf_op jit(solution)/shard_map/first/pallas_call | solution.py:381
  33.9 17.7 %shard_map.131 = (f32[8,152,256]{2,1,0:T(8,128)S(1)}, f32[8,152,256]{2,1,0:T(8,128)S(1)}) custom-call(s32[4]{0:T(128)S(1)} %pad_add_fusion.place_ref.refs_0_, bf16[8,128,512]{2,1,0:T(8,128)(2,1)S(1)} %get-tuple-element.41.refs_1_, bf16[1,2,128,256]{3,2,1,0:T(8,128)(2,1)S(1)} %collective-permute-done.8.b.refs_2_, ...), custom_call_target="tpu_custom_call" | custom-call | flops 3221225472 | bytes 1048576 | tf_op jit(solution)/shard_map/pallas_call | solution.py:248
  51.5 1.6 collective-permute-start.12
  53.7 39.8 %shard_map.132 = (f32[8,152,256]{2,1,0:T(8,128)S(1)}, f32[8,152,256]{2,1,0:T(8,128)S(1)}) custom-call(s32[4]{0:T(128)S(1)} %pad_add_fusion.place_ref.refs_0_, bf16[8,128,512]{2,1,0:T(8,128)(2,1)S(1)} %get-tuple-element.41.refs_1_, bf16[4,2,128,256]{3,2,1,0:T(8,128)(2,1)S(1)} %collective-permute-done.11.refs_2_, ...), custom_call_target="tpu_custom_call" | custom-call | flops 8589934592 | bytes 1048576 | tf_op jit(solution)/shard_map/pallas_call | solution.py:248
  93.6 2.0 collective-permute-start.17
  95.6 39.8 %shard_map.133 = (f32[8,152,256]{2,1,0:T(8,128)S(1)}, f32[8,152,256]{2,1,0:T(8,128)S(1)}) custom-call(s32[4]{0:T(128)S(1)} %pad_add_fusion.place_ref.refs_0_, bf16[8,128,512]{2,1,0:T(8,128)(2,1)S(1)} %get-tuple-element.41.refs_1_, bf16[4,2,128,256]{3,2,1,0:T(8,128)(2,1)S(1)} %collective-permute-done.12.refs_2_, ...), custom_call_target="tpu_custom_call" | custom-call | flops 8589934592 | bytes 1048576 | tf_op jit(solution)/shard_map/pallas_call | solution.py:248
  135.5 2.3 %collective-permute-start.18 = (bf16[2,2,128,256]{3,2,1,0:T(8,128)(2,1)S(1)}, bf16[2,2,128,256]{3,2,1,0:T(8,128)(2,1)S(1)}, u32[]{:S(2)}, u32[]{:S(2)}) collective-permute-start(bf16[2,2,128,256]{3,2,1,0:T(8,128)(2,1)S(1)} %slice.13), channel_id=1, source_target_pairs={{0,224},{32,0},{64,32},{96,64},{128,96},{160,128},{192,160},{224,1... | collective-permute-start | bytes 786440 | tf_op jit(solution)/shard_map/ppermute | solution.py:366
  137.8 39.8 %shard_map.134 = (f32[8,152,256]{2,1,0:T(8,128)S(1)}, f32[8,152,256]{2,1,0:T(8,128)S(1)}) custom-call(s32[4]{0:T(128)S(1)} %pad_add_fusion.place_ref.refs_0_, bf16[8,128,512]{2,1,0:T(8,128)(2,1)S(1)} %get-tuple-element.41.refs_1_, bf16[4,2,128,256]{3,2,1,0:T(8,128)(2,1)S(1)} %collective-permute-done.13.refs_2_, ...), custom_call_target="tpu_custom_call" | custom-call | flops 8589934592 | bytes 1048576 | tf_op jit(solution)/shard_map/pallas_call | solution.py:248
  177.7 20.3 %shard_map.135 = (f32[8,152,256]{2,1,0:T(8,128)S(1)}, f32[8,152,256]{2,1,0:T(8,128)S(1)}) custom-call(s32[4]{0:T(128)S(1)} %pad_add_fusion.place_ref.refs_0_, bf16[8,128,512]{2,1,0:T(8,128)(2,1)S(1)} %get-tuple-element.41.refs_1_, bf16[2,2,128,256]{3,2,1,0:T(8,128)(2,1)S(1)} %collective-permute-done.14.refs_2_, ...), custom_call_target="tpu_custom_call" | custom-call | flops 4294967296 | bytes 1048576 | tf_op jit(solution)/shard_map/pallas_call | solution.py:248
  198.1 2.4 %collective-permute-start.20 = (bf16[16,512]{1,0:T(8,128)(2,1)S(1)}, bf16[16,512]{1,0:T(8,128)(2,1)S(1)}, u32[]{:S(2)}, u32[]{:S(2)}) collective-permute-start(bf16[16,512]{1,0:T(8,128)(2,1)S(1)} %slice.14), channel_id=1, source_target_pairs={{0,4},{4,8},{8,12},{12,16},{16,20},{20,24},{24,28},{28,32},{32,36}... | collective-permute-start | bytes 49160 | tf_op jit(solution)/shard_map/ppermute | solution.py:376
  204.3 1.7 finish.1
  206.0 1.6 collective-permute-start.21
  207.5 1.8 collective-permute-start.23
  209.3 2.9 %collective-permute-done.21 = bf16[32,2048]{1,0:T(8,128)(2,1)S(1)} collective-permute-done((bf16[32,2048]{1,0:T(8,128)(2,1)S(1)}, bf16[32,2048]{1,0:T(8,128)(2,1)S(1)}, u32[]{:S(2)}, u32[]{:S(2)}) %collective-permute-start.21) | collective-permute-done | bytes 131104 | tf_op jit(solution)/shard_map/ppermute | solution.py:420
  212.7 3.0 %collective-permute-start.24 = (bf16[64,2048]{1,0:T(8,128)(2,1)S(1)}, bf16[64,2048]{1,0:T(8,128)(2,1)S(1)}, u32[]{:S(2)}, u32[]{:S(2)}) collective-permute-start(bf16[64,2048]{1,0:T(8,128)(2,1)S(1)} %pad_maximum_fusion.1), channel_id=1, source_target_pairs={{0,3},{1,0},{2,1},{3,2},{4,7},{5,4},{6,5},{7,6},{8,11},{9,8},{10,9... | collective-permute-start | bytes 786440 | tf_op jit(solution)/shard_map/ppermute | solution.py:427
  216.4 3.6 %collective-permute-done.22 = bf16[64,2048]{1,0:T(8,128)(2,1)S(1)} collective-permute-done((bf16[64,2048]{1,0:T(8,128)(2,1)S(1)}, bf16[64,2048]{1,0:T(8,128)(2,1)S(1)}, u32[]{:S(2)}, u32[]{:S(2)}) %collective-permute-start.22) | collective-permute-done | bytes 262176 | tf_op jit(solution)/shard_map/ppermute | solution.py:426
  (77 shorter events, 18.2 us)
Async XLA Ops:
  1.8 6.7 %collective-permute-start = (bf16[32,2048]{1,0:T(8,128)(2,1)S(1)}, bf16[32,2048]{1,0:T(8,128)(2,1)S(1)}, u32[]{:S(2)}, u32[]{:S(2)}) collective-permute-start(bf16[32,2048]{1,0:T(8,128)(2,1)S(1)} %get-tuple-element.35.p0a), channel_id=1, source_target_pairs={{0,1},{1,2},{2,3},{3,0},{4,5},{5,6},{6,7},{7,4},{8,9},{9,10},{10,1... | collective-permute-start | bytes 393224 | tf_op jit(solution)/shard_map/ppermute | solution.py:325
  3.3 6.4 %collective-permute-start.3 = (bf16[32,2048]{1,0:T(8,128)(2,1)S(1)}, bf16[32,2048]{1,0:T(8,128)(2,1)S(1)}, u32[]{:S(2)}, u32[]{:S(2)}) collective-permute-start(bf16[32,2048]{1,0:T(8,128)(2,1)S(1)} %get-tuple-element.36.p0b), channel_id=1, source_target_pairs={{0,3},{1,0},{2,1},{3,2},{4,7},{5,4},{6,5},{7,6},{8,11},{9,8},{10,9... | collective-permute-start | bytes 393224 | tf_op jit(solution)/shard_map/ppermute | solution.py:326
  5.1 8.9 %collective-permute-start.1 = (bf16[32,2048]{1,0:T(8,128)(2,1)S(1)}, bf16[32,2048]{1,0:T(8,128)(2,1)S(1)}, u32[]{:S(2)}, u32[]{:S(2)}) collective-permute-start(bf16[32,2048]{1,0:T(8,128)(2,1)S(1)} %get-tuple-element.36.p0b), channel_id=1, source_target_pairs={{0,1},{1,2},{2,3},{3,0},{4,5},{5,6},{6,7},{7,4},{8,9},{9,10},{10,1... | collective-permute-start | bytes 393224 | tf_op jit(solution)/shard_map/ppermute | solution.py:327
  5.4 8.7 %collective-permute-start.5 = (bf16[32,2048]{1,0:T(8,128)(2,1)S(1)}, bf16[32,2048]{1,0:T(8,128)(2,1)S(1)}, u32[]{:S(2)}, u32[]{:S(2)}) collective-permute-start(bf16[32,2048]{1,0:T(8,128)(2,1)S(1)} %get-tuple-element.35.p0a), channel_id=1, source_target_pairs={{0,3},{1,0},{2,1},{3,2},{4,7},{5,4},{6,5},{7,6},{8,11},{9,8},{10,9... | collective-permute-start | bytes 393224 | tf_op jit(solution)/shard_map/ppermute | solution.py:328
  8.4 6.2 %collective-permute-start.2 = (bf16[32,2048]{1,0:T(8,128)(2,1)S(1)}, bf16[32,2048]{1,0:T(8,128)(2,1)S(1)}, u32[]{:S(2)}, u32[]{:S(2)}) collective-permute-start(bf16[32,2048]{1,0:T(8,128)(2,1)S(1)} %collective-permute-done.p1a), channel_id=1, source_target_pairs={{0,1},{1,2},{2,3},{3,0},{4,5},{5,6},{6,7},{7,4},{8,9},{9,10},{10,1... | collective-permute-start | bytes 393224 | tf_op jit(solution)/shard_map/ppermute | solution.py:329
  16.1 14.6 %collective-permute-start.6 = (bf16[1,2,128,256]{3,2,1,0:T(8,128)(2,1)S(1)}, bf16[1,2,128,256]{3,2,1,0:T(8,128)(2,1)S(1)}, u32[]{:S(2)}, u32[]{:S(2)}) collective-permute-start(bf16[1,2,128,256]{3,2,1,0:T(8,128)(2,1)S(1)} %get-tuple-element.38.kv_ref.a), channel_id=1, source_target_pairs={{0,4},{4,0},{1,5},{5,1},{2,6},{6,2},{3,7},{7,3},{8,12},{12,8},{9,1... | collective-permute-start | bytes 393224 | tf_op jit(solution)/shard_map/ppermute | solution.py:347
  16.2 8.0 %collective-permute-start.10 = (bf16[1,2,128,256]{3,2,1,0:T(8,128)(2,1)S(1)}, bf16[1,2,128,256]{3,2,1,0:T(8,128)(2,1)S(1)}, u32[]{:S(2)}, u32[]{:S(2)}) collective-permute-start(bf16[1,2,128,256]{3,2,1,0:T(8,128)(2,1)S(1)} %get-tuple-element.38.kv_ref.a), channel_id=1, source_target_pairs={{0,16},{8,24},{16,0},{24,8},{1,17},{9,25},{17,1},{25,9},{2,18},{10... | collective-permute-start | bytes 393224 | tf_op jit(solution)/shard_map/ppermute | solution.py:351
  17.5 6.6 %collective-permute-start.8 = (bf16[1,2,128,256]{3,2,1,0:T(8,128)(2,1)S(1)}, bf16[1,2,128,256]{3,2,1,0:T(8,128)(2,1)S(1)}, u32[]{:S(2)}, u32[]{:S(2)}) collective-permute-start(bf16[1,2,128,256]{3,2,1,0:T(8,128)(2,1)S(1)} %get-tuple-element.38.kv_ref.a), channel_id=1, source_target_pairs={{0,8},{8,16},{16,24},{24,0},{1,9},{9,17},{17,25},{25,1},{2,10},{10... | collective-permute-start | bytes 393224 | tf_op jit(solution)/shard_map/ppermute | solution.py:351
  19.7 6.9 %collective-permute-start.9 = (bf16[1,2,128,256]{3,2,1,0:T(8,128)(2,1)S(1)}, bf16[1,2,128,256]{3,2,1,0:T(8,128)(2,1)S(1)}, u32[]{:S(2)}, u32[]{:S(2)}) collective-permute-start(bf16[1,2,128,256]{3,2,1,0:T(8,128)(2,1)S(1)} %get-tuple-element.38.kv_ref.a), channel_id=1, source_target_pairs={{0,24},{8,0},{16,8},{24,16},{1,25},{9,1},{17,9},{25,17},{2,26},{10... | collective-permute-start | bytes 393224 | tf_op jit(solution)/shard_map/ppermute | solution.py:351
  20.7 10.0 %collective-permute-start.7 = (bf16[512,256]{1,0:T(8,128)(2,1)S(1)}, bf16[512,256]{1,0:T(8,128)(2,1)S(1)}, u32[]{:S(2)}, u32[]{:S(2)}) collective-permute-start(bf16[512,256]{1,0:T(8,128)(2,1)S(1)} %fusion.14.q_own_ref), channel_id=1, source_target_pairs={{0,4},{4,0},{1,5},{5,1},{2,6},{6,2},{3,7},{7,3},{8,12},{12,8},{9,1... | collective-permute-start | bytes 786440 | tf_op jit(solution)/shard_map/ppermute | solution.py:373
  26.6 24.9 %collective-permute-start.11 = (bf16[4,2,128,256]{3,2,1,0:T(8,128)(2,1)S(1)}, bf16[4,2,128,256]{3,2,1,0:T(8,128)(2,1)S(1)}, u32[]{:S(2)}, u32[]{:S(2)}) collective-permute-start(bf16[4,2,128,256]{3,2,1,0:T(8,128)(2,1)S(1)} %join.1), channel_id=1, source_target_pairs={{0,32},{32,64},{64,96},{96,128},{128,160},{160,192},{192,224},{224... | collective-permute-start | bytes 1572872 | tf_op jit(solution)/shard_map/ppermute | solution.py:363
  26.7 26.4 %collective-permute-start.15 = (bf16[4,2,128,256]{3,2,1,0:T(8,128)(2,1)S(1)}, bf16[4,2,128,256]{3,2,1,0:T(8,128)(2,1)S(1)}, u32[]{:S(2)}, u32[]{:S(2)}) collective-permute-start(bf16[4,2,128,256]{3,2,1,0:T(8,128)(2,1)S(1)} %join.1), channel_id=1, source_target_pairs={{0,224},{32,0},{64,32},{96,64},{128,96},{160,128},{192,160},{224,1... | collective-permute-start | bytes 1572872 | tf_op jit(solution)/shard_map/ppermute | solution.py:364
  51.5 41.9 %collective-permute-start.12 = (bf16[4,2,128,256]{3,2,1,0:T(8,128)(2,1)S(1)}, bf16[4,2,128,256]{3,2,1,0:T(8,128)(2,1)S(1)}, u32[]{:S(2)}, u32[]{:S(2)}) collective-permute-start(bf16[4,2,128,256]{3,2,1,0:T(8,128)(2,1)S(1)} %collective-permute-done.11.refs_2_), channel_id=1, source_target_pairs={{0,32},{32,64},{64,96},{96,128},{128,160},{160,192},{192,224},{224... | collective-permute-start | bytes 1572872 | tf_op jit(solution)/shard_map/ppermute | solution.py:363
  53.1 40.5 %collective-permute-start.16 = (bf16[4,2,128,256]{3,2,1,0:T(8,128)(2,1)S(1)}, bf16[4,2,128,256]{3,2,1,0:T(8,128)(2,1)S(1)}, u32[]{:S(2)}, u32[]{:S(2)}) collective-permute-start(bf16[4,2,128,256]{3,2,1,0:T(8,128)(2,1)S(1)} %collective-permute-done.15.refs_3_), channel_id=1, source_target_pairs={{0,224},{32,0},{64,32},{96,64},{128,96},{160,128},{192,160},{224,1... | collective-permute-start | bytes 1572872 | tf_op jit(solution)/shard_map/ppermute | solution.py:364
  93.5 41.9 %collective-permute-start.13 = (bf16[4,2,128,256]{3,2,1,0:T(8,128)(2,1)S(1)}, bf16[4,2,128,256]{3,2,1,0:T(8,128)(2,1)S(1)}, u32[]{:S(2)}, u32[]{:S(2)}) collective-permute-start(bf16[4,2,128,256]{3,2,1,0:T(8,128)(2,1)S(1)} %collective-permute-done.12.refs_2_), channel_id=1, source_target_pairs={{0,32},{32,64},{64,96},{96,128},{128,160},{160,192},{192,224},{224... | collective-permute-start | bytes 1572872 | tf_op jit(solution)/shard_map/ppermute | solution.py:363
  93.6 41.9 %collective-permute-start.17 = (bf16[4,2,128,256]{3,2,1,0:T(8,128)(2,1)S(1)}, bf16[4,2,128,256]{3,2,1,0:T(8,128)(2,1)S(1)}, u32[]{:S(2)}, u32[]{:S(2)}) collective-permute-start(bf16[4,2,128,256]{3,2,1,0:T(8,128)(2,1)S(1)} %collective-permute-done.16.refs_3_), channel_id=1, source_target_pairs={{0,224},{32,0},{64,32},{96,64},{128,96},{160,128},{192,160},{224,1... | collective-permute-start | bytes 1572872 | tf_op jit(solution)/shard_map/ppermute | solution.py:364
  135.4 42.2 %collective-permute-start.14 = (bf16[2,2,128,256]{3,2,1,0:T(8,128)(2,1)S(1)}, bf16[2,2,128,256]{3,2,1,0:T(8,128)(2,1)S(1)}, u32[]{:S(2)}, u32[]{:S(2)}) collective-permute-start(bf16[2,2,128,256]{3,2,1,0:T(8,128)(2,1)S(1)} %slice.12), channel_id=1, source_target_pairs={{0,32},{32,64},{64,96},{96,128},{128,160},{160,192},{192,224},{224... | collective-permute-start | bytes 786440 | tf_op jit(solution)/shard_map/ppermute | solution.py:365
  135.5 42.1 %collective-permute-start.18 = (bf16[2,2,128,256]{3,2,1,0:T(8,128)(2,1)S(1)}, bf16[2,2,128,256]{3,2,1,0:T(8,128)(2,1)S(1)}, u32[]{:S(2)}, u32[]{:S(2)}) collective-permute-start(bf16[2,2,128,256]{3,2,1,0:T(8,128)(2,1)S(1)} %slice.13), channel_id=1, source_target_pairs={{0,224},{32,0},{64,32},{96,64},{128,96},{160,128},{192,160},{224,1... | collective-permute-start | bytes 786440 | tf_op jit(solution)/shard_map/ppermute | solution.py:366
  198.0 6.3 %collective-permute-start.19 = (f32[8,152,256]{2,1,0:T(8,128)S(1)}, f32[8,152,256]{2,1,0:T(8,128)S(1)}, u32[]{:S(2)}, u32[]{:S(2)}) collective-permute-start(f32[8,152,256]{2,1,0:T(8,128)S(1)} %get-tuple-element.54), channel_id=1, source_target_pairs={{0,4},{4,0},{1,5},{5,1},{2,6},{6,2},{3,7},{7,3},{8,12},{12,8},{9,1... | collective-permute-start | bytes 3735560 | tf_op jit(solution)/shard_map/ppermute | solution.py:398
  198.1 5.1 %collective-permute-start.20 = (bf16[16,512]{1,0:T(8,128)(2,1)S(1)}, bf16[16,512]{1,0:T(8,128)(2,1)S(1)}, u32[]{:S(2)}, u32[]{:S(2)}) collective-permute-start(bf16[16,512]{1,0:T(8,128)(2,1)S(1)} %slice.14), channel_id=1, source_target_pairs={{0,4},{4,8},{8,12},{12,16},{16,20},{20,24},{24,28},{28,32},{32,36}... | collective-permute-start | bytes 49160 | tf_op jit(solution)/shard_map/ppermute | solution.py:376
  206.0 6.3 %collective-permute-start.21 = (bf16[32,2048]{1,0:T(8,128)(2,1)S(1)}, bf16[32,2048]{1,0:T(8,128)(2,1)S(1)}, u32[]{:S(2)}, u32[]{:S(2)}) collective-permute-start(bf16[32,2048]{1,0:T(8,128)(2,1)S(1)} %get-tuple-element.62), channel_id=1, source_target_pairs={{0,1},{1,2},{2,3},{3,0},{4,5},{5,6},{6,7},{7,4},{8,9},{9,10},{10,1... | collective-permute-start | bytes 393224 | tf_op jit(solution)/shard_map/ppermute | solution.py:420
  207.5 5.1 %collective-permute-start.23 = (bf16[32,2048]{1,0:T(8,128)(2,1)S(1)}, bf16[32,2048]{1,0:T(8,128)(2,1)S(1)}, u32[]{:S(2)}, u32[]{:S(2)}) collective-permute-start(bf16[32,2048]{1,0:T(8,128)(2,1)S(1)} %get-tuple-element.66), channel_id=1, source_target_pairs={{0,3},{1,0},{2,1},{3,2},{4,7},{5,4},{6,5},{7,6},{8,11},{9,8},{10,9... | collective-permute-start | bytes 393224 | tf_op jit(solution)/shard_map/ppermute | solution.py:421
  212.3 7.7 %collective-permute-start.22 = (bf16[64,2048]{1,0:T(8,128)(2,1)S(1)}, bf16[64,2048]{1,0:T(8,128)(2,1)S(1)}, u32[]{:S(2)}, u32[]{:S(2)}) collective-permute-start(bf16[64,2048]{1,0:T(8,128)(2,1)S(1)} %pad_maximum_fusion), channel_id=1, source_target_pairs={{0,1},{1,2},{2,3},{3,0},{4,5},{5,6},{6,7},{7,4},{8,9},{9,10},{10,1... | collective-permute-start | bytes 786440 | tf_op jit(solution)/shard_map/ppermute | solution.py:426
  212.7 7.2 %collective-permute-start.24 = (bf16[64,2048]{1,0:T(8,128)(2,1)S(1)}, bf16[64,2048]{1,0:T(8,128)(2,1)S(1)}, u32[]{:S(2)}, u32[]{:S(2)}) collective-permute-start(bf16[64,2048]{1,0:T(8,128)(2,1)S(1)} %pad_maximum_fusion.1), channel_id=1, source_target_pairs={{0,3},{1,0},{2,1},{3,2},{4,7},{5,4},{6,5},{7,6},{8,11},{9,8},{10,9... | collective-permute-start | bytes 786440 | tf_op jit(solution)/shard_map/ppermute | solution.py:427
  (13 other events, 74.6 us)
